TPU v7x, 512 devices: a 4x2x32 block of a 4x8x32 slice. The times are simulated.
512 devices in a mesh: grp: 2 (over y), kv: 32 (over z), tp: 8 (over x, core).
Axes of the slice: x: 4, y: 2, z: 32, core: 2. Of those that a mesh axis runs over, the one named last changes fastest.
The devices are a block of a 4x8x32 slice.
Arguments:
- tokens: bfloat16 [48, 4096], P('grp', ('kv', 'tp')), parts along dimension 0, may hold values from -12 to 12
- lengths: int32 [48], P('grp'), parts along dimension 0, may hold values from 1 to 1024, 12288 in all
- attn_gain: float32 [4096], P('kv'), may hold values from 0.1 to 1.9
- w_query: bfloat16 [4096, 4096], P('kv', 'tp'), may hold values from -0.09375 to 0.09375
- w_key: bfloat16 [4096, 4096], P('kv', 'tp'), may hold values from -0.09375 to 0.09375
- w_value: bfloat16 [4096, 4096], P('kv', 'tp'), may hold values from -0.09375 to 0.09375
- w_gate: bfloat16 [4096, 4096], P('kv', 'tp'), may hold values from -0.09375 to 0.09375
- log_decay: float32 [16], P('tp'), may hold values from -1 to 0
- key_cache: bfloat16 [48, 1024, 4096], P('grp', 'kv', 'tp'), parts along dimension 0, may hold values from -6 to 6
- value_cache: bfloat16 [48, 1024, 4096], P('grp', 'kv', 'tp'), parts along dimension 0, may hold values from -6 to 6
- gn_gain: float32 [4096], P('tp'), may hold values from 0.1 to 1.9
- w_out: bfloat16 [4096, 4096], P('tp', 'kv'), may hold values from -0.1875 to 0.1875
- ffn_gain: float32 [4096], P('kv'), may hold values from 0.1 to 1.9
- w_ffn_gate: bfloat16 [4096, 11264], P('kv', 'tp'), may hold values from -0.09375 to 0.09375
- w_ffn_up: bfloat16 [4096, 11264], P('kv', 'tp'), may hold values from -0.09375 to 0.09375
- w_ffn_down: bfloat16 [11264, 4096], P('tp', 'kv'), may hold values from -0.109375 to 0.109375
Outputs:
- layer_out: bfloat16 [48, 4096], P('grp', ('kv', 'tp')), parts along dimension 0
There are 2 independent parts, one for each index of `grp`. A program takes and returns all parts, laid end to end along the dimension named above; an argument that names none is the same for every part. Nothing has to cross between parts.
All inputs are finite; a program needn't handle non-finite values.
Results may differ from a plain program's by a relative error of at most 0.012.
Values may be sent and summed in bfloat16 or wider, within the bound.
No kernel may reach another device: no remote copies, remote signals or barrier semaphores. Data moves between devices by JAX's collectives and lax.ppermute only.
A program may use at most 64 MiB of HBM per device.

v0:
```python
import jax
import jax.numpy as jnp
from jax import lax
from jax.sharding import PartitionSpec as P

DK = 256
D = 4096


RMS_EPS = 0.1
GN_EPS = 1.0
ROPE_BASE = 10000.0


def from_everyone(array, axis):
    copies = jnp.broadcast_to(array, (lax.axis_size(axis), *array.shape))
    return lax.all_to_all(copies, axis, split_axis=0, concat_axis=0, tiled=True)


def over_copies(array, axis):
    return from_everyone(array, axis).sum(axis=0)


def in_order(blocks, dim):
    blocks = jnp.moveaxis(blocks, 0, dim)
    lengths = blocks.shape
    return blocks.reshape(*lengths[:dim], lengths[dim] * lengths[dim + 1], *lengths[dim + 2 :])


def collect(array, axis, dim):
    return in_order(from_everyone(array, axis), dim)


def in_blocks(array, dim, peers):
    lengths = array.shape
    blocks = array.reshape(*lengths[:dim], peers, lengths[dim] // peers, *lengths[dim + 1 :])
    return jnp.moveaxis(blocks, dim, 0)


def sum_at_owner(array, axis, dim):
    blocks = in_blocks(array, dim, lax.axis_size(axis))
    arrived = lax.all_to_all(blocks, axis, split_axis=0, concat_axis=0, tiled=True)
    return arrived.sum(axis=0)


def side_by_side(arrays, axis, dim, along):
    both = jnp.concatenate(arrays, axis=along)
    filled, at, outs = (sum_at_owner(both, axis, dim), 0, [])
    for a in arrays:
        outs.append(lax.slice_in_dim(filled, at, at + a.shape[along], axis=along))
        at += a.shape[along]
    return tuple(outs)


def packed_total(arrays, axis):
    vector, at, outs = (jnp.concatenate([a.reshape(-1) for a in arrays]), 0, [])
    total = over_copies(vector, axis)
    for a in arrays:
        outs.append(total[at : at + a.size].reshape(a.shape))
        at += a.size
    return tuple(outs)


def rotate_share(vectors, positions, offset):
    share_width = vectors.shape[-1]
    index_list = (offset + jnp.arange(share_width, dtype=jnp.int32)).astype(jnp.float32)
    inverse = ROPE_BASE ** (-index_list / (DK // 2))
    angles = positions[:, None, :] * inverse[None, None, :]
    cosine = jnp.cos(angles)
    sine_part = jnp.sin(angles)
    front_part = vectors[:, :, 0, :]
    back_part = vectors[:, :, 1, :]
    return jnp.stack(
        [front_part * cosine - back_part * sine_part, front_part * sine_part + back_part * cosine],
        axis=2,
    )


def channel_stat(own_squares):
    return over_copies(own_squares, "kv")


def input_stat(own_squares):
    return over_copies(own_squares, "kv")


def cache_partial(query_low, lengths, log_decay, key_cache, value_cache, heads_here):
    batch_rows = query_low.shape[0]
    span = key_cache.shape[1]
    slots = lax.axis_index("kv") * span + jnp.arange(span, dtype=jnp.int32)
    live = slots[None, :] < lengths[:, None]
    gaps = jnp.maximum((lengths[:, None] - slots[None, :]).astype(jnp.float32), 0.0)
    decays = jnp.exp(log_decay[None, None, :] * gaps[:, :, None])
    keys_here = key_cache.reshape(batch_rows, span, heads_here, DK)
    values_here = value_cache.reshape(batch_rows, span, heads_here, DK)
    scores = jnp.einsum("bphd,bhd->bph", keys_here, query_low, preferred_element_type=jnp.float32)
    mixing = jnp.where(live[:, :, None], scores * decays, 0.0).astype(jnp.bfloat16)
    return jnp.einsum("bph,bphd->bhd", mixing, values_here, preferred_element_type=jnp.float32)


def local(
    tokens,
    lengths,
    attn_gain,
    w_query,
    w_key,
    w_value,
    w_gate,
    log_decay,
    key_cache,
    value_cache,
    gn_gain,
    w_out,
    ffn_gain,
    w_ffn_gate,
    w_ffn_up,
    w_ffn_down,
):
    batch_rows = tokens.shape[0]
    heads_here = log_decay.shape[0]
    half_dim = DK // 2
    row_block = collect(tokens, "tp", 1)
    widened = row_block.astype(jnp.float32)
    own_squares = jnp.sum(widened * widened, axis=1)
    scaled = (widened * attn_gain).astype(jnp.bfloat16)
    part_query = jnp.dot(scaled, w_query, preferred_element_type=jnp.float32)
    part_key = jnp.dot(scaled, w_key, preferred_element_type=jnp.float32)
    part_value = jnp.dot(scaled, w_value, preferred_element_type=jnp.float32)
    part_gate = jnp.dot(scaled, w_gate, preferred_element_type=jnp.float32)
    positions = lengths.astype(jnp.float32)
    quad = (batch_rows, heads_here, 2, half_dim)
    total_squares = input_stat(own_squares)
    queries, new_keys, new_values, gates = side_by_side(
        (
            part_query.reshape(quad),
            part_key.reshape(quad),
            part_value.reshape(quad),
            part_gate.reshape(quad),
        ),
        "kv",
        3,
        0,
    )
    share_width = queries.shape[3]
    offset = lax.axis_index("kv") * share_width
    factor = lax.rsqrt(total_squares / D + RMS_EPS)[:, None, None, None]
    queries = rotate_share(queries * factor, positions[:, None], offset) * DK ** (-0.5)
    new_keys = rotate_share(new_keys * factor, positions[:, None], offset)
    new_values = new_values * factor
    gates = gates * factor
    query_low = queries.astype(jnp.bfloat16)
    query_full = collect(query_low, "kv", 3).reshape(batch_rows, heads_here, DK)
    partial_value = cache_partial(
        query_full, lengths, log_decay, key_cache, value_cache, heads_here
    )
    own_dot = over_copies(jnp.sum(queries * new_keys, axis=(2, 3)), "kv")
    cached = sum_at_owner(partial_value.reshape(quad), "kv", 3)
    totals = cached + own_dot[:, :, None, None] * new_values
    sum_one, sum_two = packed_total(
        (jnp.sum(totals, axis=(2, 3)), jnp.sum(totals * totals, axis=(2, 3))), "kv"
    )
    center = (sum_one / DK)[:, :, None, None]
    spread = (sum_two / DK)[:, :, None, None] - center * center
    gain_share = lax.dynamic_slice_in_dim(
        gn_gain.reshape(heads_here, 2, half_dim), offset, share_width, 2
    )
    normed = (totals - center) * lax.rsqrt(spread + GN_EPS) * gain_share[None]
    gated_share = (jax.nn.silu(gates) * normed).astype(jnp.bfloat16)
    gated = collect(gated_share, "kv", 3).reshape(batch_rows, heads_here * DK)
    out_partial = jnp.dot(gated, w_out, preferred_element_type=jnp.float32)
    mixed = sum_at_owner(out_partial, "tp", 1)
    resid = (tokens.astype(jnp.float32) + mixed).astype(jnp.bfloat16)
    resid_block = collect(resid, "tp", 1).astype(jnp.float32)
    mid_squares = jnp.sum(resid_block * resid_block, axis=1)
    scaled_mid = (resid_block * ffn_gain).astype(jnp.bfloat16)
    gate_part = jnp.dot(scaled_mid, w_ffn_gate, preferred_element_type=jnp.float32)
    up_part = jnp.dot(scaled_mid, w_ffn_up, preferred_element_type=jnp.float32)
    total_mid = channel_stat(mid_squares)
    factor_mid = lax.rsqrt(total_mid / D + RMS_EPS)[:, None]
    gate_share, up_share = side_by_side((gate_part, up_part), "kv", 1, 0)
    hidden_share = (jax.nn.silu(gate_share * factor_mid) * (up_share * factor_mid)).astype(
        jnp.bfloat16
    )
    hidden = collect(hidden_share, "kv", 1)
    down_partial = jnp.dot(hidden, w_ffn_down, preferred_element_type=jnp.float32)
    down = sum_at_owner(down_partial, "tp", 1)
    return (resid.astype(jnp.float32) + down).astype(jnp.bfloat16)


def solution(mesh):
    return jax.shard_map(
        local,
        mesh=mesh,
        in_specs=(
            P("grp", ("kv", "tp")),
            P("grp"),
            P("kv"),
            P("kv", "tp"),
            P("kv", "tp"),
            P("kv", "tp"),
            P("kv", "tp"),
            P("tp"),
            P("grp", "kv", "tp"),
            P("grp", "kv", "tp"),
            P("tp"),
            P("tp", "kv"),
            P("kv"),
            P("kv", "tp"),
            P("kv", "tp"),
            P("tp", "kv"),
        ),
        out_specs=P("grp", ("kv", "tp")),
        check_vma=False,
    )
```

profile of v0, /device:TPU:33, one launch (start us, length us, event | category | flops | bytes accessed | tf_op | source)
XLA Modules:
  0.0 403.2 jit_solution(1669051512535924834)
XLA Ops:
  0.0 0.7 broadcast_bitcast_fusion.3
  0.8 0.7 reshape.272
  1.5 44.7 %all-to-all-start = ((bf16[8,2,192]{2,1,0:T(2,128)(2,1)}), bf16[8,2,192]{2,1,0:T(2,128)(2,1)S(1)}, u32[]{:S(2)}, u32[]{:S(2)}) async-start(bf16[8,2,192]{2,1,0:T(2,128)(2,1)} %reshape.272), calls=%async_computation | async-start | bytes 16384 | tf_op jit(solution)/shard_map/all_to_all | solution.py:17
  46.1 0.7 mul.241
  46.9 1.0 copy.119
  47.9 1.0 copy.120
  48.9 1.0 copy.121
  50.1 0.7 all-to-all-done
  51.2 0.2 fusion.21
  51.4 0.2 fusion.22
  51.6 0.2 fusion.23
  51.8 0.6 broadcast_in_dim.31
  52.4 6.7 %all-to-all-start.2 = ((f32[32,1,24]{2,1,0:T(1,128)}), f32[32,1,24]{2,1,0:T(1,128)S(1)}, u32[]{:S(2)}, u32[]{:S(2)}) async-start(f32[32,1,24]{2,1,0:T(1,128)} %broadcast_in_dim.31), calls=%async_computation.2 | async-start | bytes 32768 | tf_op jit(solution)/shard_map/all_to_all | solution.py:17
  59.3 0.7 copy.83
  60.0 19.7 %all-to-all-done.2 = f32[32,1,24]{2,1,0:T(1,128)S(1)} async-done(((f32[32,1,24]{2,1,0:T(1,128)}), f32[32,1,24]{2,1,0:T(1,128)S(1)}, u32[]{:S(2)}, u32[]{:S(2)}) %all-to-all-start.2) | async-done | bytes 3104 | tf_op jit(solution)/shard_map/all_to_all | solution.py:17
  79.7 4.8 %all-to-all-start.1 = ((f32[32,96,2,2,4]{1,4,3,2,0:T(4,128)}), f32[32,96,2,2,4]{1,4,3,2,0:T(4,128)S(1)}, u32[]{:S(2)}, u32[]{:S(2)}) async-start(f32[32,96,2,2,4]{1,4,3,2,0:T(4,128)} %copy.83), calls=%async_computation.1 | async-start | bytes 524288 | tf_op jit(solution)/shard_map/all_to_all | solution.py:42
  84.6 0.2 reshape.256
  84.8 0.9 copy-done.2
  86.1 36.4 %all-to-all-done.1 = f32[32,96,2,2,4]{1,4,3,2,0:T(4,128)S(1)} async-done(((f32[32,96,2,2,4]{1,4,3,2,0:T(4,128)}), f32[32,96,2,2,4]{1,4,3,2,0:T(4,128)S(1)}, u32[]{:S(2)}, u32[]{:S(2)}) %all-to-all-start.1) | async-done | bytes 196640 | tf_op jit(solution)/shard_map/all_to_all | solution.py:42
  122.8 0.8 reshape.274
  123.5 6.0 %all-to-all-start.3 = ((bf16[32,2,192]{2,1,0:T(2,128)(2,1)}), bf16[32,2,192]{2,1,0:T(2,128)(2,1)S(1)}, u32[]{:S(2)}, u32[]{:S(2)}) async-start(bf16[32,2,192]{2,1,0:T(2,128)(2,1)} %reshape.274), calls=%async_computation.3 | async-start | bytes 65536 | tf_op jit(solution)/shard_map/all_to_all | solution.py:17
  129.6 21.2 %all-to-all-done.3 = bf16[32,2,192]{2,1,0:T(2,128)(2,1)S(1)} async-done(((bf16[32,2,192]{2,1,0:T(2,128)(2,1)}), bf16[32,2,192]{2,1,0:T(2,128)(2,1)S(1)}, u32[]{:S(2)}, u32[]{:S(2)}) %all-to-all-start.3) | async-done | bytes 24608 | tf_op jit(solution)/shard_map/all_to_all | solution.py:17
  150.9 0.6 broadcast_in_dim.61
  151.5 4.8 %all-to-all-start.5 = ((f32[32,24,2]{1,2,0:T(2,128)}), f32[32,24,2]{1,2,0:T(2,128)S(1)}, u32[]{:S(2)}, u32[]{:S(2)}) async-start(f32[32,24,2]{1,2,0:T(2,128)} %broadcast_in_dim.61), calls=%async_computation.5 | async-start | bytes 65536 | tf_op jit(solution)/shard_map/all_to_all | solution.py:17
  156.6 0.9 multiply_reduce_fusion.1
  157.5 0.3 fusion.3
  157.8 1.0 multiply_reduce_fusion
  159.0 0.9 reshape.276
  160.0 17.5 %all-to-all-done.5 = f32[32,24,2]{1,2,0:T(2,128)S(1)} async-done(((f32[32,24,2]{1,2,0:T(2,128)}), f32[32,24,2]{1,2,0:T(2,128)S(1)}, u32[]{:S(2)}, u32[]{:S(2)}) %all-to-all-start.5) | async-done | bytes 6176 | tf_op jit(solution)/shard_map/all_to_all | solution.py:17
  177.4 4.8 %all-to-all-start.4 = ((f32[32,1,384]{2,1,0:T(1,128)}), f32[32,1,384]{2,1,0:T(1,128)S(1)}, u32[]{:S(2)}, u32[]{:S(2)}) async-start(f32[32,1,384]{2,1,0:T(1,128)} %reshape.276), calls=%async_computation.4 | async-start | bytes 98304 | tf_op jit(solution)/shard_map/all_to_all | solution.py:42
  182.2 21.8 %all-to-all-done.4 = f32[32,1,384]{2,1,0:T(1,128)S(1)} async-done(((f32[32,1,384]{2,1,0:T(1,128)}), f32[32,1,384]{2,1,0:T(1,128)S(1)}, u32[]{:S(2)}, u32[]{:S(2)}) %all-to-all-start.4) | async-done | bytes 49184 | tf_op jit(solution)/shard_map/all_to_all | solution.py:42
  204.1 0.5 broadcast.192
  204.6 0.8 reduce.11
  205.3 0.4 reshape.277
  206.3 0.6 broadcast_in_dim.62
  206.9 4.8 %all-to-all-start.6 = ((f32[32,1,96]{2,1,0:T(1,128)}), f32[32,1,96]{2,1,0:T(1,128)S(1)}, u32[]{:S(2)}, u32[]{:S(2)}) async-start(f32[32,1,96]{2,1,0:T(1,128)} %broadcast_in_dim.62), calls=%async_computation.6 | async-start | bytes 32768 | tf_op jit(solution)/shard_map/all_to_all | solution.py:17
  211.8 20.3 %all-to-all-done.6 = f32[32,1,96]{2,1,0:T(1,128)S(1)} async-done(((f32[32,1,96]{2,1,0:T(1,128)}), f32[32,1,96]{2,1,0:T(1,128)S(1)}, u32[]{:S(2)}, u32[]{:S(2)}) %all-to-all-start.6) | async-done | bytes 12320 | tf_op jit(solution)/shard_map/all_to_all | solution.py:17
  232.7 0.8 reshape.278
  233.5 4.9 %all-to-all-start.7 = ((bf16[32,2,192]{2,1,0:T(2,128)(2,1)}), bf16[32,2,192]{2,1,0:T(2,128)(2,1)S(1)}, u32[]{:S(2)}, u32[]{:S(2)}) async-start(bf16[32,2,192]{2,1,0:T(2,128)(2,1)} %reshape.278), calls=%async_computation.7 | async-start | bytes 65536 | tf_op jit(solution)/shard_map/all_to_all | solution.py:17
  238.6 20.9 %all-to-all-done.7 = bf16[32,2,192]{2,1,0:T(2,128)(2,1)S(1)} async-done(((bf16[32,2,192]{2,1,0:T(2,128)(2,1)}), bf16[32,2,192]{2,1,0:T(2,128)(2,1)S(1)}, u32[]{:S(2)}, u32[]{:S(2)}) %all-to-all-start.7) | async-done | bytes 24608 | tf_op jit(solution)/shard_map/all_to_all | solution.py:17
  260.0 17.5 %all_to_all.73 = f32[8,1,384]{2,1,0:T(1,128)S(1)} all-to-all(f32[8,1,384]{2,1,0:T(1,128)S(1)} %reshape.280), channel_id=1, replica_groups=mesh['grp'=2,'kv'=32,'tp'=8] {'tp'}, dimensions={0} | all-to-all | bytes 24576 | tf_op jit(solution)/shard_map/all_to_all | solution.py:42
  277.5 0.7 reduce.12
  278.5 7.8 %all_to_all.74 = bf16[8,2,192]{2,1,0:T(2,128)(2,1)S(1)} all-to-all(bf16[8,2,192]{2,1,0:T(2,128)(2,1)S(1)} %reshape.282), channel_id=1, replica_groups=mesh['grp'=2,'kv'=32,'tp'=8] {'tp'}, dimensions={0} | all-to-all | bytes 12288 | tf_op jit(solution)/shard_map/all_to_all | solution.py:17
  286.4 0.2 fusion.14
  286.8 0.6 broadcast_in_dim.65
  287.4 4.7 %all-to-all-start.11 = ((f32[32,1,24]{2,1,0:T(1,128)}), f32[32,1,24]{2,1,0:T(1,128)S(1)}, u32[]{:S(2)}, u32[]{:S(2)}) async-start(f32[32,1,24]{2,1,0:T(1,128)} %broadcast_in_dim.65), calls=%async_computation.11 | async-start | bytes 32768 | tf_op jit(solution)/shard_map/all_to_all | solution.py:17
  292.1 1.1 reshape.261
  293.2 0.5 copy.96
  293.7 1.5 reshape.284
  295.1 17.4 %all-to-all-done.11 = f32[32,1,24]{2,1,0:T(1,128)S(1)} async-done(((f32[32,1,24]{2,1,0:T(1,128)}), f32[32,1,24]{2,1,0:T(1,128)S(1)}, u32[]{:S(2)}, u32[]{:S(2)}) %all-to-all-start.11) | async-done | bytes 3104 | tf_op jit(solution)/shard_map/all_to_all | solution.py:17
  312.5 4.8 %all-to-all-start.10 = ((f32[32,1,2112]{2,1,0:T(1,128)}), f32[32,1,2112]{2,1,0:T(1,128)S(1)}, u32[]{:S(2)}, u32[]{:S(2)}) async-start(f32[32,1,2112]{2,1,0:T(1,128)} %reshape.284), calls=%async_computation.10 | async-start | bytes 557056 | tf_op jit(solution)/shard_map/all_to_all | solution.py:42
  317.4 39.4 %all-to-all-done.10 = f32[32,1,2112]{2,1,0:T(1,128)S(1)} async-done(((f32[32,1,2112]{2,1,0:T(1,128)}), f32[32,1,2112]{2,1,0:T(1,128)S(1)}, u32[]{:S(2)}, u32[]{:S(2)}) %all-to-all-start.10) | async-done | bytes 270368 | tf_op jit(solution)/shard_map/all_to_all | solution.py:42
  356.8 1.3 reduce.13
  358.1 0.5 reshape.285
  358.8 0.9 reshape.286
  359.8 6.0 %all-to-all-start.12 = ((bf16[32,2,528]{2,1,0:T(2,128)(2,1)}), bf16[32,2,528]{2,1,0:T(2,128)(2,1)S(1)}, u32[]{:S(2)}, u32[]{:S(2)}) async-start(bf16[32,2,528]{2,1,0:T(2,128)(2,1)} %reshape.286), calls=%async_computation.12 | async-start | bytes 163840 | tf_op jit(solution)/shard_map/all_to_all | solution.py:17
  365.8 0.2 copy.99
  366.0 23.3 %all-to-all-done.12 = bf16[32,2,528]{2,1,0:T(2,128)(2,1)S(1)} async-done(((bf16[32,2,528]{2,1,0:T(2,128)(2,1)}), bf16[32,2,528]{2,1,0:T(2,128)(2,1)S(1)}, u32[]{:S(2)}, u32[]{:S(2)}) %all-to-all-start.12) | async-done | bytes 67616 | tf_op jit(solution)/shard_map/all_to_all | solution.py:17
  389.3 0.3 reshape.287
  389.6 0.3 reshape.270
  389.9 0.2 fusion.18
  390.2 11.6 %all_to_all.75 = f32[8,1,384]{2,1,0:T(1,128)S(1)} all-to-all(f32[8,1,384]{2,1,0:T(1,128)S(1)} %reshape.288), channel_id=1, replica_groups=mesh['grp'=2,'kv'=32,'tp'=8] {'tp'}, dimensions={0} | all-to-all | bytes 24576 | tf_op jit(solution)/shard_map/all_to_all | solution.py:42
  401.8 0.7 reduce.14
  402.6 0.6 add_convert_fusion
  (93 shorter events, 4.9 us)
Async XLA Ops:
  0.0 286.4 %copy-start = (bf16[128,1408]{1,0:T(8,128)(2,1)S(1)}, bf16[128,1408]{1,0:T(8,128)(2,1)}, u32[]{:S(2)}) copy-start(bf16[128,1408]{1,0:T(8,128)(2,1)} %param.30) | copy-start | bytes 1081348
  0.0 50.0 %copy-start.5 = (bf16[128,512]{1,0:T(8,128)(2,1)S(1)}, bf16[128,512]{1,0:T(8,128)(2,1)}, u32[]{:S(2)}) copy-start(bf16[128,512]{1,0:T(8,128)(2,1)} %param.22) | copy-start | bytes 393220
  1.5 49.4 %all-to-all-start = ((bf16[8,2,192]{2,1,0:T(2,128)(2,1)}), bf16[8,2,192]{2,1,0:T(2,128)(2,1)S(1)}, u32[]{:S(2)}, u32[]{:S(2)}) async-start(bf16[8,2,192]{2,1,0:T(2,128)(2,1)} %reshape.272), calls=%async_computation | async-start | bytes 16384 | tf_op jit(solution)/shard_map/all_to_all | solution.py:17
  52.4 27.3 %all-to-all-start.2 = ((f32[32,1,24]{2,1,0:T(1,128)}), f32[32,1,24]{2,1,0:T(1,128)S(1)}, u32[]{:S(2)}, u32[]{:S(2)}) async-start(f32[32,1,24]{2,1,0:T(1,128)} %broadcast_in_dim.31), calls=%async_computation.2 | async-start | bytes 32768 | tf_op jit(solution)/shard_map/all_to_all | solution.py:17
  59.1 25.4 %copy-start.10 = (s32[24]{0:T(128)S(1)}, s32[24]{0:T(128)}, u32[]{:S(2)}) copy-start(s32[24]{0:T(128)} %param.17) | copy-start | bytes 292
  59.2 25.4 %copy-start.1 = (bf16[24,32,512]{2,1,0:T(8,128)(2,1)S(1)}, bf16[24,32,512]{2,1,0:T(8,128)(2,1)}, u32[]{:S(2)}) copy-start(bf16[24,32,512]{2,1,0:T(8,128)(2,1)} %param.24) | copy-start | bytes 2359300
  79.7 42.8 %all-to-all-start.1 = ((f32[32,96,2,2,4]{1,4,3,2,0:T(4,128)}), f32[32,96,2,2,4]{1,4,3,2,0:T(4,128)S(1)}, u32[]{:S(2)}, u32[]{:S(2)}) async-start(f32[32,96,2,2,4]{1,4,3,2,0:T(4,128)} %copy.83), calls=%async_computation.1 | async-start | bytes 524288 | tf_op jit(solution)/shard_map/all_to_all | solution.py:42
  84.5 1.1 copy-start.2
  123.5 27.3 %all-to-all-start.3 = ((bf16[32,2,192]{2,1,0:T(2,128)(2,1)}), bf16[32,2,192]{2,1,0:T(2,128)(2,1)S(1)}, u32[]{:S(2)}, u32[]{:S(2)}) async-start(bf16[32,2,192]{2,1,0:T(2,128)(2,1)} %reshape.274), calls=%async_computation.3 | async-start | bytes 65536 | tf_op jit(solution)/shard_map/all_to_all | solution.py:17
  151.5 25.9 %all-to-all-start.5 = ((f32[32,24,2]{1,2,0:T(2,128)}), f32[32,24,2]{1,2,0:T(2,128)S(1)}, u32[]{:S(2)}, u32[]{:S(2)}) async-start(f32[32,24,2]{1,2,0:T(2,128)} %broadcast_in_dim.61), calls=%async_computation.5 | async-start | bytes 65536 | tf_op jit(solution)/shard_map/all_to_all | solution.py:17
  156.5 1.1 copy-start.11
  159.0 52.8 %copy-start.9 = (f32[512]{0:T(512)S(1)}, f32[512]{0:T(512)}, u32[]{:S(2)}) copy-start(f32[512]{0:T(512)} %param.26) | copy-start | bytes 6148
  160.0 78.5 %copy-start.6 = (bf16[512,128]{1,0:T(8,128)(2,1)S(1)}, bf16[512,128]{1,0:T(8,128)(2,1)}, u32[]{:S(2)}) copy-start(bf16[512,128]{1,0:T(8,128)(2,1)} %param.27) | copy-start | bytes 393220
  177.4 26.6 %all-to-all-start.4 = ((f32[32,1,384]{2,1,0:T(1,128)}), f32[32,1,384]{2,1,0:T(1,128)S(1)}, u32[]{:S(2)}, u32[]{:S(2)}) async-start(f32[32,1,384]{2,1,0:T(1,128)} %reshape.276), calls=%async_computation.4 | async-start | bytes 98304 | tf_op jit(solution)/shard_map/all_to_all | solution.py:42
  206.9 25.2 %all-to-all-start.6 = ((f32[32,1,96]{2,1,0:T(1,128)}), f32[32,1,96]{2,1,0:T(1,128)S(1)}, u32[]{:S(2)}, u32[]{:S(2)}) async-start(f32[32,1,96]{2,1,0:T(1,128)} %broadcast_in_dim.62), calls=%async_computation.6 | async-start | bytes 32768 | tf_op jit(solution)/shard_map/all_to_all | solution.py:17
  233.5 25.9 %all-to-all-start.7 = ((bf16[32,2,192]{2,1,0:T(2,128)(2,1)}), bf16[32,2,192]{2,1,0:T(2,128)(2,1)S(1)}, u32[]{:S(2)}, u32[]{:S(2)}) async-start(bf16[32,2,192]{2,1,0:T(2,128)(2,1)} %reshape.278), calls=%async_computation.7 | async-start | bytes 65536 | tf_op jit(solution)/shard_map/all_to_all | solution.py:17
  238.6 39.7 %copy-start.7 = (bf16[24,16]{0,1:T(8,128)(2,1)S(1)}, bf16[24,16]{0,1:T(8,128)(2,1)}, u32[]{:S(2)}) copy-start(bf16[24,16]{0,1:T(8,128)(2,1)} %param.16) | copy-start | bytes 2308
  259.6 26.8 %copy-start.8 = (f32[128]{0:T(128)S(1)}, f32[128]{0:T(128)}, u32[]{:S(2)}) copy-start(f32[128]{0:T(128)} %param.28) | copy-start | bytes 1540
  259.7 26.9 %copy-start.3 = (bf16[128,1408]{1,0:T(8,128)(2,1)S(1)}, bf16[128,1408]{1,0:T(8,128)(2,1)}, u32[]{:S(2)}) copy-start(bf16[128,1408]{1,0:T(8,128)(2,1)} %param.29) | copy-start | bytes 1081348
  287.4 25.1 %all-to-all-start.11 = ((f32[32,1,24]{2,1,0:T(1,128)}), f32[32,1,24]{2,1,0:T(1,128)S(1)}, u32[]{:S(2)}, u32[]{:S(2)}) async-start(f32[32,1,24]{2,1,0:T(1,128)} %broadcast_in_dim.65), calls=%async_computation.11 | async-start | bytes 32768 | tf_op jit(solution)/shard_map/all_to_all | solution.py:17
  312.5 44.3 %all-to-all-start.10 = ((f32[32,1,2112]{2,1,0:T(1,128)}), f32[32,1,2112]{2,1,0:T(1,128)S(1)}, u32[]{:S(2)}, u32[]{:S(2)}) async-start(f32[32,1,2112]{2,1,0:T(1,128)} %reshape.284), calls=%async_computation.10 | async-start | bytes 557056 | tf_op jit(solution)/shard_map/all_to_all | solution.py:42
  358.6 7.2 %copy-start.4 = (bf16[1408,128]{1,0:T(8,128)(2,1)S(1)}, bf16[1408,128]{1,0:T(8,128)(2,1)}, u32[]{:S(2)}) copy-start(bf16[1408,128]{1,0:T(8,128)(2,1)} %param.31) | copy-start | bytes 1081348
  359.8 29.5 %all-to-all-start.12 = ((bf16[32,2,528]{2,1,0:T(2,128)(2,1)}), bf16[32,2,528]{2,1,0:T(2,128)(2,1)S(1)}, u32[]{:S(2)}, u32[]{:S(2)}) async-start(bf16[32,2,528]{2,1,0:T(2,128)(2,1)} %reshape.286), calls=%async_computation.12 | async-start | bytes 163840 | tf_op jit(solution)/shard_map/all_to_all | solution.py:17
where the time goes:
time: 404 us; the launch traced here: 403 us
  waiting for transfers between devices  238 us (59%)
  starting transfers between devices  97 us (24%)
  blocking collectives  36.8 us (9%)
  local copies, waits for them, and re-layouts  21.1 us (5%)
  other arithmetic  7.62 us (2%)
    all_to_all x8, waiting for transfers between devices, from_everyone(): return lax.all_to_all(copies, axis, split_axis=0, concat_axis=0, tiled=True)  141 us
    all_to_all x3, waiting for transfers between devices, sum_at_owner(): lax.all_to_all(blocks, axis, split_axis=0, concat_axis=0, tiled=True)  97.6 us
    all_to_all x8, starting transfers between devices, from_everyone(): return lax.all_to_all(copies, axis, split_axis=0, concat_axis=0, tiled=True)  82.6 us
    all_to_all x2, blocking collectives, sum_at_owner(): lax.all_to_all(blocks, axis, split_axis=0, concat_axis=0, tiled=True)  29.1 us
    all_to_all x3, starting transfers between devices, sum_at_owner(): lax.all_to_all(blocks, axis, split_axis=0, concat_axis=0, tiled=True)  14.3 us
    unnamed x49, local copies, waits for them, and re-layouts  9.94 us
  transfers between devices with their start and end apart: 11, of which 11 were waited for; matrix products, arithmetic and copies ran while one was open for 3% of the time, Pallas kernels for 0%

commit v1 on v0

v1 whole, which is shorter than its diff:
```python
import jax
import jax.numpy as jnp
from jax import lax
from jax.sharding import PartitionSpec as P

DK = 256
D = 4096
LANES = 128
NEAR = 4

RMS_EPS = 0.1
GN_EPS = 1.0
ROPE_BASE = 10000.0


def groups_near():
    n = lax.axis_size("kv")
    return [list(range(i, i + NEAR)) for i in range(0, n, NEAR)]


def groups_far():
    n = lax.axis_size("kv")
    return [list(range(i, n, NEAR)) for i in range(NEAR)]


def exchange(blocks, axis, groups=None):
    return lax.all_to_all(
        blocks, axis, split_axis=0, concat_axis=0, tiled=True, axis_index_groups=groups
    )


def spread(array, axis, peers, groups=None):
    return exchange(jnp.broadcast_to(array, (peers, *array.shape)), axis, groups)


def wide_sum(blocks):
    return jnp.sum(blocks.astype(jnp.float32), axis=0)


def hi_lo_rows(vector):
    high = lax.reduce_precision(vector, 8, 7)
    rows = jnp.stack([high, vector - high])
    return jnp.pad(rows, ((0, 6), (0, LANES - vector.shape[0])))


def near_blocks(array):
    return jnp.stack(
        [array[:, i * LANES : (i + 1) * LANES] for i in range(array.shape[1] // LANES)]
    )


def side(blocks):
    return jnp.concatenate([blocks[i] for i in range(blocks.shape[0])], axis=1)


def reduce_pair(first, second, extra=None):
    far = lax.axis_size("kv") // NEAR
    rows = first.shape[0]
    blocks = jnp.concatenate([near_blocks(first), near_blocks(second)], axis=1)
    if extra is not None:
        tail = jnp.broadcast_to(hi_lo_rows(extra), (NEAR, 8, LANES))
        blocks = jnp.concatenate([blocks, tail], axis=1)
    got = wide_sum(exchange(blocks.astype(jnp.bfloat16), "kv", groups_near()))
    if extra is not None:
        vector = got[2 * rows] + got[2 * rows + 1]
        got = jnp.concatenate([got[: 2 * rows], hi_lo_rows(vector[: extra.shape[0]])], axis=0)
    got = wide_sum(spread(got.astype(jnp.bfloat16), "kv", far, groups_far()))
    whole = spread(got[: 2 * rows].astype(jnp.bfloat16), "kv", NEAR, groups_near())
    outs = (
        side(whole[:, :rows]).astype(jnp.float32),
        side(whole[:, rows:]).astype(jnp.float32),
    )
    if extra is None:
        return outs
    return (*outs, (got[2 * rows] + got[2 * rows + 1])[: extra.shape[0]])


def rotate(vectors, cosine, sine):
    half = DK // 2
    outs = []
    for h in range(vectors.shape[1] // DK):
        a = vectors[:, h * DK : h * DK + half]
        b = vectors[:, h * DK + half : (h + 1) * DK]
        outs += [a * cosine - b * sine, a * sine + b * cosine]
    return jnp.concatenate(outs, axis=1)


def cache_partial(query_low, lengths, log_decay, key_cache, value_cache, heads_here):
    batch_rows = query_low.shape[0]
    span = key_cache.shape[1]
    slots = lax.axis_index("kv") * span + jnp.arange(span, dtype=jnp.int32)
    live = slots[None, :] < lengths[:, None]
    gaps = jnp.maximum((lengths[:, None] - slots[None, :]).astype(jnp.float32), 0.0)
    decays = jnp.exp(log_decay[None, None, :] * gaps[:, :, None])
    keys_here = key_cache.reshape(batch_rows, span, heads_here, DK)
    values_here = value_cache.reshape(batch_rows, span, heads_here, DK)
    scores = jnp.einsum("bphd,bhd->bph", keys_here, query_low, preferred_element_type=jnp.float32)
    mixing = jnp.where(live[:, :, None], scores * decays, 0.0).astype(jnp.bfloat16)
    return jnp.einsum("bph,bphd->bhd", mixing, values_here, preferred_element_type=jnp.float32)


def local(
    tokens,
    lengths,
    attn_gain,
    w_query,
    w_key,
    w_value,
    w_gate,
    log_decay,
    key_cache,
    value_cache,
    gn_gain,
    w_out,
    ffn_gain,
    w_ffn_gate,
    w_ffn_up,
    w_ffn_down,
):
    rows = tokens.shape[0]
    heads_here = log_decay.shape[0]
    kv = lax.axis_size("kv")
    tp = lax.axis_size("tp")
    own_width = tokens.shape[1]
    gathered = spread(tokens, "tp", tp)
    x = jnp.moveaxis(gathered, 0, 1).reshape(rows, tp * own_width).astype(jnp.float32)
    own_squares = jnp.sum(x * x, axis=1)
    scaled = (x * attn_gain).astype(jnp.bfloat16)
    dot = lambda a, w: jnp.dot(a, w, preferred_element_type=jnp.float32)
    q_raw, k_raw, squares = reduce_pair(dot(scaled, w_query), dot(scaled, w_key), own_squares)
    factor = lax.rsqrt(squares / D + RMS_EPS)[:, None]
    positions = lengths.astype(jnp.float32)
    half = DK // 2
    inverse = ROPE_BASE ** (-jnp.arange(half, dtype=jnp.float32) / half)
    angles = positions[:, None] * inverse[None, :]
    cosine, sine = jnp.cos(angles), jnp.sin(angles)
    queries = rotate(q_raw * factor, cosine, sine) * DK ** (-0.5)
    keys = rotate(k_raw * factor, cosine, sine)
    by_head = (rows, heads_here, DK)
    own_dot = jnp.sum((queries * keys).reshape(by_head), axis=-1, keepdims=True)
    cached = cache_partial(
        queries.astype(jnp.bfloat16).reshape(by_head),
        lengths,
        log_decay,
        key_cache,
        value_cache,
        heads_here,
    )
    part_value = dot(scaled, w_value) * factor
    totals = cached + own_dot * part_value.reshape(by_head)
    totals = totals - jnp.mean(totals, axis=-1, keepdims=True)
    part_gate = dot(scaled, w_gate) * factor
    totals, gates = reduce_pair(totals.reshape(rows, heads_here * DK), part_gate)
    totals = totals.reshape(by_head)
    center = jnp.mean(totals, axis=-1, keepdims=True)
    spread_ = jnp.mean(totals * totals, axis=-1, keepdims=True) - center * center
    normed = ((totals - center) * lax.rsqrt(spread_ + GN_EPS)).reshape(rows, heads_here * DK)
    gated = (jax.nn.silu(gates) * (normed * gn_gain)).astype(jnp.bfloat16)
    mixed = wide_sum(spread(dot(gated, w_out).astype(jnp.bfloat16), "tp", tp))
    resid = (x + mixed).astype(jnp.bfloat16)
    resid_wide = resid.astype(jnp.float32)
    mid_squares = jnp.sum(resid_wide * resid_wide, axis=1)
    scaled_mid = (resid_wide * ffn_gain).astype(jnp.bfloat16)
    gate_part = dot(scaled_mid, w_ffn_gate)
    up_part = dot(scaled_mid, w_ffn_up)
    wide = gate_part.shape[1]
    share = wide // kv

    def for_peers(a):
        return jnp.moveaxis(a.reshape(rows, kv, share), 1, 0).reshape(kv, rows * share)

    high = lax.reduce_precision(mid_squares, 8, 7)
    stat = jnp.broadcast_to(jnp.concatenate([high, mid_squares - high]), (kv, 2 * rows))
    flat = jnp.concatenate([for_peers(gate_part), for_peers(up_part), stat], axis=1)
    size = flat.shape[1]
    flat = jnp.pad(flat, ((0, 0), (0, -size % LANES))).astype(jnp.bfloat16)
    got = wide_sum(exchange(flat, "kv"))
    gate_share = got[: rows * share].reshape(rows, share)
    up_share = got[rows * share : 2 * rows * share].reshape(rows, share)
    total_mid = got[2 * rows * share : 2 * rows * share + rows]
    total_mid = total_mid + got[2 * rows * share + rows : size]
    factor_mid = lax.rsqrt(total_mid / D + RMS_EPS)[:, None]
    hidden_share = (jax.nn.silu(gate_share * factor_mid) * (up_share * factor_mid)).astype(
        jnp.bfloat16
    )
    hidden = jnp.moveaxis(spread(hidden_share, "kv", kv), 0, 1).reshape(rows, wide)
    down_part = dot(hidden, w_ffn_down).astype(jnp.bfloat16)
    down = wide_sum(
        exchange(jnp.moveaxis(down_part.reshape(rows, tp, own_width), 1, 0), "tp")
    )
    own_at = lax.axis_index("tp") * own_width
    own_resid = lax.dynamic_slice_in_dim(resid_wide, own_at, own_width, 1)
    return (own_resid + down).astype(jnp.bfloat16)


def solution(mesh):
    return jax.shard_map(
        local,
        mesh=mesh,
        in_specs=(
            P("grp", ("kv", "tp")),
            P("grp"),
            P("kv"),
            P("kv", "tp"),
            P("kv", "tp"),
            P("kv", "tp"),
            P("kv", "tp"),
            P("tp"),
            P("grp", "kv", "tp"),
            P("grp", "kv", "tp"),
            P("tp"),
            P("tp", "kv"),
            P("kv"),
            P("kv", "tp"),
            P("kv", "tp"),
            P("tp", "kv"),
        ),
        out_specs=P("grp", ("kv", "tp")),
        check_vma=False,
    )
```

time: 404 us -> 246 us (0.61)
  waiting for transfers between devices: 238 us -> 35.6 us
  blocking collectives: 36.8 us -> 161 us
  starting transfers between devices: 97 us -> 30 us
  local copies, waits for them, and re-layouts: 21.1 us -> 12.6 us
  other arithmetic: 7.62 us -> 2.63 us
    all_to_all x11 -> x4, waiting for transfers between devices: 238 us -> 35.6 us  [exchange(): lax.all_to_all(blocks, axis, split_axis=0, concat_axis=0, tiled=True, axi...]
    all_to_all x3 -> x7, blocking collectives: 36.8 us -> 161 us  [exchange(): lax.all_to_all(blocks, axis, split_axis=0, concat_axis=0, tiled=True, axi...]
    all_to_all x11 -> x4, starting transfers between devices: 97 us -> 30 us  [exchange(): lax.all_to_all(blocks, axis, split_axis=0, concat_axis=0, tiled=True, axi...]
    unnamed x49 -> x45, local copies, waits for them, and re-layouts: 9.94 us -> 6.14 us
  transfers between devices with their start and end apart: 11 -> 4, of which waited for: 11 -> 4; matrix products, arithmetic and copies ran while one was open for 3% -> 0% of each run, Pallas kernels for 0% -> 0%
where the time goes in v1:
time: 246 us; the launch traced here: 245 us
  blocking collectives  161 us (65%)
  waiting for transfers between devices  35.6 us (14%)
  starting transfers between devices  30 us (12%)
  local copies, waits for them, and re-layouts  12.6 us (5%)
  other arithmetic  2.63 us (1%)
    all_to_all x7, blocking collectives, exchange(): lax.all_to_all(blocks, axis, split_axis=0, concat_axis=0, tiled=True, axi...  161 us
    all_to_all x4, waiting for transfers between devices, exchange(): lax.all_to_all(blocks, axis, split_axis=0, concat_axis=0, tiled=True, axi...  35.6 us
    all_to_all x4, starting transfers between devices, exchange(): lax.all_to_all(blocks, axis, split_axis=0, concat_axis=0, tiled=True, axi...  30 us
    unnamed x45, local copies, waits for them, and re-layouts  6.14 us
  transfers between devices with their start and end apart: 4, of which 4 were waited for; matrix products, arithmetic and copies ran while one was open for 0% of the time, Pallas kernels for 0%

profile of v1, /device:TPU:33, one launch (start us, length us, event | category | flops | bytes accessed | tf_op | source)
XLA Modules:
  0.0 245.0 jit_solution(15991239335635144964)
XLA Ops:
  0.0 0.7 broadcast_bitcast_fusion
  0.7 0.1 reshape.211
  0.9 48.5 %all_to_all.59 = bf16[8,2,192]{2,1,0:T(2,128)(2,1)S(1)} all-to-all(bf16[8,2,192]{2,1,0:T(2,128)(2,1)S(1)} %reshape.211), channel_id=1, replica_groups=mesh['grp'=2,'kv'=32,'tp'=8] {'tp'}, dimensions={0} | all-to-all | bytes 12288 | tf_op jit(solution)/shard_map/all_to_all | solution.py:27
  49.3 0.1 reshape.212
  49.6 0.5 copy-done.9
  50.1 0.1 copy-done.4
  50.2 0.1 convolution_convert_fusion.2
  50.4 0.1 convolution_convert_fusion.3
  50.6 7.0 %all_to_all.60 = bf16[4,56,128]{2,1,0:T(8,128)(2,1)S(1)} all-to-all(bf16[4,56,128]{2,1,0:T(8,128)(2,1)S(1)} %pad_maximum_fusion), channel_id=1, replica_groups={{0,8,16,24},{32,40,48,56},{64,72,80,88},{96,104,112,120},{128,136,144,1..., dimensions={0} | all-to-all | bytes 114688 | tf_op jit(solution)/shard_map/all_to_all | solution.py:27
  57.7 0.7 broadcast_in_dim.33
  58.3 8.0 %all-to-all-start.2 = ((bf16[8,56,128]{2,1,0:T(8,128)(2,1)}), bf16[8,56,128]{2,1,0:T(8,128)(2,1)S(1)}, u32[]{:S(2)}, u32[]{:S(2)}) async-start(bf16[8,56,128]{2,1,0:T(8,128)(2,1)} %broadcast_in_dim.33), calls=%async_computation.2 | async-start | bytes 229376 | tf_op jit(solution)/shard_map/all_to_all | solution.py:27
  66.3 0.6 copy-done.8
  67.2 23.4 %all-to-all-done.2 = bf16[8,56,128]{2,1,0:T(8,128)(2,1)S(1)} async-done(((bf16[8,56,128]{2,1,0:T(8,128)(2,1)}), bf16[8,56,128]{2,1,0:T(8,128)(2,1)S(1)}, u32[]{:S(2)}, u32[]{:S(2)}) %all-to-all-start.2) | async-done | bytes 114720 | tf_op jit(solution)/shard_map/all_to_all | solution.py:27
  90.6 0.6 broadcast_in_dim.34
  91.3 4.8 %all-to-all-start.3 = ((bf16[4,48,128]{2,1,0:T(8,128)(2,1)}), bf16[4,48,128]{2,1,0:T(8,128)(2,1)S(1)}, u32[]{:S(2)}, u32[]{:S(2)}) async-start(bf16[4,48,128]{2,1,0:T(8,128)(2,1)} %broadcast_in_dim.34), calls=%async_computation.3 | async-start | bytes 98304 | tf_op jit(solution)/shard_map/all_to_all | solution.py:27
  96.2 0.1 fusion.5
  96.4 4.2 %all-to-all-done.3 = bf16[4,48,128]{2,1,0:T(8,128)(2,1)S(1)} async-done(((bf16[4,48,128]{2,1,0:T(8,128)(2,1)}), bf16[4,48,128]{2,1,0:T(8,128)(2,1)S(1)}, u32[]{:S(2)}, u32[]{:S(2)}) %all-to-all-start.3) | async-done | bytes 49184 | tf_op jit(solution)/shard_map/all_to_all | solution.py:27
  100.7 0.1 fusion.51
  101.0 0.3 fusion.9
  101.3 0.2 copy.96
  101.5 0.1 copy-done.11
  101.6 0.3 fusion.14
  101.9 0.3 copy.97
  102.2 0.2 copy-done.1
  102.4 0.2 fusion.6
  102.6 0.2 fusion.76
  103.0 7.0 %all_to_all.61 = bf16[4,48,128]{2,1,0:T(8,128)(2,1)S(1)} all-to-all(bf16[4,48,128]{2,1,0:T(8,128)(2,1)S(1)} %maximum_maximum_fusion), channel_id=1, replica_groups={{0,8,16,24},{32,40,48,56},{64,72,80,88},{96,104,112,120},{128,136,144,1..., dimensions={0} | all-to-all | bytes 98304 | tf_op jit(solution)/shard_map/all_to_all | solution.py:27
  110.0 28.3 %all_to_all.62 = bf16[8,48,128]{2,1,0:T(8,128)(2,1)S(1)} all-to-all(bf16[8,48,128]{2,1,0:T(8,128)(2,1)S(1)} %broadcast_in_dim.63), channel_id=1, replica_groups={{0,32,64,96,128,160,192,224},{8,40,72,104,136,168,200,232},{16,48,80,11..., dimensions={0} | all-to-all | bytes 196608 | tf_op jit(solution)/shard_map/all_to_all | solution.py:27
  138.4 8.5 %all_to_all.63 = bf16[4,48,128]{2,1,0:T(8,128)(2,1)S(1)} all-to-all(bf16[4,48,128]{2,1,0:T(8,128)(2,1)S(1)} %broadcast_in_dim.64), channel_id=1, replica_groups={{0,8,16,24},{32,40,48,56},{64,72,80,88},{96,104,112,120},{128,136,144,1..., dimensions={0} | all-to-all | bytes 98304 | tf_op jit(solution)/shard_map/all_to_all | solution.py:27
  146.9 0.1 fusion.73
  147.3 0.1 mul.260
  147.6 0.7 copy-done.13
  148.3 0.2 convolution_convert_fusion.4
  148.4 0.6 broadcast_in_dim.65
  149.1 9.9 %all-to-all-start.7 = ((bf16[8,24,128]{2,1,0:T(8,128)(2,1)}), bf16[8,24,128]{2,1,0:T(8,128)(2,1)S(1)}, u32[]{:S(2)}, u32[]{:S(2)}) async-start(bf16[8,24,128]{2,1,0:T(8,128)(2,1)} %broadcast_in_dim.65), calls=%async_computation.7 | async-start | bytes 98304 | tf_op jit(solution)/shard_map/all_to_all | solution.py:27
  159.1 0.2 copy.87
  159.4 0.9 copy-done.3
  160.3 0.2 copy.88
  160.6 3.2 %all-to-all-done.7 = bf16[8,24,128]{2,1,0:T(8,128)(2,1)S(1)} async-done(((bf16[8,24,128]{2,1,0:T(8,128)(2,1)}), bf16[8,24,128]{2,1,0:T(8,128)(2,1)S(1)}, u32[]{:S(2)}, u32[]{:S(2)}) %all-to-all-start.7) | async-done | bytes 49184 | tf_op jit(solution)/shard_map/all_to_all | solution.py:27
  163.9 0.1 copy.101
  164.0 0.5 fusion.1
  164.5 0.2 reshape.195
  164.7 0.5 fusion.2
  165.2 0.2 reshape.196
  165.5 0.1 concatenate.47
  165.6 0.5 broadcast.166
  166.1 0.7 reduce.5
  166.8 0.2 reshape.213
  167.0 34.1 %all_to_all.64 = bf16[32,2,1088]{2,1,0:T(2,128)(2,1)S(1)} all-to-all(bf16[32,2,1088]{2,1,0:T(2,128)(2,1)S(1)} %reshape.213), channel_id=1, replica_groups=mesh['grp'=2,'kv'=32,'tp'=8] {'kv'}, dimensions={0} | all-to-all | bytes 278528 | tf_op jit(solution)/shard_map/all_to_all | solution.py:27
  201.1 0.1 reshape.214
  201.3 0.3 convert_reduce_fusion
  201.7 0.1 reshape.198
  202.0 0.3 reshape.215
  202.3 28.0 %all_to_all.65 = bf16[32,2,528]{2,1,0:T(2,128)(2,1)S(1)} all-to-all(bf16[32,2,528]{2,1,0:T(2,128)(2,1)S(1)} %reshape.215), channel_id=1, replica_groups=mesh['grp'=2,'kv'=32,'tp'=8] {'kv'}, dimensions={0} | all-to-all | bytes 135168 | tf_op jit(solution)/shard_map/all_to_all | solution.py:27
  230.4 0.3 reshape.216
  230.7 0.3 reshape.199
  231.0 0.2 convolution_convert_fusion.5
  231.1 0.1 reshape.200
  231.2 0.1 copy.91
  231.3 0.7 reshape.217
  232.1 7.3 %all-to-all-start.10 = ((bf16[8,2,192]{2,1,0:T(2,128)(2,1)}), bf16[8,2,192]{2,1,0:T(2,128)(2,1)S(1)}, u32[]{:S(2)}, u32[]{:S(2)}) async-start(bf16[8,2,192]{2,1,0:T(2,128)(2,1)} %reshape.217), calls=%async_computation.10 | async-start | bytes 16384 | tf_op jit(solution)/shard_map/all_to_all | solution.py:27
  239.3 4.7 %all-to-all-done.10 = bf16[8,2,192]{2,1,0:T(2,128)(2,1)S(1)} async-done(((bf16[8,2,192]{2,1,0:T(2,128)(2,1)}), bf16[8,2,192]{2,1,0:T(2,128)(2,1)S(1)}, u32[]{:S(2)}, u32[]{:S(2)}) %all-to-all-start.10) | async-done | bytes 6176 | tf_op jit(solution)/shard_map/all_to_all | solution.py:27
  244.0 0.1 reshape.218
  244.3 0.7 copy.93
  (93 shorter events, 2.4 us)
Async XLA Ops:
  0.0 231.0 %copy-start = (bf16[1408,128]{1,0:T(8,128)(2,1)S(1)}, bf16[1408,128]{1,0:T(8,128)(2,1)}, u32[]{:S(2)}) copy-start(bf16[1408,128]{1,0:T(8,128)(2,1)} %param.31) | copy-start | bytes 1081348
  49.3 0.9 copy-start.4
  49.4 0.7 copy-start.9
  49.5 0.9 copy-start.5
  58.3 32.2 %all-to-all-start.2 = ((bf16[8,56,128]{2,1,0:T(8,128)(2,1)}), bf16[8,56,128]{2,1,0:T(8,128)(2,1)S(1)}, u32[]{:S(2)}, u32[]{:S(2)}) async-start(bf16[8,56,128]{2,1,0:T(8,128)(2,1)} %broadcast_in_dim.33), calls=%async_computation.2 | async-start | bytes 229376 | tf_op jit(solution)/shard_map/all_to_all | solution.py:27
  66.3 0.7 copy-start.8
  67.2 28.9 %copy-start.7 = (bf16[128,512]{1,0:T(8,128)(2,1)S(1)}, bf16[128,512]{1,0:T(8,128)(2,1)}, u32[]{:S(2)}) copy-start(bf16[128,512]{1,0:T(8,128)(2,1)} %param.21) | copy-start | bytes 393220
  91.3 4.9 %copy-start.6 = (bf16[128,512]{1,0:T(8,128)(2,1)S(1)}, bf16[128,512]{1,0:T(8,128)(2,1)}, u32[]{:S(2)}) copy-start(bf16[128,512]{1,0:T(8,128)(2,1)} %param.22) | copy-start | bytes 393220
  91.3 9.7 %copy-start.12 = (bf16[24,32,512]{2,1,0:T(8,128)(2,1)S(1)}, bf16[24,32,512]{2,1,0:T(8,128)(2,1)}, u32[]{:S(2)}) copy-start(bf16[24,32,512]{2,1,0:T(8,128)(2,1)} %param.24) | copy-start | bytes 2359300
  91.3 9.4 %all-to-all-start.3 = ((bf16[4,48,128]{2,1,0:T(8,128)(2,1)}), bf16[4,48,128]{2,1,0:T(8,128)(2,1)S(1)}, u32[]{:S(2)}, u32[]{:S(2)}) async-start(bf16[4,48,128]{2,1,0:T(8,128)(2,1)} %broadcast_in_dim.34), calls=%async_computation.3 | async-start | bytes 98304 | tf_op jit(solution)/shard_map/all_to_all | solution.py:27
  101.0 0.7 copy-start.11
  101.3 1.2 copy-start.1
  147.4 0.9 copy-start.13
  147.4 0.9 copy-start.14
  147.6 11.5 %copy-start.2 = (bf16[128,1408]{1,0:T(8,128)(2,1)S(1)}, bf16[128,1408]{1,0:T(8,128)(2,1)}, u32[]{:S(2)}) copy-start(bf16[128,1408]{1,0:T(8,128)(2,1)} %param.29) | copy-start | bytes 1081348
  149.1 9.9 %copy-start.10 = (f32[128]{0:T(128)S(1)}, f32[128]{0:T(128)}, u32[]{:S(2)}) copy-start(f32[128]{0:T(128)} %param.28) | copy-start | bytes 1540
  149.1 14.8 %all-to-all-start.7 = ((bf16[8,24,128]{2,1,0:T(8,128)(2,1)}), bf16[8,24,128]{2,1,0:T(8,128)(2,1)S(1)}, u32[]{:S(2)}, u32[]{:S(2)}) async-start(bf16[8,24,128]{2,1,0:T(8,128)(2,1)} %broadcast_in_dim.65), calls=%async_computation.7 | async-start | bytes 98304 | tf_op jit(solution)/shard_map/all_to_all | solution.py:27
  159.3 1.0 copy-start.3
  232.1 12.0 %all-to-all-start.10 = ((bf16[8,2,192]{2,1,0:T(2,128)(2,1)}), bf16[8,2,192]{2,1,0:T(2,128)(2,1)S(1)}, u32[]{:S(2)}, u32[]{:S(2)}) async-start(bf16[8,2,192]{2,1,0:T(2,128)(2,1)} %reshape.217), calls=%async_computation.10 | async-start | bytes 16384 | tf_op jit(solution)/shard_map/all_to_all | solution.py:27

commit v2 on v1

v2 whole, which is shorter than its diff:
```python
import jax
import jax.numpy as jnp
from jax import lax
from jax.experimental import pallas as pl
from jax.experimental.pallas import tpu as pltpu
from jax.sharding import PartitionSpec as P

DK = 256
D = 4096
LANES = 128
NEAR = 4
F32 = jnp.float32
BF16 = jnp.bfloat16

RMS_EPS = 0.1
GN_EPS = 1.0
ROPE_BASE = 10000.0


def groups_near():
    n = lax.axis_size("kv")
    return [list(range(i, i + NEAR)) for i in range(0, n, NEAR)]


def groups_far():
    n = lax.axis_size("kv")
    return [list(range(i, n, NEAR)) for i in range(NEAR)]


def exchange(blocks, axis, groups=None):
    return lax.all_to_all(
        blocks, axis, split_axis=0, concat_axis=0, tiled=True, axis_index_groups=groups
    )


def spread(array, axis, peers, groups=None):
    return exchange(jnp.broadcast_to(array, (peers, *array.shape)), axis, groups)


def wide_sum(blocks):
    return jnp.sum(blocks.astype(F32), axis=0)


def side(blocks):
    return jnp.concatenate([blocks[i] for i in range(blocks.shape[0])], axis=1)


def kernel(body, outs, *args, scratch=(), scalars=0):
    vmem = pl.BlockSpec(memory_space=pltpu.VMEM)
    smem = pl.BlockSpec(memory_space=pltpu.SMEM)
    return pl.pallas_call(
        body,
        out_shape=outs,
        in_specs=[smem] * scalars + [vmem] * (len(args) - scalars),
        out_specs=jax.tree.map(lambda _: vmem, outs),
        scratch_shapes=list(scratch),
    )(*args)


def iota(shape, dim):
    return lax.broadcasted_iota(jnp.int32, shape, dim)


def mm(a, b):
    return jnp.dot(a, b, preferred_element_type=F32)


def column_to_row(column):
    shape = (column.shape[0], LANES)
    return jnp.sum(
        jnp.where(iota(shape, 0) == iota(shape, 1), column, 0.0), axis=0, keepdims=True
    )


def place_body(at, tokens, out):
    peers, rows, _ = out.shape
    width = tokens.shape[1]
    shape = (width, LANES)
    pick = jnp.where(iota(shape, 1) == iota(shape, 0) + at[0] * width, 1.0, 0.0).astype(BF16)
    placed = mm(tokens[...], pick).astype(BF16)
    for i in range(peers):
        out[i] = placed


def project_body(parts, gain, w_query, w_key, w_value, w_gate, blocks, value, gate, x_out):
    peers, rows, _ = parts.shape
    x = parts[0].astype(F32)
    for i in range(1, peers):
        x = x + parts[i].astype(F32)
    x_out[...] = x
    squares = column_to_row(jnp.sum(x * x, axis=1, keepdims=True))
    high = squares.astype(BF16).astype(F32)
    at = iota((8, LANES), 0)
    tail = jnp.where(at == 0, high, jnp.where(at == 1, squares - high, 0.0)).astype(BF16)
    scaled = (x * gain[...]).astype(BF16)
    query = mm(scaled, w_query[...])
    key = mm(scaled, w_key[...])
    for n in range(NEAR):
        lanes = slice(n * LANES, (n + 1) * LANES)
        blocks[n, 0:rows, :] = query[:, lanes].astype(BF16)
        blocks[n, rows : 2 * rows, :] = key[:, lanes].astype(BF16)
        blocks[n, 2 * rows : 2 * rows + 8, :] = tail
    value[...] = mm(scaled, w_value[...])
    gate[...] = mm(scaled, w_gate[...])


def mix_body(blocks, gain, w_out, out):
    peers, rows, _ = out.shape
    mixed = jnp.zeros((rows, LANES), F32)
    for h in range(NEAR // 2):
        a, b = (blocks[n, 0:rows, :].astype(F32) for n in (2 * h, 2 * h + 1))
        center = (
            jnp.sum(a, axis=1, keepdims=True) + jnp.sum(b, axis=1, keepdims=True)
        ) / DK
        a, b = a - center, b - center
        spread_ = (
            jnp.sum(a * a, axis=1, keepdims=True) + jnp.sum(b * b, axis=1, keepdims=True)
        ) / DK
        scale = lax.rsqrt(spread_ + GN_EPS)
        for n, half in ((2 * h, a), (2 * h + 1, b)):
            lanes = slice(n * LANES, (n + 1) * LANES)
            gates = blocks[n, rows : 2 * rows, :].astype(F32)
            silu = gates / (1.0 + jnp.exp(-gates))
            gated = (silu * (half * scale * gain[:, lanes])).astype(BF16)
            mixed = mixed + mm(gated, w_out[lanes, :])
    mixed = mixed.astype(BF16)
    for i in range(peers):
        out[i] = mixed


def ffn_in_body(x, parts, gain, w_gate, w_up, blocks, resid_out, gate_s, up_s, pack_s):
    peers, rows, _ = parts.shape
    wide = w_gate.shape[1]
    cuts = wide // LANES
    own = rows // NEAR
    mixed = parts[0].astype(F32)
    for i in range(1, peers):
        mixed = mixed + parts[i].astype(F32)
    resid = (x[...] + mixed).astype(BF16)
    resid_out[...] = resid
    resid = resid.astype(F32)
    squares = jnp.sum(resid * resid, axis=1, keepdims=True)
    scaled = (resid * gain[...]).astype(BF16)
    gate_s[...] = mm(scaled, w_gate[...])
    up_s[...] = mm(scaled, w_up[...])
    stat = 2 * cuts * own
    at = iota((rows, LANES), 0)
    lane = iota((rows, LANES), 1)
    for n in range(NEAR):
        for c in range(cuts):
            lanes = slice(c * LANES, (c + 1) * LANES)
            pack_s[n, c * own : (c + 1) * own, :] = gate_s[n * own : (n + 1) * own, lanes]
            pack_s[n, (cuts + c) * own : (cuts + c + 1) * own, :] = up_s[
                n * own : (n + 1) * own, lanes
            ]
        row = jnp.sum(jnp.where(at == lane + n * own, squares, 0.0), axis=0, keepdims=True)
        keep = iota((1, LANES), 1) < own
        row = jnp.where(keep, row, 0.0)
        pack_s[n, stat : pack_s.shape[1], :] = jnp.broadcast_to(
            row, (pack_s.shape[1] - stat, LANES)
        )
    blocks[...] = pack_s[...].astype(BF16)


def hidden_body(arrived, out, sum_s, *, own, cuts):
    total = arrived[0].astype(F32)
    for i in range(1, arrived.shape[0]):
        total = total + arrived[i].astype(F32)
    sum_s[...] = total
    half = own * cuts
    padded = out.shape[1]
    row = sum_s[2 * half : 2 * half + 1, :]
    shape = (padded, LANES)
    row_at = lax.rem(iota(shape, 0), own)
    squares = jnp.sum(jnp.where(row_at == iota(shape, 1), row, 0.0), axis=1, keepdims=True)
    factor = lax.rsqrt(squares / D + RMS_EPS)[0:half]
    gate = sum_s[0:half, :] * factor
    up = sum_s[half : 2 * half, :] * factor
    hidden = gate / (1.0 + jnp.exp(-gate)) * up
    for i in range(out.shape[0]):
        out[i, 0:half, :] = hidden.astype(BF16)
        if padded > half:
            out[i, half:padded, :] = jnp.zeros((padded - half, LANES), BF16)


def down_body(arrived, w_down, out, wide_s, row_s):
    peers, rows, _ = out.shape
    own = rows // NEAR
    cuts = w_down.shape[0] // LANES
    for n in range(NEAR):
        wide_s[n] = arrived[n].astype(F32)
    for c in range(cuts):
        for n in range(NEAR):
            row_s[n * own : (n + 1) * own, c * LANES : (c + 1) * LANES] = wide_s[
                n, c * own : (c + 1) * own, :
            ]
    down = mm(row_s[...].astype(BF16), w_down[...]).astype(BF16)
    for i in range(peers):
        out[i] = down


def last_body(at, arrived, resid, out):
    width = out.shape[1]
    down = arrived[0].astype(F32)
    for i in range(1, arrived.shape[0]):
        down = down + arrived[i].astype(F32)
    whole = (resid[...].astype(F32) + down).astype(BF16)
    shape = (LANES, width)
    pick = jnp.where(iota(shape, 0) == iota(shape, 1) + at[0] * width, 1.0, 0.0).astype(BF16)
    out[...] = mm(whole, pick).astype(BF16)


def rotate(vectors, cosine, sine):
    half = DK // 2
    outs = []
    for h in range(vectors.shape[1] // DK):
        a = vectors[:, h * DK : h * DK + half]
        b = vectors[:, h * DK + half : (h + 1) * DK]
        outs += [a * cosine - b * sine, a * sine + b * cosine]
    return jnp.concatenate(outs, axis=1)


def cache_partial(query_low, lengths, log_decay, key_cache, value_cache, heads_here):
    batch_rows = query_low.shape[0]
    span = key_cache.shape[1]
    slots = lax.axis_index("kv") * span + jnp.arange(span, dtype=jnp.int32)
    live = slots[None, :] < lengths[:, None]
    gaps = jnp.maximum((lengths[:, None] - slots[None, :]).astype(F32), 0.0)
    decays = jnp.exp(log_decay[None, None, :] * gaps[:, :, None])
    keys_here = key_cache.reshape(batch_rows, span, heads_here, DK)
    values_here = value_cache.reshape(batch_rows, span, heads_here, DK)
    scores = jnp.einsum("bphd,bhd->bph", keys_here, query_low, preferred_element_type=F32)
    mixing = jnp.where(live[:, :, None], scores * decays, 0.0).astype(BF16)
    return jnp.einsum("bph,bphd->bhd", mixing, values_here, preferred_element_type=F32)


def local(
    tokens,
    lengths,
    attn_gain,
    w_query,
    w_key,
    w_value,
    w_gate,
    log_decay,
    key_cache,
    value_cache,
    gn_gain,
    w_out,
    ffn_gain,
    w_ffn_gate,
    w_ffn_up,
    w_ffn_down,
):
    shape = jax.ShapeDtypeStruct
    rows = tokens.shape[0]
    heads_here = log_decay.shape[0]
    width = heads_here * DK
    kv = lax.axis_size("kv")
    tp = lax.axis_size("tp")
    far = kv // NEAR
    own = rows // NEAR
    at = lax.axis_index("tp").astype(jnp.int32).reshape(1)

    placed = kernel(place_body, shape((tp, rows, LANES), BF16), at, tokens, scalars=1)
    blocks, part_value, part_gate, x = kernel(
        project_body,
        (
            shape((NEAR, 2 * rows + 8, LANES), BF16),
            shape((rows, width), F32),
            shape((rows, width), F32),
            shape((rows, LANES), F32),
        ),
        exchange(placed, "tp"),
        attn_gain.reshape(1, LANES),
        w_query,
        w_key,
        w_value,
        w_gate,
    )
    got = wide_sum(exchange(blocks, "kv", groups_near()))
    vector = got[2 * rows] + got[2 * rows + 1]
    high = lax.reduce_precision(vector, 8, 7)
    tail = jnp.pad(jnp.stack([high, vector - high]), ((0, 6), (0, 0)))
    got = jnp.concatenate([got[: 2 * rows], tail], axis=0)
    got = wide_sum(spread(got.astype(BF16), "kv", far, groups_far()))
    squares = (got[2 * rows] + got[2 * rows + 1])[:rows]
    whole = spread(got[: 2 * rows].astype(BF16), "kv", NEAR, groups_near())
    q_raw, k_raw = side(whole[:, :rows]).astype(F32), side(whole[:, rows:]).astype(F32)

    factor = lax.rsqrt(squares / D + RMS_EPS)[:, None]
    positions = lengths.astype(F32)
    half = DK // 2
    inverse = ROPE_BASE ** (-jnp.arange(half, dtype=F32) / half)
    angles = positions[:, None] * inverse[None, :]
    cosine, sine = jnp.cos(angles), jnp.sin(angles)
    queries = rotate(q_raw * factor, cosine, sine) * DK ** (-0.5)
    keys = rotate(k_raw * factor, cosine, sine)
    by_head = (rows, heads_here, DK)
    own_dot = jnp.sum((queries * keys).reshape(by_head), axis=-1, keepdims=True)
    cached = cache_partial(
        queries.astype(BF16).reshape(by_head),
        lengths,
        log_decay,
        key_cache,
        value_cache,
        heads_here,
    )
    totals = cached + own_dot * (part_value * factor).reshape(by_head)
    totals = totals - jnp.mean(totals, axis=-1, keepdims=True)
    totals = totals.reshape(rows, width)
    gates = part_gate * factor
    both = jnp.stack(
        [
            jnp.concatenate([a[:, n * LANES : (n + 1) * LANES] for a in (totals, gates)], axis=0)
            for n in range(NEAR)
        ]
    )
    got = wide_sum(exchange(both.astype(BF16), "kv", groups_near()))
    got = wide_sum(spread(got.astype(BF16), "kv", far, groups_far()))
    whole = spread(got.astype(BF16), "kv", NEAR, groups_near())

    mixed = kernel(
        mix_body, shape((tp, rows, LANES), BF16), whole, gn_gain.reshape(1, width), w_out
    )
    wide = w_ffn_gate.shape[1]
    cuts = wide // LANES
    packed = -(-(2 * cuts * own + 1) // 8) * 8
    blocks, resid = kernel(
        ffn_in_body,
        (shape((NEAR, packed, LANES), BF16), shape((rows, LANES), BF16)),
        x,
        exchange(mixed, "tp"),
        ffn_gain.reshape(1, LANES),
        w_ffn_gate,
        w_ffn_up,
        scratch=(
            pltpu.VMEM((rows, wide), F32),
            pltpu.VMEM((rows, wide), F32),
            pltpu.VMEM((NEAR, packed, LANES), F32),
        ),
    )
    got = wide_sum(exchange(blocks, "kv", groups_near()))
    arrived = spread(got.astype(BF16), "kv", far, groups_far())
    padded = -(-cuts * own // 8) * 8
    hidden = kernel(
        lambda *refs: hidden_body(*refs, own=own, cuts=cuts),
        shape((NEAR, padded, LANES), BF16),
        arrived,
        scratch=(pltpu.VMEM((packed, LANES), F32),),
    )
    down = kernel(
        down_body,
        shape((tp, rows, LANES), BF16),
        exchange(hidden, "kv", groups_near()),
        w_ffn_down,
        scratch=(pltpu.VMEM((NEAR, padded, LANES), F32), pltpu.VMEM((rows, wide), F32)),
    )
    return kernel(
        last_body, shape(tokens.shape, BF16), at, exchange(down, "tp"), resid, scalars=1
    )


def solution(mesh):
    return jax.shard_map(
        local,
        mesh=mesh,
        in_specs=(
            P("grp", ("kv", "tp")),
            P("grp"),
            P("kv"),
            P("kv", "tp"),
            P("kv", "tp"),
            P("kv", "tp"),
            P("kv", "tp"),
            P("tp"),
            P("grp", "kv", "tp"),
            P("grp", "kv", "tp"),
            P("tp"),
            P("tp", "kv"),
            P("kv"),
            P("kv", "tp"),
            P("kv", "tp"),
            P("tp", "kv"),
        ),
        out_specs=P("grp", ("kv", "tp")),
        check_vma=False,
    )
```

time: 246 us -> 252 us (1.024)
  blocking collectives: 161 us -> 192 us
  starting transfers between devices: 30 us -> 10.6 us
  Pallas kernels: 0 us -> 12.5 us
  waiting for transfers between devices: 35.6 us -> 28.1 us
  local copies, waits for them, and re-layouts: 12.6 us -> 5.71 us
    all_to_all x7 -> x10, blocking collectives: 161 us -> 192 us  [exchange(): lax.all_to_all(blocks, axis, split_axis=0, concat_axis=0, tiled=True, axi...]
    all_to_all x4 -> x2, starting transfers between devices: 30 us -> 10.6 us  [exchange(): lax.all_to_all(blocks, axis, split_axis=0, concat_axis=0, tiled=True, axi...]
    pallas_call x0 -> x7, Pallas kernels: none -> 12.5 us  [kernel(): pl.pallas_call(body, out_shape=outs, in_specs=[smem] * scalars + [vmem] *...]
    all_to_all x4 -> x2, waiting for transfers between devices: 35.6 us -> 28.1 us  [exchange(): lax.all_to_all(blocks, axis, split_axis=0, concat_axis=0, tiled=True, axi...]
    unnamed x45 -> x16, local copies, waits for them, and re-layouts: 6.14 us -> 2.33 us
  transfers between devices with their start and end apart: 4 -> 2, of which waited for: 4 -> 2; matrix products, arithmetic and copies ran while one was open for 0% -> 0% of each run, Pallas kernels for 0% -> 0%
where the time goes in v2:
time: 252 us; the launch traced here: 250 us
  blocking collectives  192 us (76%)
  waiting for transfers between devices  28.1 us (11%)
  Pallas kernels  12.5 us (5%)
  starting transfers between devices  10.6 us (4%)
  local copies, waits for them, and re-layouts  5.71 us (2%)
    all_to_all x10, blocking collectives, exchange(): lax.all_to_all(blocks, axis, split_axis=0, concat_axis=0, tiled=True, axi...  192 us
    all_to_all x2, waiting for transfers between devices, exchange(): lax.all_to_all(blocks, axis, split_axis=0, concat_axis=0, tiled=True, axi...  28.1 us
    pallas_call x7, Pallas kernels, kernel(): pl.pallas_call(body, out_shape=outs, in_specs=[smem] * scalars + [vmem] *...  12.5 us
    all_to_all x2, starting transfers between devices, exchange(): lax.all_to_all(blocks, axis, split_axis=0, concat_axis=0, tiled=True, axi...  10.6 us
  transfers between devices with their start and end apart: 2, of which 2 were waited for; matrix products, arithmetic and copies ran while one was open for 0% of the time, Pallas kernels for 0%

profile of v2, /device:TPU:33, one launch (start us, length us, event | category | flops | bytes accessed | tf_op | source)
XLA Modules:
  0.0 250.3 jit_solution(9032175833250625613)
XLA Ops:
  0.0 0.0 copy-start.3
  0.0 0.7 copy-done.3
  0.7 0.7 copy.19.tokens
  1.4 1.4 shard_map.154
  2.8 50.2 %all_to_all.60.parts = bf16[8,24,128]{2,1,0:T(8,128)(2,1)} all-to-all(bf16[8,24,128]{2,1,0:T(8,128)(2,1)} %shard_map.154), channel_id=1, replica_groups=mesh['grp'=2,'kv'=32,'tp'=8] {'tp'}, dimensions={0} | all-to-all | bytes 98304 | tf_op jit(solution)/shard_map/all_to_all | solution.py:31
  53.0 0.0 copy-start.6
  53.0 2.0 shard_map.155
  55.0 7.9 %all_to_all.61 = bf16[4,56,128]{2,1,0:T(8,128)(2,1)S(1)} all-to-all(bf16[4,56,128]{2,1,0:T(8,128)(2,1)} %get-tuple-element.12), channel_id=1, replica_groups={{0,8,16,24},{32,40,48,56},{64,72,80,88},{96,104,112,120},{128,136,144,1..., dimensions={0} | all-to-all | bytes 114688 | tf_op jit(solution)/shard_map/all_to_all | solution.py:31
  63.0 0.6 broadcast_in_dim.23
  63.6 6.0 %all-to-all-start.2 = ((bf16[8,56,128]{2,1,0:T(8,128)(2,1)}), bf16[8,56,128]{2,1,0:T(8,128)(2,1)S(1)}, u32[]{:S(2)}, u32[]{:S(2)}) async-start(bf16[8,56,128]{2,1,0:T(8,128)(2,1)} %broadcast_in_dim.23), calls=%async_computation.2 | async-start | bytes 229376 | tf_op jit(solution)/shard_map/all_to_all | solution.py:31
  69.7 0.0 copy-start.4
  69.7 0.7 copy-done.4
  70.4 0.1 broadcast_compare_fusion
  70.4 0.1 convert_maximum_fusion
  70.5 23.6 %all-to-all-done.2 = bf16[8,56,128]{2,1,0:T(8,128)(2,1)S(1)} async-done(((bf16[8,56,128]{2,1,0:T(8,128)(2,1)}), bf16[8,56,128]{2,1,0:T(8,128)(2,1)S(1)}, u32[]{:S(2)}, u32[]{:S(2)}) %all-to-all-start.2) | async-done | bytes 114720 | tf_op jit(solution)/shard_map/all_to_all | solution.py:31
  94.1 0.6 broadcast_in_dim.24
  94.7 4.5 %all-to-all-start.3 = ((bf16[4,48,128]{2,1,0:T(8,128)(2,1)}), bf16[4,48,128]{2,1,0:T(8,128)(2,1)S(1)}, u32[]{:S(2)}, u32[]{:S(2)}) async-start(bf16[4,48,128]{2,1,0:T(8,128)(2,1)} %broadcast_in_dim.24), calls=%async_computation.3 | async-start | bytes 98304 | tf_op jit(solution)/shard_map/all_to_all | solution.py:31
  99.3 0.0 copy-start.1
  99.3 0.0 copy-start.2
  99.3 4.5 %all-to-all-done.3 = bf16[4,48,128]{2,1,0:T(8,128)(2,1)S(1)} async-done(((bf16[4,48,128]{2,1,0:T(8,128)(2,1)}), bf16[4,48,128]{2,1,0:T(8,128)(2,1)S(1)}, u32[]{:S(2)}, u32[]{:S(2)}) %all-to-all-start.3) | async-done | bytes 49184 | tf_op jit(solution)/shard_map/all_to_all | solution.py:31
  103.8 0.0 copy-done.1
  103.8 0.0 copy-done.2
  103.8 0.1 convert_multiply_fusion.1
  103.9 0.1 fusion.29
  104.2 0.0 copy-done.6
  104.2 0.0 copy-start.5
  104.2 0.3 fusion.6
  104.5 0.0 copy-start
  104.5 0.2 copy.23
  104.8 0.1 copy-done.5
  104.9 0.3 fusion.11
  105.2 0.3 copy.24
  105.5 0.2 copy-done
  105.7 0.2 fusion.3
  105.9 0.2 fusion.43
  106.1 0.1 subtract_convert_fusion
  106.3 7.0 %all_to_all.62 = bf16[4,48,128]{2,1,0:T(8,128)(2,1)S(1)} all-to-all(bf16[4,48,128]{2,1,0:T(8,128)(2,1)S(1)} %pad_maximum_fusion), channel_id=1, replica_groups={{0,8,16,24},{32,40,48,56},{64,72,80,88},{96,104,112,120},{128,136,144,1..., dimensions={0} | all-to-all | bytes 98304 | tf_op jit(solution)/shard_map/all_to_all | solution.py:31
  113.3 28.3 %all_to_all.63 = bf16[8,48,128]{2,1,0:T(8,128)(2,1)S(1)} all-to-all(bf16[8,48,128]{2,1,0:T(8,128)(2,1)S(1)} %broadcast_in_dim.43), channel_id=1, replica_groups={{0,32,64,96,128,160,192,224},{8,40,72,104,136,168,200,232},{16,48,80,11..., dimensions={0} | all-to-all | bytes 196608 | tf_op jit(solution)/shard_map/all_to_all | solution.py:31
  141.7 8.6 %all_to_all.64.blocks = bf16[4,48,128]{2,1,0:T(8,128)(2,1)} all-to-all(bf16[4,48,128]{2,1,0:T(8,128)(2,1)S(1)} %broadcast_in_dim.44), channel_id=1, replica_groups={{0,8,16,24},{32,40,48,56},{64,72,80,88},{96,104,112,120},{128,136,144,1..., dimensions={0} | all-to-all | bytes 98304 | tf_op jit(solution)/shard_map/all_to_all | solution.py:31
  150.2 1.9 shard_map.156
  152.1 15.3 %all_to_all.65.parts = bf16[8,24,128]{2,1,0:T(8,128)(2,1)} all-to-all(bf16[8,24,128]{2,1,0:T(8,128)(2,1)} %shard_map.156), channel_id=1, replica_groups=mesh['grp'=2,'kv'=32,'tp'=8] {'tp'}, dimensions={0} | all-to-all | bytes 98304 | tf_op jit(solution)/shard_map/all_to_all | solution.py:31
  167.4 2.1 shard_map.157
  169.5 8.8 %all_to_all.66 = bf16[4,136,128]{2,1,0:T(8,128)(2,1)S(1)} all-to-all(bf16[4,136,128]{2,1,0:T(8,128)(2,1)} %get-tuple-element.15), channel_id=1, replica_groups={{0,8,16,24},{32,40,48,56},{64,72,80,88},{96,104,112,120},{128,136,144,1..., dimensions={0} | all-to-all | bytes 278528 | tf_op jit(solution)/shard_map/all_to_all | solution.py:31
  178.4 35.6 %all_to_all.67.refs_0_ = bf16[8,136,128]{2,1,0:T(8,128)(2,1)} all-to-all(bf16[8,136,128]{2,1,0:T(8,128)(2,1)S(1)} %broadcast_in_dim.45), channel_id=1, replica_groups={{0,32,64,96,128,160,192,224},{8,40,72,104,136,168,200,232},{16,48,80,11..., dimensions={0} | all-to-all | bytes 557056 | tf_op jit(solution)/shard_map/all_to_all | solution.py:31
  214.0 1.7 shard_map.158
  215.7 16.7 %all_to_all.68.arrived = bf16[4,72,128]{2,1,0:T(8,128)(2,1)} all-to-all(bf16[4,72,128]{2,1,0:T(8,128)(2,1)} %shard_map.158), channel_id=1, replica_groups={{0,8,16,24},{32,40,48,56},{64,72,80,88},{96,104,112,120},{128,136,144,1..., dimensions={0} | all-to-all | bytes 147456 | tf_op jit(solution)/shard_map/all_to_all | solution.py:31
  232.4 1.8 shard_map.159
  234.3 13.1 %all_to_all.69.arrived = bf16[8,24,128]{2,1,0:T(8,128)(2,1)} all-to-all(bf16[8,24,128]{2,1,0:T(8,128)(2,1)} %shard_map.159), channel_id=1, replica_groups=mesh['grp'=2,'kv'=32,'tp'=8] {'tp'}, dimensions={0} | all-to-all | bytes 98304 | tf_op jit(solution)/shard_map/all_to_all | solution.py:31
  247.4 1.5 shard_map.160
  248.9 1.4 copy.20
  (30 shorter events, 0.4 us)
Async XLA Ops:
  0.0 0.7 copy-start.3
  53.0 51.2 %copy-start.6 = (bf16[24,32,512]{2,1,0:T(8,128)(2,1)S(1)}, bf16[24,32,512]{2,1,0:T(8,128)(2,1)}, u32[]{:S(2)}) copy-start(bf16[24,32,512]{2,1,0:T(8,128)(2,1)} %param.24) | copy-start | bytes 2359300
  63.6 30.4 %all-to-all-start.2 = ((bf16[8,56,128]{2,1,0:T(8,128)(2,1)}), bf16[8,56,128]{2,1,0:T(8,128)(2,1)S(1)}, u32[]{:S(2)}, u32[]{:S(2)}) async-start(bf16[8,56,128]{2,1,0:T(8,128)(2,1)} %broadcast_in_dim.23), calls=%async_computation.2 | async-start | bytes 229376 | tf_op jit(solution)/shard_map/all_to_all | solution.py:31
  69.7 0.7 copy-start.4
  94.7 9.1 %all-to-all-start.3 = ((bf16[4,48,128]{2,1,0:T(8,128)(2,1)}), bf16[4,48,128]{2,1,0:T(8,128)(2,1)S(1)}, u32[]{:S(2)}, u32[]{:S(2)}) async-start(bf16[4,48,128]{2,1,0:T(8,128)(2,1)} %broadcast_in_dim.24), calls=%async_computation.3 | async-start | bytes 98304 | tf_op jit(solution)/shard_map/all_to_all | solution.py:31
  99.3 4.5 %copy-start.1 = (f32[24,512]{1,0:T(8,128)S(1)}, f32[24,512]{1,0:T(8,128)}, u32[]{:S(2)}) copy-start(f32[24,512]{1,0:T(8,128)} %get-tuple-element.13) | copy-start | bytes 147460
  99.3 4.5 %copy-start.2 = (f32[24,512]{1,0:T(8,128)S(1)}, f32[24,512]{1,0:T(8,128)}, u32[]{:S(2)}) copy-start(f32[24,512]{1,0:T(8,128)} %get-tuple-element.14) | copy-start | bytes 147460
  104.2 0.7 copy-start.5
  104.5 1.2 copy-start

commit v3 on v1

v3 whole, which is shorter than its diff:
```python
import jax
import jax.numpy as jnp
import numpy as np
from jax import lax
from jax.sharding import PartitionSpec as P

DK = 256
D = 4096
LANES = 128
NEAR = 4

RMS_EPS = 0.1
GN_EPS = 1.0
ROPE_BASE = 10000.0


def groups_near():
    n = lax.axis_size("kv")
    return [list(range(i, i + NEAR)) for i in range(0, n, NEAR)]


def groups_far():
    n = lax.axis_size("kv")
    return [list(range(i, n, NEAR)) for i in range(NEAR)]


def exchange(blocks, axis, groups=None):
    return lax.all_to_all(
        blocks, axis, split_axis=0, concat_axis=0, tiled=True, axis_index_groups=groups
    )


def spread(array, axis, peers, groups=None):
    return exchange(jnp.broadcast_to(array, (peers, *array.shape)), axis, groups)


def wide_sum(blocks):
    return jnp.sum(blocks.astype(jnp.float32), axis=0)


def hi_lo_rows(vector):
    high = lax.reduce_precision(vector, 8, 7)
    rows = jnp.stack([high, vector - high])
    return jnp.pad(rows, ((0, 6), (0, LANES - vector.shape[0])))


def near_blocks(array):
    return jnp.stack(
        [array[:, i * LANES : (i + 1) * LANES] for i in range(array.shape[1] // LANES)]
    )


def side(blocks):
    return jnp.concatenate([blocks[i] for i in range(blocks.shape[0])], axis=1)


def reduce_pair(first, second, extra=None, work=None, inputs=()):
    far = lax.axis_size("kv") // NEAR
    rows = first.shape[0]
    blocks = jnp.concatenate([near_blocks(first), near_blocks(second)], axis=1)
    if extra is not None:
        tail = jnp.broadcast_to(hi_lo_rows(extra), (NEAR, 8, LANES))
        blocks = jnp.concatenate([blocks, tail], axis=1)
    got = wide_sum(exchange(blocks.astype(jnp.bfloat16), "kv", groups_near()))
    if extra is not None:
        vector = got[2 * rows] + got[2 * rows + 1]
        got = jnp.concatenate([got[: 2 * rows], hi_lo_rows(vector[: extra.shape[0]])], axis=0)
    got = got.astype(jnp.bfloat16)
    if work is not None:
        got, inputs = lax.optimization_barrier((got, inputs))
        done = work(*inputs)
    got = spread(got, "kv", far, groups_far())
    if work is not None:
        got, done = lax.optimization_barrier((got, done))
    got = wide_sum(got)
    mine = got[: 2 * rows].astype(jnp.bfloat16)
    if extra is not None:
        vector = (got[2 * rows] + got[2 * rows + 1])[: extra.shape[0]]
        vector = lax.rsqrt(vector / D + RMS_EPS)
        mine, vector = lax.optimization_barrier((mine, vector))
    whole = spread(mine, "kv", NEAR, groups_near())
    outs = (
        side(whole[:, :rows]).astype(jnp.float32),
        side(whole[:, rows:]).astype(jnp.float32),
    )
    if extra is None:
        return outs
    return (*outs, vector, done)


def near_columns(gate, up, stat, padded):
    quarter = gate.shape[1] // NEAR
    rest = padded - quarter
    zeros = jnp.zeros((gate.shape[0], rest), gate.dtype)
    fill = jnp.concatenate([stat[:, None].astype(gate.dtype), zeros[:, 1:]], axis=1)
    blocks = []
    for n in range(NEAR):
        own = slice(n * quarter, (n + 1) * quarter)
        blocks.append(jnp.concatenate([gate[:, own], fill, up[:, own], zeros], axis=1))
    return jnp.stack(blocks)


def rotate(vectors, cosine, sine):
    half = DK // 2
    outs = []
    for h in range(vectors.shape[1] // DK):
        a = vectors[:, h * DK : h * DK + half]
        b = vectors[:, h * DK + half : (h + 1) * DK]
        outs += [a * cosine - b * sine, a * sine + b * cosine]
    return jnp.concatenate(outs, axis=1)


def decay_factors(lengths, log_decay, span, at):
    slots = at * span + jnp.arange(span, dtype=jnp.int32)
    gaps = (lengths[:, None] - slots[None, :]).astype(jnp.float32)
    live = gaps > 0.0
    decays = jnp.exp(log_decay[None, None, :] * jnp.maximum(gaps, 0.0)[:, :, None])
    return jnp.where(live[:, :, None], decays, 0.0)


def cache_partial(query_low, decays, key_cache, value_cache, heads_here):
    batch_rows, span = decays.shape[:2]
    keys_here = key_cache.reshape(batch_rows, span, heads_here, DK)
    values_here = value_cache.reshape(batch_rows, span, heads_here, DK)
    scores = jnp.einsum("bphd,bhd->bph", keys_here, query_low, preferred_element_type=jnp.float32)
    mixing = (scores * decays).astype(jnp.bfloat16)
    return jnp.einsum("bph,bphd->bhd", mixing, values_here, preferred_element_type=jnp.float32)


def local(
    tokens,
    lengths,
    attn_gain,
    w_query,
    w_key,
    w_value,
    w_gate,
    log_decay,
    key_cache,
    value_cache,
    gn_gain,
    w_out,
    ffn_gain,
    w_ffn_gate,
    w_ffn_up,
    w_ffn_down,
):
    rows = tokens.shape[0]
    heads_here = log_decay.shape[0]
    kv = lax.axis_size("kv")
    tp = lax.axis_size("tp")
    own_width = tokens.shape[1]
    gathered = spread(tokens, "tp", tp)
    x = jnp.moveaxis(gathered, 0, 1).reshape(rows, tp * own_width).astype(jnp.float32)
    own_squares = jnp.sum(x * x, axis=1)
    scaled = (x * attn_gain).astype(jnp.bfloat16)
    dot = lambda a, w: jnp.dot(a, w, preferred_element_type=jnp.float32)

    def ahead(scaled, lengths, log_decay, w_value, w_gate, kv_at):
        half = DK // 2
        inverse = (ROPE_BASE ** (-np.arange(half) / half)).astype(np.float32)
        angles = lengths.astype(jnp.float32)[:, None] * inverse[None, :]
        return (
            jnp.cos(angles),
            jnp.sin(angles),
            decay_factors(lengths, log_decay, key_cache.shape[1], kv_at),
            dot(scaled, w_value),
            dot(scaled, w_gate),
        )

    q_raw, k_raw, factor, made = reduce_pair(
        dot(scaled, w_query),
        dot(scaled, w_key),
        own_squares,
        ahead,
        (scaled, lengths, log_decay, w_value, w_gate, lax.axis_index("kv")),
    )
    cosine, sine, decays, part_value, part_gate = made
    factor = factor[:, None]
    queries = rotate(q_raw * factor, cosine, sine) * DK ** (-0.5)
    keys = rotate(k_raw * factor, cosine, sine)
    by_head = (rows, heads_here, DK)
    own_dot = jnp.sum((queries * keys).reshape(by_head), axis=-1, keepdims=True)
    cached = cache_partial(
        queries.astype(jnp.bfloat16).reshape(by_head),
        decays,
        key_cache,
        value_cache,
        heads_here,
    )
    part_value = part_value * factor
    totals = cached + own_dot * part_value.reshape(by_head)
    totals = totals - jnp.mean(totals, axis=-1, keepdims=True)
    part_gate = part_gate * factor
    totals, gates = reduce_pair(totals.reshape(rows, heads_here * DK), part_gate)
    totals = totals.reshape(by_head)
    center = jnp.mean(totals, axis=-1, keepdims=True)
    spread_ = jnp.mean(totals * totals, axis=-1, keepdims=True) - center * center
    normed = ((totals - center) * lax.rsqrt(spread_ + GN_EPS)).reshape(rows, heads_here * DK)
    gated = (jax.nn.silu(gates) * (normed * gn_gain)).astype(jnp.bfloat16)
    mixed = dot(gated, w_out).astype(jnp.bfloat16)
    own_at = (lax.axis_index("tp") * own_width).astype(jnp.uint32)
    mixed, own_at = lax.optimization_barrier((mixed, own_at))
    mixed = wide_sum(spread(mixed, "tp", tp))
    resid = (x + mixed).astype(jnp.bfloat16)
    resid_wide = resid.astype(jnp.float32)
    mid_squares = jnp.sum(resid_wide * resid_wide, axis=1)
    scaled_mid = (resid_wide * ffn_gain).astype(jnp.bfloat16)
    own_resid = lax.dynamic_slice(resid_wide, (jnp.uint32(0), own_at), (rows, own_width))
    quarter = w_ffn_gate.shape[1] // NEAR
    padded = -(-(quarter + 1) // LANES) * LANES
    blocks = near_columns(
        dot(scaled_mid, w_ffn_gate).astype(jnp.bfloat16),
        dot(scaled_mid, w_ffn_up).astype(jnp.bfloat16),
        mid_squares,
        padded,
    )
    blocks, own_resid = lax.optimization_barrier((blocks, own_resid))
    got = wide_sum(exchange(blocks, "kv", groups_near()))
    got = wide_sum(spread(got.astype(jnp.bfloat16), "kv", kv // NEAR, groups_far()))
    factor_mid = lax.rsqrt(got[:, quarter : quarter + 1] / D + RMS_EPS)
    hidden = jax.nn.silu(got[:, :padded] * factor_mid) * (got[:, padded:] * factor_mid)
    whole = spread(hidden.astype(jnp.bfloat16), "kv", NEAR, groups_near())
    hidden = side(whole[:, :, :quarter])
    down_part = dot(hidden, w_ffn_down).astype(jnp.bfloat16)
    down = wide_sum(
        exchange(jnp.moveaxis(down_part.reshape(rows, tp, own_width), 1, 0), "tp")
    )
    return (own_resid + down).astype(jnp.bfloat16)


def solution(mesh):
    return jax.shard_map(
        local,
        mesh=mesh,
        in_specs=(
            P("grp", ("kv", "tp")),
            P("grp"),
            P("kv"),
            P("kv", "tp"),
            P("kv", "tp"),
            P("kv", "tp"),
            P("kv", "tp"),
            P("tp"),
            P("grp", "kv", "tp"),
            P("grp", "kv", "tp"),
            P("tp"),
            P("tp", "kv"),
            P("kv"),
            P("kv", "tp"),
            P("kv", "tp"),
            P("tp", "kv"),
        ),
        out_specs=P("grp", ("kv", "tp")),
        check_vma=False,
    )
```

time: 246 us -> 241 us (0.980)
  blocking collectives: 161 us -> 179 us
  starting transfers between devices: 30 us -> 14.9 us
  waiting for transfers between devices: 35.6 us -> 31.4 us
  local copies, waits for them, and re-layouts: 12.6 us -> 9.79 us
    all_to_all x7 -> x9, blocking collectives: 161 us -> 179 us  [exchange(): lax.all_to_all(blocks, axis, split_axis=0, concat_axis=0, tiled=True, axi...]
    all_to_all x4 -> x3, starting transfers between devices: 30 us -> 14.9 us  [exchange(): lax.all_to_all(blocks, axis, split_axis=0, concat_axis=0, tiled=True, axi...]
    all_to_all x4 -> x3, waiting for transfers between devices: 35.6 us -> 31.4 us  [exchange(): lax.all_to_all(blocks, axis, split_axis=0, concat_axis=0, tiled=True, axi...]
    unnamed x45 -> x43, local copies, waits for them, and re-layouts: 6.14 us -> 5.44 us
  transfers between devices with their start and end apart: 4 -> 3, of which waited for: 4 -> 3; matrix products, arithmetic and copies ran while one was open for 0% -> 0% of each run, Pallas kernels for 0% -> 0%
where the time goes in v3:
time: 241 us; the launch traced here: 240 us
  blocking collectives  179 us (74%)
  waiting for transfers between devices  31.4 us (13%)
  starting transfers between devices  14.9 us (6%)
  local copies, waits for them, and re-layouts  9.79 us (4%)
    all_to_all x9, blocking collectives, exchange(): lax.all_to_all(blocks, axis, split_axis=0, concat_axis=0, tiled=True, axi...  179 us
    all_to_all x3, waiting for transfers between devices, exchange(): lax.all_to_all(blocks, axis, split_axis=0, concat_axis=0, tiled=True, axi...  31.4 us
    all_to_all x3, starting transfers between devices, exchange(): lax.all_to_all(blocks, axis, split_axis=0, concat_axis=0, tiled=True, axi...  14.9 us
    unnamed x43, local copies, waits for them, and re-layouts  5.44 us
  transfers between devices with their start and end apart: 3, of which 3 were waited for; matrix products, arithmetic and copies ran while one was open for 0% of the time, Pallas kernels for 0%

profile of v3, /device:TPU:33, one launch (start us, length us, event | category | flops | bytes accessed | tf_op | source)
XLA Modules:
  0.0 239.7 jit_solution(17725689024347360548)
XLA Ops:
  0.0 0.7 broadcast_bitcast_fusion
  0.7 0.1 reshape.171
  0.9 48.5 %all_to_all.60 = bf16[8,2,192]{2,1,0:T(2,128)(2,1)S(1)} all-to-all(bf16[8,2,192]{2,1,0:T(2,128)(2,1)S(1)} %reshape.171), channel_id=1, replica_groups=mesh['grp'=2,'kv'=32,'tp'=8] {'tp'}, dimensions={0} | all-to-all | bytes 12288 | tf_op jit(solution)/shard_map/all_to_all | solution.py:28
  49.3 0.1 reshape.172
  49.6 0.5 copy-done.11
  50.1 0.1 copy-done.4
  50.2 0.1 convolution_convert_fusion.2
  50.4 0.1 convolution_convert_fusion.3
  50.6 0.6 pad_maximum_fusion.1
  51.2 3.4 %all-to-all-start.1 = ((bf16[4,56,128]{2,1,0:T(8,128)(2,1)}), bf16[4,56,128]{2,1,0:T(8,128)(2,1)S(1)}, u32[]{:S(2)}, u32[]{:S(2)}) async-start(bf16[4,56,128]{2,1,0:T(8,128)(2,1)} %pad_maximum_fusion.1), calls=%async_computation.1 | async-start | bytes 114688 | tf_op jit(solution)/shard_map/all_to_all | solution.py:28
  54.6 4.5 %all-to-all-done.1 = bf16[4,56,128]{2,1,0:T(8,128)(2,1)S(1)} async-done(((bf16[4,56,128]{2,1,0:T(8,128)(2,1)}), bf16[4,56,128]{2,1,0:T(8,128)(2,1)S(1)}, u32[]{:S(2)}, u32[]{:S(2)}) %all-to-all-start.1) | async-done | bytes 57376 | tf_op jit(solution)/shard_map/all_to_all | solution.py:28
  59.2 0.7 broadcast_in_dim.59
  59.8 7.5 %all-to-all-start.2 = ((bf16[8,56,128]{2,1,0:T(8,128)(2,1)}), bf16[8,56,128]{2,1,0:T(8,128)(2,1)S(1)}, u32[]{:S(2)}, u32[]{:S(2)}) async-start(bf16[8,56,128]{2,1,0:T(8,128)(2,1)} %broadcast_in_dim.59), calls=%async_computation.2 | async-start | bytes 229376 | tf_op jit(solution)/shard_map/all_to_all | solution.py:28
  67.4 0.1 multiply_sine_fusion
  67.6 0.1 fusion.51
  67.8 0.5 copy-done.7
  68.2 0.1 fusion.52
  68.3 0.5 copy-done.10
  68.9 0.3 exponential_select_fusion
  69.1 22.4 %all-to-all-done.2 = bf16[8,56,128]{2,1,0:T(8,128)(2,1)S(1)} async-done(((bf16[8,56,128]{2,1,0:T(8,128)(2,1)}), bf16[8,56,128]{2,1,0:T(8,128)(2,1)S(1)}, u32[]{:S(2)}, u32[]{:S(2)}) %all-to-all-start.2) | async-done | bytes 114720 | tf_op jit(solution)/shard_map/all_to_all | solution.py:28
  91.6 9.0 %all_to_all.61 = bf16[4,48,128]{2,1,0:T(8,128)(2,1)S(1)} all-to-all(bf16[4,48,128]{2,1,0:T(8,128)(2,1)S(1)} %broadcast_in_dim.62), channel_id=1, replica_groups={{0,8,16,24},{32,40,48,56},{64,72,80,88},{96,104,112,120},{128,136,144,1..., dimensions={0} | all-to-all | bytes 98304 | tf_op jit(solution)/shard_map/all_to_all | solution.py:28
  100.9 0.3 fusion.6
  101.2 0.2 copy.108
  101.5 0.3 copy.109
  101.9 0.5 copy-done.1
  102.4 0.2 fusion.3
  102.6 0.2 fusion.50
  102.8 0.1 subtract_convert_fusion
  102.9 7.0 %all_to_all.62 = bf16[4,48,128]{2,1,0:T(8,128)(2,1)S(1)} all-to-all(bf16[4,48,128]{2,1,0:T(8,128)(2,1)S(1)} %maximum_maximum_fusion), channel_id=1, replica_groups={{0,8,16,24},{32,40,48,56},{64,72,80,88},{96,104,112,120},{128,136,144,1..., dimensions={0} | all-to-all | bytes 98304 | tf_op jit(solution)/shard_map/all_to_all | solution.py:28
  109.9 27.7 %all_to_all.63 = bf16[8,48,128]{2,1,0:T(8,128)(2,1)S(1)} all-to-all(bf16[8,48,128]{2,1,0:T(8,128)(2,1)S(1)} %broadcast_in_dim.63), channel_id=1, replica_groups={{0,32,64,96,128,160,192,224},{8,40,72,104,136,168,200,232},{16,48,80,11..., dimensions={0} | all-to-all | bytes 196608 | tf_op jit(solution)/shard_map/all_to_all | solution.py:28
  137.6 0.6 broadcast_in_dim.64
  138.2 4.1 %all-to-all-start.6 = ((bf16[4,48,128]{2,1,0:T(8,128)(2,1)}), bf16[4,48,128]{2,1,0:T(8,128)(2,1)S(1)}, u32[]{:S(2)}, u32[]{:S(2)}) async-start(bf16[4,48,128]{2,1,0:T(8,128)(2,1)} %broadcast_in_dim.64), calls=%async_computation.6 | async-start | bytes 98304 | tf_op jit(solution)/shard_map/all_to_all | solution.py:28
  142.3 4.6 %all-to-all-done.6 = bf16[4,48,128]{2,1,0:T(8,128)(2,1)S(1)} async-done(((bf16[4,48,128]{2,1,0:T(8,128)(2,1)}), bf16[4,48,128]{2,1,0:T(8,128)(2,1)S(1)}, u32[]{:S(2)}, u32[]{:S(2)}) %all-to-all-start.6) | async-done | bytes 49184 | tf_op jit(solution)/shard_map/all_to_all | solution.py:28
  147.0 0.1 fusion.47
  147.3 0.1 copy.97
  147.3 0.1 mul.261
  147.7 0.7 copy-done.14
  148.4 0.2 convolution_convert_fusion.4
  148.5 13.7 %all_to_all.64 = bf16[8,24,128]{2,1,0:T(8,128)(2,1)S(1)} all-to-all(bf16[8,24,128]{2,1,0:T(8,128)(2,1)S(1)} %broadcast_in_dim.65), channel_id=1, replica_groups=mesh['grp'=2,'kv'=32,'tp'=8] {'tp'}, dimensions={0} | all-to-all | bytes 98304 | tf_op jit(solution)/shard_map/all_to_all | solution.py:28
  162.3 0.1 copy.113
  162.4 0.5 copy-done.9
  163.0 0.2 convolution_convert_fusion.1
  163.1 0.1 fusion.49
  163.3 0.1 copy.99
  163.4 0.6 copy-done.2
  163.9 0.2 convolution_convert_fusion
  164.1 0.1 fusion.48
  164.3 0.1 concatenate.62
  164.4 0.1 concatenate.61
  164.5 0.1 concatenate.60
  164.6 0.1 concatenate.59
  164.7 7.9 %all_to_all.65 = bf16[4,24,768]{2,1,0:T(8,128)(2,1)S(1)} all-to-all(bf16[4,24,768]{2,1,0:T(8,128)(2,1)S(1)} %pad_maximum_fusion), channel_id=1, replica_groups={{0,8,16,24},{32,40,48,56},{64,72,80,88},{96,104,112,120},{128,136,144,1..., dimensions={0} | all-to-all | bytes 294912 | tf_op jit(solution)/shard_map/all_to_all | solution.py:28
  172.7 37.2 %all_to_all.66 = bf16[8,24,768]{2,1,0:T(8,128)(2,1)S(1)} all-to-all(bf16[8,24,768]{2,1,0:T(8,128)(2,1)S(1)} %broadcast_in_dim.67), channel_id=1, replica_groups={{0,32,64,96,128,160,192,224},{8,40,72,104,136,168,200,232},{16,48,80,11..., dimensions={0} | all-to-all | bytes 589824 | tf_op jit(solution)/shard_map/all_to_all | solution.py:28
  209.9 0.2 fusion.33
  210.1 0.1 fusion.19
  210.2 18.3 %all_to_all.67 = bf16[4,24,384]{2,1,0:T(8,128)(2,1)S(1)} all-to-all(bf16[4,24,384]{2,1,0:T(8,128)(2,1)S(1)} %broadcast_in_dim.68), channel_id=1, replica_groups={{0,8,16,24},{32,40,48,56},{64,72,80,88},{96,104,112,120},{128,136,144,1..., dimensions={0} | all-to-all | bytes 147456 | tf_op jit(solution)/shard_map/all_to_all | solution.py:28
  228.5 0.1 concatenate.63
  228.6 0.2 convolution_convert_fusion.5
  228.8 0.1 reshape.160
  228.9 0.1 copy.103
  229.0 0.1 reshape.173
  229.1 9.7 %all_to_all.68 = bf16[8,2,192]{2,1,0:T(2,128)(2,1)S(1)} all-to-all(bf16[8,2,192]{2,1,0:T(2,128)(2,1)S(1)} %reshape.173), channel_id=1, replica_groups=mesh['grp'=2,'kv'=32,'tp'=8] {'tp'}, dimensions={0} | all-to-all | bytes 12288 | tf_op jit(solution)/shard_map/all_to_all | solution.py:28
  238.9 0.1 reshape.174
  239.1 0.7 copy.105
  (89 shorter events, 1.6 us)
Async XLA Ops:
  0.0 162.4 %copy-start = (bf16[128,1408]{1,0:T(8,128)(2,1)S(1)}, bf16[128,1408]{1,0:T(8,128)(2,1)}, u32[]{:S(2)}) copy-start(bf16[128,1408]{1,0:T(8,128)(2,1)} %param.30) | copy-start | bytes 1081348
  49.3 0.9 copy-start.4
  49.4 0.7 copy-start.11
  49.5 0.9 copy-start.5
  51.2 7.9 %all-to-all-start.1 = ((bf16[4,56,128]{2,1,0:T(8,128)(2,1)}), bf16[4,56,128]{2,1,0:T(8,128)(2,1)S(1)}, u32[]{:S(2)}, u32[]{:S(2)}) async-start(bf16[4,56,128]{2,1,0:T(8,128)(2,1)} %pad_maximum_fusion.1), calls=%async_computation.1 | async-start | bytes 114688 | tf_op jit(solution)/shard_map/all_to_all | solution.py:28
  59.8 7.5 %copy-start.8 = (s32[24]{0:T(128)S(1)}, s32[24]{0:T(128)}, u32[]{:S(2)}) copy-start(s32[24]{0:T(128)} %param.18) | copy-start | bytes 292
  59.8 7.6 %copy-start.12 = (f32[128]{0:T(128)S(1)}, f32[128]{0:T(128)}, u32[]{:S(2)}) copy-start(f32[128]{0:T(128)} %constant.57) | copy-start | bytes 1540
  59.8 7.8 %copy-start.6 = (bf16[128,512]{1,0:T(8,128)(2,1)S(1)}, bf16[128,512]{1,0:T(8,128)(2,1)}, u32[]{:S(2)}) copy-start(bf16[128,512]{1,0:T(8,128)(2,1)} %param.22) | copy-start | bytes 393220
  59.8 31.7 %all-to-all-start.2 = ((bf16[8,56,128]{2,1,0:T(8,128)(2,1)}), bf16[8,56,128]{2,1,0:T(8,128)(2,1)S(1)}, u32[]{:S(2)}, u32[]{:S(2)}) async-start(bf16[8,56,128]{2,1,0:T(8,128)(2,1)} %broadcast_in_dim.59), calls=%async_computation.2 | async-start | bytes 229376 | tf_op jit(solution)/shard_map/all_to_all | solution.py:28
  67.3 0.9 copy-start.7
  68.2 0.7 copy-start.10
  69.1 31.8 %copy-start.13 = (bf16[24,32,512]{2,1,0:T(8,128)(2,1)S(1)}, bf16[24,32,512]{2,1,0:T(8,128)(2,1)}, u32[]{:S(2)}) copy-start(bf16[24,32,512]{2,1,0:T(8,128)(2,1)} %param.25) | copy-start | bytes 2359300
  101.2 1.2 copy-start.1
  138.2 8.7 %all-to-all-start.6 = ((bf16[4,48,128]{2,1,0:T(8,128)(2,1)}), bf16[4,48,128]{2,1,0:T(8,128)(2,1)S(1)}, u32[]{:S(2)}, u32[]{:S(2)}) async-start(bf16[4,48,128]{2,1,0:T(8,128)(2,1)} %broadcast_in_dim.64), calls=%async_computation.6 | async-start | bytes 98304 | tf_op jit(solution)/shard_map/all_to_all | solution.py:28
  147.4 0.9 copy-start.14
  147.7 0.7 copy-start.15
  162.3 0.7 copy-start.9
  163.0 1.0 copy-start.2
  209.9 18.7 %copy-start.3 = (bf16[1408,128]{1,0:T(8,128)(2,1)S(1)}, bf16[1408,128]{1,0:T(8,128)(2,1)}, u32[]{:S(2)}) copy-start(bf16[1408,128]{1,0:T(8,128)(2,1)} %param.32) | copy-start | bytes 1081348

commit v4 on v3

--- a/solution.py
+++ b/solution.py
@@ -147,9 +147,11 @@
 ):
     rows = tokens.shape[0]
     heads_here = log_decay.shape[0]
-    kv = lax.axis_size("kv")
     tp = lax.axis_size("tp")
     own_width = tokens.shape[1]
+    kv_at = lax.axis_index("kv")
+    own_at = (lax.axis_index("tp") * own_width).astype(jnp.uint32)
+    tokens, kv_at, own_at = lax.optimization_barrier((tokens, kv_at, own_at))
     gathered = spread(tokens, "tp", tp)
     x = jnp.moveaxis(gathered, 0, 1).reshape(rows, tp * own_width).astype(jnp.float32)
     own_squares = jnp.sum(x * x, axis=1)
@@ -173,7 +175,7 @@
         dot(scaled, w_key),
         own_squares,
         ahead,
-        (scaled, lengths, log_decay, w_value, w_gate, lax.axis_index("kv")),
+        (scaled, lengths, log_decay, w_value, w_gate, kv_at),
     )
     cosine, sine, decays, part_value, part_gate = made
     factor = factor[:, None]
@@ -199,8 +201,6 @@
     normed = ((totals - center) * lax.rsqrt(spread_ + GN_EPS)).reshape(rows, heads_here * DK)
     gated = (jax.nn.silu(gates) * (normed * gn_gain)).astype(jnp.bfloat16)
     mixed = dot(gated, w_out).astype(jnp.bfloat16)
-    own_at = (lax.axis_index("tp") * own_width).astype(jnp.uint32)
-    mixed, own_at = lax.optimization_barrier((mixed, own_at))
     mixed = wide_sum(spread(mixed, "tp", tp))
     resid = (x + mixed).astype(jnp.bfloat16)
     resid_wide = resid.astype(jnp.float32)
@@ -217,7 +217,9 @@
     )
     blocks, own_resid = lax.optimization_barrier((blocks, own_resid))
     got = wide_sum(exchange(blocks, "kv", groups_near()))
-    got = wide_sum(spread(got.astype(jnp.bfloat16), "kv", kv // NEAR, groups_far()))
+    got = wide_sum(
+        lax.all_gather(got.astype(jnp.bfloat16), "kv", axis_index_groups=groups_far())
+    )
     factor_mid = lax.rsqrt(got[:, quarter : quarter + 1] / D + RMS_EPS)
     hidden = jax.nn.silu(got[:, :padded] * factor_mid) * (got[:, padded:] * factor_mid)
     whole = spread(hidden.astype(jnp.bfloat16), "kv", NEAR, groups_near())

time: 241 us -> 228 us (0.946)
  waiting for transfers between devices: 31.4 us -> 22.4 us
  starting transfers between devices: 14.9 us -> 8.14 us
  blocking collectives: 179 us -> 184 us
    all_gather x0 -> x1, blocking collectives: none -> 31.9 us  [local(): lax.all_gather(got.astype(jnp.bfloat16), 'kv', axis_index_groups=groups_f...]
    all_to_all x9 -> x10, blocking collectives: 179 us -> 152 us  [exchange(): lax.all_to_all(blocks, axis, split_axis=0, concat_axis=0, tiled=True, axi...]
    all_to_all x3 -> x1, waiting for transfers between devices: 31.4 us -> 22.4 us  [exchange(): lax.all_to_all(blocks, axis, split_axis=0, concat_axis=0, tiled=True, axi...]
    all_to_all x3 -> x1, starting transfers between devices: 14.9 us -> 8.14 us  [exchange(): lax.all_to_all(blocks, axis, split_axis=0, concat_axis=0, tiled=True, axi...]
    unnamed x43 -> x45, local copies, waits for them, and re-layouts: 5.44 us -> 5.44 us
  transfers between devices with their start and end apart: 3 -> 1, of which waited for: 3 -> 1; matrix products, arithmetic and copies ran while one was open for 0% -> 0% of each run, Pallas kernels for 0% -> 0%
where the time goes in v4:
time: 228 us; the launch traced here: 227 us
  blocking collectives  184 us (81%)
  waiting for transfers between devices  22.4 us (10%)
  local copies, waits for them, and re-layouts  9.16 us (4%)
  starting transfers between devices  8.14 us (4%)
    all_to_all x10, blocking collectives, exchange(): lax.all_to_all(blocks, axis, split_axis=0, concat_axis=0, tiled=True, axi...  152 us
    all_gather x1, blocking collectives, local(): lax.all_gather(got.astype(jnp.bfloat16), 'kv', axis_index_groups=groups_f...  31.9 us
    all_to_all x1, waiting for transfers between devices, exchange(): lax.all_to_all(blocks, axis, split_axis=0, concat_axis=0, tiled=True, axi...  22.4 us
    all_to_all x1, starting transfers between devices, exchange(): lax.all_to_all(blocks, axis, split_axis=0, concat_axis=0, tiled=True, axi...  8.14 us
    unnamed x45, local copies, waits for them, and re-layouts  5.44 us
  transfers between devices with their start and end apart: 1, of which 1 were waited for; matrix products, arithmetic and copies ran while one was open for 0% of the time, Pallas kernels for 0%

profile of v4, /device:TPU:33, one launch (start us, length us, event | category | flops | bytes accessed | tf_op | source)
XLA Modules:
  0.0 227.4 jit_solution(9035647978246345478)
XLA Ops:
  0.0 0.7 copy-done.8
  0.7 0.1 reshape.173
  0.9 48.5 %all_to_all.55 = bf16[8,2,192]{2,1,0:T(2,128)(2,1)S(1)} all-to-all(bf16[8,2,192]{2,1,0:T(2,128)(2,1)S(1)} %reshape.173), channel_id=1, replica_groups=mesh['grp'=2,'kv'=32,'tp'=8] {'tp'}, dimensions={0} | all-to-all | bytes 12288 | tf_op jit(solution)/shard_map/all_to_all | solution.py:28
  49.3 0.1 reshape.174
  49.6 0.5 copy-done.12
  50.1 0.1 copy-done.4
  50.2 0.1 convolution_convert_fusion.2
  50.4 0.1 convolution_convert_fusion.3
  50.6 7.0 %all_to_all.56 = bf16[4,56,128]{2,1,0:T(8,128)(2,1)S(1)} all-to-all(bf16[4,56,128]{2,1,0:T(8,128)(2,1)S(1)} %pad_maximum_fusion.1), channel_id=1, replica_groups={{0,8,16,24},{32,40,48,56},{64,72,80,88},{96,104,112,120},{128,136,144,1..., dimensions={0} | all-to-all | bytes 114688 | tf_op jit(solution)/shard_map/all_to_all | solution.py:28
  57.7 0.7 broadcast_in_dim.56
  58.3 8.1 %all-to-all-start.2 = ((bf16[8,56,128]{2,1,0:T(8,128)(2,1)}), bf16[8,56,128]{2,1,0:T(8,128)(2,1)S(1)}, u32[]{:S(2)}, u32[]{:S(2)}) async-start(bf16[8,56,128]{2,1,0:T(8,128)(2,1)} %broadcast_in_dim.56), calls=%async_computation.2 | async-start | bytes 229376 | tf_op jit(solution)/shard_map/all_to_all | solution.py:28
  66.6 0.1 multiply_sine_fusion
  66.8 0.1 fusion.51
  66.9 0.5 copy-done.7
  67.4 0.1 fusion.52
  67.5 0.5 copy-done.11
  68.1 0.3 exponential_select_fusion
  68.3 22.4 %all-to-all-done.2 = bf16[8,56,128]{2,1,0:T(8,128)(2,1)S(1)} async-done(((bf16[8,56,128]{2,1,0:T(8,128)(2,1)}), bf16[8,56,128]{2,1,0:T(8,128)(2,1)S(1)}, u32[]{:S(2)}, u32[]{:S(2)}) %all-to-all-start.2) | async-done | bytes 114720 | tf_op jit(solution)/shard_map/all_to_all | solution.py:28
  90.8 9.0 %all_to_all.57 = bf16[4,48,128]{2,1,0:T(8,128)(2,1)S(1)} all-to-all(bf16[4,48,128]{2,1,0:T(8,128)(2,1)S(1)} %broadcast_in_dim.59), channel_id=1, replica_groups={{0,8,16,24},{32,40,48,56},{64,72,80,88},{96,104,112,120},{128,136,144,1..., dimensions={0} | all-to-all | bytes 98304 | tf_op jit(solution)/shard_map/all_to_all | solution.py:28
  99.8 0.1 convert_multiply_fusion.2
  100.1 0.3 fusion.6
  100.4 0.2 copy.108
  100.7 0.3 copy.109
  101.1 0.5 copy-done.1
  101.6 0.2 fusion.3
  101.8 0.2 fusion.50
  102.0 0.1 subtract_convert_fusion
  102.1 7.0 %all_to_all.58 = bf16[4,48,128]{2,1,0:T(8,128)(2,1)S(1)} all-to-all(bf16[4,48,128]{2,1,0:T(8,128)(2,1)S(1)} %maximum_maximum_fusion), channel_id=1, replica_groups={{0,8,16,24},{32,40,48,56},{64,72,80,88},{96,104,112,120},{128,136,144,1..., dimensions={0} | all-to-all | bytes 98304 | tf_op jit(solution)/shard_map/all_to_all | solution.py:28
  109.1 27.7 %all_to_all.59 = bf16[8,48,128]{2,1,0:T(8,128)(2,1)S(1)} all-to-all(bf16[8,48,128]{2,1,0:T(8,128)(2,1)S(1)} %broadcast_in_dim.60), channel_id=1, replica_groups={{0,32,64,96,128,160,192,224},{8,40,72,104,136,168,200,232},{16,48,80,11..., dimensions={0} | all-to-all | bytes 196608 | tf_op jit(solution)/shard_map/all_to_all | solution.py:28
  136.8 8.5 %all_to_all.60 = bf16[4,48,128]{2,1,0:T(8,128)(2,1)S(1)} all-to-all(bf16[4,48,128]{2,1,0:T(8,128)(2,1)S(1)} %broadcast_in_dim.61), channel_id=1, replica_groups={{0,8,16,24},{32,40,48,56},{64,72,80,88},{96,104,112,120},{128,136,144,1..., dimensions={0} | all-to-all | bytes 98304 | tf_op jit(solution)/shard_map/all_to_all | solution.py:28
  145.3 0.1 fusion.47
  145.5 0.1 copy.114
  145.6 0.1 copy.97
  145.7 0.1 mul.262
  145.9 0.1 copy.95
  145.9 0.1 sub.83
  146.1 0.7 copy-done.15
  146.7 0.2 convolution_convert_fusion.4
  146.9 13.7 %all_to_all.61 = bf16[8,24,128]{2,1,0:T(8,128)(2,1)S(1)} all-to-all(bf16[8,24,128]{2,1,0:T(8,128)(2,1)S(1)} %broadcast_in_dim.62), channel_id=1, replica_groups=mesh['grp'=2,'kv'=32,'tp'=8] {'tp'}, dimensions={0} | all-to-all | bytes 98304 | tf_op jit(solution)/shard_map/all_to_all | solution.py:28
  160.7 0.1 copy.113
  160.8 0.5 copy-done.10
  161.3 0.2 convolution_convert_fusion.1
  161.5 0.1 fusion.49
  161.6 0.1 copy.99
  161.7 0.6 copy-done.2
  162.3 0.2 convolution_convert_fusion
  162.5 0.1 fusion.48
  162.7 0.1 concatenate.62
  162.8 0.1 concatenate.61
  162.9 0.1 concatenate.60
  163.0 0.1 concatenate.59
  163.1 7.9 %all_to_all.62 = bf16[4,24,768]{2,1,0:T(8,128)(2,1)S(1)} all-to-all(bf16[4,24,768]{2,1,0:T(8,128)(2,1)S(1)} %pad_maximum_fusion), channel_id=1, replica_groups={{0,8,16,24},{32,40,48,56},{64,72,80,88},{96,104,112,120},{128,136,144,1..., dimensions={0} | all-to-all | bytes 294912 | tf_op jit(solution)/shard_map/all_to_all | solution.py:28
  171.0 31.9 %all-gather = bf16[192,768]{1,0:T(8,128)(2,1)S(1)} all-gather(bf16[24,768]{1,0:T(8,128)(2,1)S(1)} %reduce_sum.152), channel_id=2, replica_groups={{0,32,64,96,128,160,192,224},{8,40,72,104,136,168,200,232},{16,48,80,11..., dimensions={0}, use_global_device_ids=true | all-gather | bytes 331776 | tf_op jit(solution)/shard_map/all_gather | solution.py:221
  203.0 0.2 fusion.33
  203.2 0.1 fusion.19
  203.3 7.1 %all_to_all.63 = bf16[4,24,384]{2,1,0:T(8,128)(2,1)S(1)} all-to-all(bf16[4,24,384]{2,1,0:T(8,128)(2,1)S(1)} %broadcast_in_dim.64), channel_id=1, replica_groups={{0,8,16,24},{32,40,48,56},{64,72,80,88},{96,104,112,120},{128,136,144,1..., dimensions={0} | all-to-all | bytes 147456 | tf_op jit(solution)/shard_map/all_to_all | solution.py:28
  210.4 0.1 concatenate.63
  210.5 0.2 convolution_convert_fusion.5
  210.7 0.1 reshape.160
  210.8 0.1 copy.103
  210.9 0.1 reshape.175
  211.0 15.5 %all_to_all.64 = bf16[8,2,192]{2,1,0:T(2,128)(2,1)S(1)} all-to-all(bf16[8,2,192]{2,1,0:T(2,128)(2,1)S(1)} %reshape.175), channel_id=1, replica_groups=mesh['grp'=2,'kv'=32,'tp'=8] {'tp'}, dimensions={0} | all-to-all | bytes 12288 | tf_op jit(solution)/shard_map/all_to_all | solution.py:28
  226.5 0.1 reshape.176
  226.7 0.7 copy.105
  (88 shorter events, 1.3 us)
Async XLA Ops:
  0.0 160.8 %copy-start = (bf16[128,1408]{1,0:T(8,128)(2,1)S(1)}, bf16[128,1408]{1,0:T(8,128)(2,1)}, u32[]{:S(2)}) copy-start(bf16[128,1408]{1,0:T(8,128)(2,1)} %param.30) | copy-start | bytes 1081348
  0.0 0.7 copy-start.8
  49.3 0.9 copy-start.4
  49.5 0.7 copy-start.12
  49.5 0.9 copy-start.5
  58.3 8.1 %copy-start.9 = (s32[24]{0:T(128)S(1)}, s32[24]{0:T(128)}, u32[]{:S(2)}) copy-start(s32[24]{0:T(128)} %param.18) | copy-start | bytes 292
  58.3 8.3 %copy-start.13 = (f32[128]{0:T(128)S(1)}, f32[128]{0:T(128)}, u32[]{:S(2)}) copy-start(f32[128]{0:T(128)} %constant.57) | copy-start | bytes 1540
  58.3 8.5 %copy-start.6 = (bf16[128,512]{1,0:T(8,128)(2,1)S(1)}, bf16[128,512]{1,0:T(8,128)(2,1)}, u32[]{:S(2)}) copy-start(bf16[128,512]{1,0:T(8,128)(2,1)} %param.22) | copy-start | bytes 393220
  58.3 32.4 %all-to-all-start.2 = ((bf16[8,56,128]{2,1,0:T(8,128)(2,1)}), bf16[8,56,128]{2,1,0:T(8,128)(2,1)S(1)}, u32[]{:S(2)}, u32[]{:S(2)}) async-start(bf16[8,56,128]{2,1,0:T(8,128)(2,1)} %broadcast_in_dim.56), calls=%async_computation.2 | async-start | bytes 229376 | tf_op jit(solution)/shard_map/all_to_all | solution.py:28
  66.5 0.9 copy-start.7
  67.4 0.7 copy-start.11
  68.3 31.8 %copy-start.14 = (bf16[24,32,512]{2,1,0:T(8,128)(2,1)S(1)}, bf16[24,32,512]{2,1,0:T(8,128)(2,1)}, u32[]{:S(2)}) copy-start(bf16[24,32,512]{2,1,0:T(8,128)(2,1)} %param.25) | copy-start | bytes 2359300
  100.4 1.2 copy-start.1
  145.8 0.9 copy-start.15
  146.0 0.7 copy-start.16
  160.7 0.7 copy-start.10
  161.3 1.0 copy-start.2
  203.0 7.6 %copy-start.3 = (bf16[1408,128]{1,0:T(8,128)(2,1)S(1)}, bf16[1408,128]{1,0:T(8,128)(2,1)}, u32[]{:S(2)}) copy-start(bf16[1408,128]{1,0:T(8,128)(2,1)} %param.32) | copy-start | bytes 1081348

commit v5 on v4

--- a/solution.py
+++ b/solution.py
@@ -61,7 +61,8 @@
     if extra is not None:
         tail = jnp.broadcast_to(hi_lo_rows(extra), (NEAR, 8, LANES))
         blocks = jnp.concatenate([blocks, tail], axis=1)
-    got = wide_sum(exchange(blocks.astype(jnp.bfloat16), "kv", groups_near()))
+    blocks, inputs = lax.optimization_barrier((blocks.astype(jnp.bfloat16), inputs))
+    got = wide_sum(exchange(blocks, "kv", groups_near()))
     if extra is not None:
         vector = got[2 * rows] + got[2 * rows + 1]
         got = jnp.concatenate([got[: 2 * rows], hi_lo_rows(vector[: extra.shape[0]])], axis=0)
@@ -152,13 +153,24 @@
     kv_at = lax.axis_index("kv")
     own_at = (lax.axis_index("tp") * own_width).astype(jnp.uint32)
     tokens, kv_at, own_at = lax.optimization_barrier((tokens, kv_at, own_at))
-    gathered = spread(tokens, "tp", tp)
-    x = jnp.moveaxis(gathered, 0, 1).reshape(rows, tp * own_width).astype(jnp.float32)
-    own_squares = jnp.sum(x * x, axis=1)
-    scaled = (x * attn_gain).astype(jnp.bfloat16)
+    own_gain = lax.dynamic_slice(attn_gain, (own_at,), (own_width,))
+    own_scaled = (tokens.astype(jnp.float32) * own_gain[None, :]).astype(jnp.bfloat16)
+    gathered = spread(jnp.stack([tokens, own_scaled]), "tp", tp)
+    x, scaled = (
+        jnp.moveaxis(gathered[:, i], 0, 1).reshape(rows, tp * own_width) for i in (0, 1)
+    )
+    own_squares = jnp.sum(x.astype(jnp.float32) * x.astype(jnp.float32), axis=1)
     dot = lambda a, w: jnp.dot(a, w, preferred_element_type=jnp.float32)
 
-    def ahead(scaled, lengths, log_decay, w_value, w_gate, kv_at):
+    quarter = w_ffn_gate.shape[1] // NEAR
+    padded = -(-(quarter + 1) // LANES) * LANES
+
+    def with_gain(gain, w):
+        return (gain[:, None] * w.astype(jnp.float32)).astype(jnp.bfloat16)
+
+    def ahead(
+        x, scaled, lengths, log_decay, w_value, w_gate, kv_at, gn_gain, w_out, ffn_gain, w_fg, w_fu
+    ):
         half = DK // 2
         inverse = (ROPE_BASE ** (-np.arange(half) / half)).astype(np.float32)
         angles = lengths.astype(jnp.float32)[:, None] * inverse[None, :]
@@ -168,6 +180,10 @@
             decay_factors(lengths, log_decay, key_cache.shape[1], kv_at),
             dot(scaled, w_value),
             dot(scaled, w_gate),
+            x.astype(jnp.float32),
+            with_gain(gn_gain, w_out),
+            with_gain(ffn_gain, w_fg),
+            with_gain(ffn_gain, w_fu),
         )
 
     q_raw, k_raw, factor, made = reduce_pair(
@@ -175,9 +191,22 @@
         dot(scaled, w_key),
         own_squares,
         ahead,
-        (scaled, lengths, log_decay, w_value, w_gate, kv_at),
-    )
-    cosine, sine, decays, part_value, part_gate = made
+        (
+            x,
+            scaled,
+            lengths,
+            log_decay,
+            w_value,
+            w_gate,
+            kv_at,
+            gn_gain,
+            w_out,
+            ffn_gain,
+            w_ffn_gate,
+            w_ffn_up,
+        ),
+    )
+    cosine, sine, decays, part_value, part_gate, x, out_gained, gate_gained, up_gained = made
     factor = factor[:, None]
     queries = rotate(q_raw * factor, cosine, sine) * DK ** (-0.5)
     keys = rotate(k_raw * factor, cosine, sine)
@@ -199,19 +228,16 @@
     center = jnp.mean(totals, axis=-1, keepdims=True)
     spread_ = jnp.mean(totals * totals, axis=-1, keepdims=True) - center * center
     normed = ((totals - center) * lax.rsqrt(spread_ + GN_EPS)).reshape(rows, heads_here * DK)
-    gated = (jax.nn.silu(gates) * (normed * gn_gain)).astype(jnp.bfloat16)
-    mixed = dot(gated, w_out).astype(jnp.bfloat16)
+    gated = (jax.nn.silu(gates) * normed).astype(jnp.bfloat16)
+    mixed = dot(gated, out_gained).astype(jnp.bfloat16)
     mixed = wide_sum(spread(mixed, "tp", tp))
     resid = (x + mixed).astype(jnp.bfloat16)
     resid_wide = resid.astype(jnp.float32)
     mid_squares = jnp.sum(resid_wide * resid_wide, axis=1)
-    scaled_mid = (resid_wide * ffn_gain).astype(jnp.bfloat16)
     own_resid = lax.dynamic_slice(resid_wide, (jnp.uint32(0), own_at), (rows, own_width))
-    quarter = w_ffn_gate.shape[1] // NEAR
-    padded = -(-(quarter + 1) // LANES) * LANES
     blocks = near_columns(
-        dot(scaled_mid, w_ffn_gate).astype(jnp.bfloat16),
-        dot(scaled_mid, w_ffn_up).astype(jnp.bfloat16),
+        dot(resid, gate_gained).astype(jnp.bfloat16),
+        dot(resid, up_gained).astype(jnp.bfloat16),
         mid_squares,
         padded,
     )

time: 228 us -> 227 us (level)
  transfers between devices with their start and end apart: 1 -> 1, of which waited for: 1 -> 1; matrix products, arithmetic and copies ran while one was open for 0% -> 1% of each run, Pallas kernels for 0% -> 0%
where the time goes in v5:
time: 227 us; the launch traced here: 226 us
  blocking collectives  184 us (81%)
  waiting for transfers between devices  21.4 us (9%)
  starting transfers between devices  8.15 us (4%)
  local copies, waits for them, and re-layouts  7.95 us (4%)
  other arithmetic  2.29 us (1%)
    all_to_all x10, blocking collectives, exchange(): lax.all_to_all(blocks, axis, split_axis=0, concat_axis=0, tiled=True, axi...  152 us
    all_gather x1, blocking collectives, local(): lax.all_gather(got.astype(jnp.bfloat16), 'kv', axis_index_groups=groups_f...  32.2 us
    all_to_all x1, waiting for transfers between devices, exchange(): lax.all_to_all(blocks, axis, split_axis=0, concat_axis=0, tiled=True, axi...  21.4 us
    all_to_all x1, starting transfers between devices, exchange(): lax.all_to_all(blocks, axis, split_axis=0, concat_axis=0, tiled=True, axi...  8.15 us
  transfers between devices with their start and end apart: 1, of which 1 were waited for; matrix products, arithmetic and copies ran while one was open for 1% of the time, Pallas kernels for 0%

profile of v5, /device:TPU:33, one launch (start us, length us, event | category | flops | bytes accessed | tf_op | source)
XLA Modules:
  0.0 225.9 jit_solution(8326627571076525501)
XLA Ops:
  0.0 0.7 copy-done.16
  0.9 0.1 reshape.176
  1.0 48.5 %all_to_all.55 = bf16[8,2,384]{2,1,0:T(2,128)(2,1)S(1)} all-to-all(bf16[8,2,384]{2,1,0:T(2,128)(2,1)S(1)} %reshape.176), channel_id=1, replica_groups=mesh['grp'=2,'kv'=32,'tp'=8] {'tp'}, dimensions={0} | all-to-all | bytes 24576 | tf_op jit(solution)/shard_map/all_to_all | solution.py:28
  49.5 0.1 reshape.177
  49.7 0.7 copy-done.4
  50.4 0.2 convolution_convert_fusion.2
  50.6 0.2 convolution_convert_fusion.3
  50.9 7.0 %all_to_all.56 = bf16[4,56,128]{2,1,0:T(8,128)(2,1)S(1)} all-to-all(bf16[4,56,128]{2,1,0:T(8,128)(2,1)S(1)} %pad_maximum_fusion.1), channel_id=1, replica_groups={{0,8,16,24},{32,40,48,56},{64,72,80,88},{96,104,112,120},{128,136,144,1..., dimensions={0} | all-to-all | bytes 114688 | tf_op jit(solution)/shard_map/all_to_all | solution.py:28
  58.0 0.7 broadcast_in_dim.32
  58.7 8.1 %all-to-all-start.2 = ((bf16[8,56,128]{2,1,0:T(8,128)(2,1)}), bf16[8,56,128]{2,1,0:T(8,128)(2,1)S(1)}, u32[]{:S(2)}, u32[]{:S(2)}) async-start(bf16[8,56,128]{2,1,0:T(8,128)(2,1)} %broadcast_in_dim.32), calls=%async_computation.2 | async-start | bytes 229376 | tf_op jit(solution)/shard_map/all_to_all | solution.py:28
  66.9 0.2 fusion.50
  67.1 0.6 copy-done.8
  67.7 0.2 fusion.51
  67.9 0.5 copy-done.14
  68.4 0.1 multiply_sine_fusion
  68.5 0.1 copy-done.6
  68.6 0.1 multiply_convert_fusion.2
  68.9 0.3 exponential_select_fusion
  69.2 0.2 copy-done.2
  69.4 0.1 copy-done.3
  69.5 0.2 multiply_convert_fusion
  69.7 21.4 %all-to-all-done.2 = bf16[8,56,128]{2,1,0:T(8,128)(2,1)S(1)} async-done(((bf16[8,56,128]{2,1,0:T(8,128)(2,1)}), bf16[8,56,128]{2,1,0:T(8,128)(2,1)S(1)}, u32[]{:S(2)}, u32[]{:S(2)}) %all-to-all-start.2) | async-done | bytes 114720 | tf_op jit(solution)/shard_map/all_to_all | solution.py:28
  91.1 9.0 %all_to_all.57 = bf16[4,48,128]{2,1,0:T(8,128)(2,1)S(1)} all-to-all(bf16[4,48,128]{2,1,0:T(8,128)(2,1)S(1)} %broadcast_in_dim.60), channel_id=1, replica_groups={{0,8,16,24},{32,40,48,56},{64,72,80,88},{96,104,112,120},{128,136,144,1..., dimensions={0} | all-to-all | bytes 98304 | tf_op jit(solution)/shard_map/all_to_all | solution.py:28
  100.2 0.1 convert_multiply_fusion.2
  100.4 0.3 fusion.6
  100.7 0.2 copy.98
  101.0 0.3 copy.99
  101.4 0.5 copy-done.1
  101.9 0.2 fusion.3
  102.1 0.2 fusion.49
  102.3 0.1 subtract_convert_fusion
  102.5 7.0 %all_to_all.58 = bf16[4,48,128]{2,1,0:T(8,128)(2,1)S(1)} all-to-all(bf16[4,48,128]{2,1,0:T(8,128)(2,1)S(1)} %maximum_maximum_fusion), channel_id=1, replica_groups={{0,8,16,24},{32,40,48,56},{64,72,80,88},{96,104,112,120},{128,136,144,1..., dimensions={0} | all-to-all | bytes 98304 | tf_op jit(solution)/shard_map/all_to_all | solution.py:28
  109.5 27.7 %all_to_all.59 = bf16[8,48,128]{2,1,0:T(8,128)(2,1)S(1)} all-to-all(bf16[8,48,128]{2,1,0:T(8,128)(2,1)S(1)} %broadcast_in_dim.61), channel_id=1, replica_groups={{0,32,64,96,128,160,192,224},{8,40,72,104,136,168,200,232},{16,48,80,11..., dimensions={0} | all-to-all | bytes 196608 | tf_op jit(solution)/shard_map/all_to_all | solution.py:28
  137.1 8.5 %all_to_all.60 = bf16[4,48,128]{2,1,0:T(8,128)(2,1)S(1)} all-to-all(bf16[4,48,128]{2,1,0:T(8,128)(2,1)S(1)} %broadcast_in_dim.62), channel_id=1, replica_groups={{0,8,16,24},{32,40,48,56},{64,72,80,88},{96,104,112,120},{128,136,144,1..., dimensions={0} | all-to-all | bytes 98304 | tf_op jit(solution)/shard_map/all_to_all | solution.py:28
  145.7 0.1 fusion.44
  146.0 0.1 copy.88
  146.1 0.1 mul.272
  146.2 0.1 copy.86
  146.3 0.1 sub.83
  146.4 0.2 convolution_convert_fusion.4
  146.5 13.7 %all_to_all.61 = bf16[8,24,128]{2,1,0:T(8,128)(2,1)S(1)} all-to-all(bf16[8,24,128]{2,1,0:T(8,128)(2,1)S(1)} %broadcast_in_dim.63), channel_id=1, replica_groups=mesh['grp'=2,'kv'=32,'tp'=8] {'tp'}, dimensions={0} | all-to-all | bytes 98304 | tf_op jit(solution)/shard_map/all_to_all | solution.py:28
  160.3 0.1 multiply_reduce_fusion.2
  160.4 0.2 convolution_convert_fusion.1
  160.6 0.1 fusion.47
  160.7 0.1 copy.89
  160.8 0.2 convolution_convert_fusion
  161.0 0.1 fusion.46
  161.1 0.1 concatenate.62
  161.2 0.1 concatenate.61
  161.3 0.1 concatenate.60
  161.4 0.1 concatenate.59
  161.6 7.9 %all_to_all.62 = bf16[4,24,768]{2,1,0:T(8,128)(2,1)S(1)} all-to-all(bf16[4,24,768]{2,1,0:T(8,128)(2,1)S(1)} %pad_maximum_fusion), channel_id=1, replica_groups={{0,8,16,24},{32,40,48,56},{64,72,80,88},{96,104,112,120},{128,136,144,1..., dimensions={0} | all-to-all | bytes 294912 | tf_op jit(solution)/shard_map/all_to_all | solution.py:28
  169.5 32.2 %all-gather = bf16[192,768]{1,0:T(8,128)(2,1)S(1)} all-gather(bf16[24,768]{1,0:T(8,128)(2,1)S(1)} %reduce_sum.149), channel_id=2, replica_groups={{0,32,64,96,128,160,192,224},{8,40,72,104,136,168,200,232},{16,48,80,11..., dimensions={0}, use_global_device_ids=true | all-gather | bytes 331776 | tf_op jit(solution)/shard_map/all_gather | solution.py:247
  201.7 0.2 fusion.30
  201.9 0.1 fusion.17
  202.0 7.0 %all_to_all.63 = bf16[4,24,384]{2,1,0:T(8,128)(2,1)S(1)} all-to-all(bf16[4,24,384]{2,1,0:T(8,128)(2,1)S(1)} %broadcast_in_dim.65), channel_id=1, replica_groups={{0,8,16,24},{32,40,48,56},{64,72,80,88},{96,104,112,120},{128,136,144,1..., dimensions={0} | all-to-all | bytes 147456 | tf_op jit(solution)/shard_map/all_to_all | solution.py:28
  209.1 0.1 concatenate.63
  209.2 0.2 convolution_convert_fusion.5
  209.4 0.1 reshape.164
  209.5 0.1 copy.93
  209.6 0.1 reshape.178
  209.7 15.3 %all_to_all.64 = bf16[8,2,192]{2,1,0:T(2,128)(2,1)S(1)} all-to-all(bf16[8,2,192]{2,1,0:T(2,128)(2,1)S(1)} %reshape.178), channel_id=1, replica_groups=mesh['grp'=2,'kv'=32,'tp'=8] {'tp'}, dimensions={0} | all-to-all | bytes 12288 | tf_op jit(solution)/shard_map/all_to_all | solution.py:28
  225.0 0.1 reshape.179
  225.2 0.7 copy.95
  (92 shorter events, 1.5 us)
Async XLA Ops:
  0.0 209.2 %copy-start = (bf16[1408,128]{1,0:T(8,128)(2,1)S(1)}, bf16[1408,128]{1,0:T(8,128)(2,1)}, u32[]{:S(2)}) copy-start(bf16[1408,128]{1,0:T(8,128)(2,1)} %param.32) | copy-start | bytes 1081348
  0.0 0.8 copy-start.9
  0.0 0.7 copy-start.16
  49.5 0.9 copy-start.4
  49.7 0.9 copy-start.5
  58.7 8.2 %copy-start.11 = (s32[24]{0:T(128)S(1)}, s32[24]{0:T(128)}, u32[]{:S(2)}) copy-start(s32[24]{0:T(128)} %param.18) | copy-start | bytes 292
  58.7 8.3 %copy-start.7 = (bf16[128,512]{1,0:T(8,128)(2,1)S(1)}, bf16[128,512]{1,0:T(8,128)(2,1)}, u32[]{:S(2)}) copy-start(bf16[128,512]{1,0:T(8,128)(2,1)} %param.22) | copy-start | bytes 393220
  58.7 32.4 %all-to-all-start.2 = ((bf16[8,56,128]{2,1,0:T(8,128)(2,1)}), bf16[8,56,128]{2,1,0:T(8,128)(2,1)S(1)}, u32[]{:S(2)}, u32[]{:S(2)}) async-start(bf16[8,56,128]{2,1,0:T(8,128)(2,1)} %broadcast_in_dim.32), calls=%async_computation.2 | async-start | bytes 229376 | tf_op jit(solution)/shard_map/all_to_all | solution.py:28
  66.8 0.9 copy-start.8
  67.7 0.7 copy-start.14
  67.7 0.9 copy-start.6
  67.7 0.9 copy-start.10
  67.7 1.1 copy-start.12
  67.7 1.4 copy-start.13
  68.4 1.0 copy-start.2
  68.4 1.1 copy-start.3
  69.7 30.7 %copy-start.15 = (bf16[24,32,512]{2,1,0:T(8,128)(2,1)S(1)}, bf16[24,32,512]{2,1,0:T(8,128)(2,1)}, u32[]{:S(2)}) copy-start(bf16[24,32,512]{2,1,0:T(8,128)(2,1)} %param.25) | copy-start | bytes 2359300
  100.7 1.2 copy-start.1

commit v6 on v5

--- a/solution.py
+++ b/solution.py
@@ -56,8 +56,8 @@
 
 def reduce_pair(first, second, extra=None, work=None, inputs=()):
     far = lax.axis_size("kv") // NEAR
-    rows = first.shape[0]
-    blocks = jnp.concatenate([near_blocks(first), near_blocks(second)], axis=1)
+    rows = first.shape[1]
+    blocks = jnp.concatenate([first, second], axis=1)
     if extra is not None:
         tail = jnp.broadcast_to(hi_lo_rows(extra), (NEAR, 8, LANES))
         blocks = jnp.concatenate([blocks, tail], axis=1)
@@ -80,10 +80,9 @@
         vector = lax.rsqrt(vector / D + RMS_EPS)
         mine, vector = lax.optimization_barrier((mine, vector))
     whole = spread(mine, "kv", NEAR, groups_near())
-    outs = (
-        side(whole[:, :rows]).astype(jnp.float32),
-        side(whole[:, rows:]).astype(jnp.float32),
-    )
+    if extra is not None:
+        whole, vector = lax.optimization_barrier((whole, vector))
+    outs = (whole[:, :rows].astype(jnp.float32), whole[:, rows:].astype(jnp.float32))
     if extra is None:
         return outs
     return (*outs, vector, done)
@@ -101,31 +100,29 @@
     return jnp.stack(blocks)
 
 
-def rotate(vectors, cosine, sine):
-    half = DK // 2
+def rotate(halves, cosine, sine):
     outs = []
-    for h in range(vectors.shape[1] // DK):
-        a = vectors[:, h * DK : h * DK + half]
-        b = vectors[:, h * DK + half : (h + 1) * DK]
+    for h in range(0, halves.shape[0], 2):
+        a, b = halves[h], halves[h + 1]
         outs += [a * cosine - b * sine, a * sine + b * cosine]
-    return jnp.concatenate(outs, axis=1)
+    return outs
 
 
 def decay_factors(lengths, log_decay, span, at):
     slots = at * span + jnp.arange(span, dtype=jnp.int32)
     gaps = (lengths[:, None] - slots[None, :]).astype(jnp.float32)
     live = gaps > 0.0
-    decays = jnp.exp(log_decay[None, None, :] * jnp.maximum(gaps, 0.0)[:, :, None])
-    return jnp.where(live[:, :, None], decays, 0.0)
+    decays = jnp.exp(log_decay[None, :, None] * jnp.maximum(gaps, 0.0)[:, None, :])
+    return jnp.where(live[:, None, :], decays, 0.0)
 
 
 def cache_partial(query_low, decays, key_cache, value_cache, heads_here):
-    batch_rows, span = decays.shape[:2]
+    batch_rows, _, span = decays.shape
     keys_here = key_cache.reshape(batch_rows, span, heads_here, DK)
     values_here = value_cache.reshape(batch_rows, span, heads_here, DK)
-    scores = jnp.einsum("bphd,bhd->bph", keys_here, query_low, preferred_element_type=jnp.float32)
+    scores = jnp.einsum("bphd,bhd->bhp", keys_here, query_low, preferred_element_type=jnp.float32)
     mixing = (scores * decays).astype(jnp.bfloat16)
-    return jnp.einsum("bph,bphd->bhd", mixing, values_here, preferred_element_type=jnp.float32)
+    return jnp.einsum("bhp,bphd->bhd", mixing, values_here, preferred_element_type=jnp.float32)
 
 
 def local(
@@ -187,8 +184,8 @@
         )
 
     q_raw, k_raw, factor, made = reduce_pair(
-        dot(scaled, w_query),
-        dot(scaled, w_key),
+        near_blocks(dot(scaled, w_query)),
+        near_blocks(dot(scaled, w_key)),
         own_squares,
         ahead,
         (
@@ -208,40 +205,47 @@
     )
     cosine, sine, decays, part_value, part_gate, x, out_gained, gate_gained, up_gained = made
     factor = factor[:, None]
-    queries = rotate(q_raw * factor, cosine, sine) * DK ** (-0.5)
+    queries = [a * DK ** (-0.5) for a in rotate(q_raw * factor, cosine, sine)]
     keys = rotate(k_raw * factor, cosine, sine)
-    by_head = (rows, heads_here, DK)
-    own_dot = jnp.sum((queries * keys).reshape(by_head), axis=-1, keepdims=True)
     cached = cache_partial(
-        queries.astype(jnp.bfloat16).reshape(by_head),
+        jnp.concatenate(queries, axis=1).astype(jnp.bfloat16).reshape(rows, heads_here, DK),
         decays,
         key_cache,
         value_cache,
         heads_here,
     )
-    part_value = part_value * factor
-    totals = cached + own_dot * part_value.reshape(by_head)
-    totals = totals - jnp.mean(totals, axis=-1, keepdims=True)
-    part_gate = part_gate * factor
-    totals, gates = reduce_pair(totals.reshape(rows, heads_here * DK), part_gate)
-    totals = totals.reshape(by_head)
-    center = jnp.mean(totals, axis=-1, keepdims=True)
-    spread_ = jnp.mean(totals * totals, axis=-1, keepdims=True) - center * center
-    normed = ((totals - center) * lax.rsqrt(spread_ + GN_EPS)).reshape(rows, heads_here * DK)
-    gated = (jax.nn.silu(gates) * normed).astype(jnp.bfloat16)
+    totals = []
+    for h in range(heads_here):
+        two = (2 * h, 2 * h + 1)
+        own_dot = sum(jnp.sum(queries[n] * keys[n], axis=1, keepdims=True) for n in two)
+        value = part_value[:, h * DK : (h + 1) * DK] * factor
+        total = cached[:, h] + own_dot * value
+        total = total - jnp.mean(total, axis=1, keepdims=True)
+        totals += [total[:, :LANES], total[:, LANES:]]
+    totals, gates = reduce_pair(jnp.stack(totals), near_blocks(part_gate * factor))
+    gated = []
+    for h in range(heads_here):
+        a, b = totals[2 * h], totals[2 * h + 1]
+        center = (jnp.sum(a, axis=1, keepdims=True) + jnp.sum(b, axis=1, keepdims=True)) / DK
+        a, b = a - center, b - center
+        spread_ = jnp.sum(a * a, axis=1, keepdims=True) + jnp.sum(b * b, axis=1, keepdims=True)
+        scale = lax.rsqrt(spread_ / DK + GN_EPS)
+        gated += [
+            (jax.nn.silu(gates[2 * h]) * (a * scale)).astype(jnp.bfloat16),
+            (jax.nn.silu(gates[2 * h + 1]) * (b * scale)).astype(jnp.bfloat16),
+        ]
+    gated = jnp.concatenate(gated, axis=1)
     mixed = dot(gated, out_gained).astype(jnp.bfloat16)
     mixed = wide_sum(spread(mixed, "tp", tp))
     resid = (x + mixed).astype(jnp.bfloat16)
     resid_wide = resid.astype(jnp.float32)
     mid_squares = jnp.sum(resid_wide * resid_wide, axis=1)
-    own_resid = lax.dynamic_slice(resid_wide, (jnp.uint32(0), own_at), (rows, own_width))
     blocks = near_columns(
         dot(resid, gate_gained).astype(jnp.bfloat16),
         dot(resid, up_gained).astype(jnp.bfloat16),
         mid_squares,
         padded,
     )
-    blocks, own_resid = lax.optimization_barrier((blocks, own_resid))
     got = wide_sum(exchange(blocks, "kv", groups_near()))
     got = wide_sum(
         lax.all_gather(got.astype(jnp.bfloat16), "kv", axis_index_groups=groups_far())
@@ -251,10 +255,10 @@
     whole = spread(hidden.astype(jnp.bfloat16), "kv", NEAR, groups_near())
     hidden = side(whole[:, :, :quarter])
     down_part = dot(hidden, w_ffn_down).astype(jnp.bfloat16)
-    down = wide_sum(
-        exchange(jnp.moveaxis(down_part.reshape(rows, tp, own_width), 1, 0), "tp")
-    )
-    return (own_resid + down).astype(jnp.bfloat16)
+    down = wide_sum(spread(down_part, "tp", tp))
+    return lax.dynamic_slice(
+        (resid_wide + down).astype(jnp.bfloat16), (jnp.uint32(0), own_at), (rows, own_width)
+    )
 
 
 def solution(mesh):

time: 227 us -> 226 us (level)
  transfers between devices with their start and end apart: 1 -> 1, of which waited for: 1 -> 1; matrix products, arithmetic and copies ran while one was open for 1% -> 0% of each run, Pallas kernels for 0% -> 0%
where the time goes in v6:
time: 226 us
  blocking collectives  184 us (81%)
  waiting for transfers between devices  22.7 us (10%)
  starting transfers between devices  8.16 us (4%)
  local copies, waits for them, and re-layouts  5.77 us (3%)
  other arithmetic  2.71 us (1%)
    all_to_all x10, blocking collectives, exchange(): lax.all_to_all(blocks, axis, split_axis=0, concat_axis=0, tiled=True, axi...  152 us
    all_gather x1, blocking collectives, local(): lax.all_gather(got.astype(jnp.bfloat16), 'kv', axis_index_groups=groups_f...  32.2 us
    all_to_all x1, waiting for transfers between devices, exchange(): lax.all_to_all(blocks, axis, split_axis=0, concat_axis=0, tiled=True, axi...  22.7 us
    all_to_all x1, starting transfers between devices, exchange(): lax.all_to_all(blocks, axis, split_axis=0, concat_axis=0, tiled=True, axi...  8.16 us
  transfers between devices with their start and end apart: 1, of which 1 were waited for; matrix products, arithmetic and copies ran while one was open for 0% of the time, Pallas kernels for 0%

profile of v6, /device:TPU:33, one launch (start us, length us, event | category | flops | bytes accessed | tf_op | source)
XLA Modules:
  0.0 225.6 jit_solution(359501634404407373)
XLA Ops:
  0.0 0.7 copy-done.16
  0.7 0.1 dynamic_slice.6
  0.8 0.1 fusion.23
  0.9 0.1 reshape.177
  1.0 48.5 %all_to_all.55 = bf16[8,2,384]{2,1,0:T(2,128)(2,1)S(1)} all-to-all(bf16[8,2,384]{2,1,0:T(2,128)(2,1)S(1)} %reshape.177), channel_id=1, replica_groups=mesh['grp'=2,'kv'=32,'tp'=8] {'tp'}, dimensions={0} | all-to-all | bytes 24576 | tf_op jit(solution)/shard_map/all_to_all | solution.py:28
  49.5 0.1 reshape.178
  49.7 0.7 copy-done.3
  50.4 0.2 convolution_convert_fusion.2
  50.6 0.0 copy-done.4
  50.6 0.2 convolution_convert_fusion.3
  50.8 0.1 copy.46
  50.9 7.0 %all_to_all.56 = bf16[4,56,128]{2,1,0:T(8,128)(2,1)S(1)} all-to-all(bf16[4,56,128]{2,1,0:T(8,128)(2,1)S(1)} %pad_maximum_fusion.1), channel_id=1, replica_groups={{0,8,16,24},{32,40,48,56},{64,72,80,88},{96,104,112,120},{128,136,144,1..., dimensions={0} | all-to-all | bytes 114688 | tf_op jit(solution)/shard_map/all_to_all | solution.py:28
  58.0 0.6 copy-done.10
  58.7 0.1 convert_compare_fusion
  58.7 0.1 convert_maximum_fusion
  58.8 0.7 broadcast_in_dim.34
  59.5 8.2 %all-to-all-start.2 = ((bf16[8,56,128]{2,1,0:T(8,128)(2,1)}), bf16[8,56,128]{2,1,0:T(8,128)(2,1)S(1)}, u32[]{:S(2)}, u32[]{:S(2)}) async-start(bf16[8,56,128]{2,1,0:T(8,128)(2,1)} %broadcast_in_dim.34), calls=%async_computation.2 | async-start | bytes 229376 | tf_op jit(solution)/shard_map/all_to_all | solution.py:28
  67.7 0.2 fusion.45
  67.9 0.2 fusion.46
  68.0 0.1 exponential_select_fusion
  68.1 0.1 multiply_sine_fusion
  68.3 0.1 multiply_convert_fusion.2
  68.4 0.2 copy-done.1
  68.6 0.1 copy-done.2
  68.8 0.3 copy-done.12
  69.0 0.2 multiply_convert_fusion
  69.2 22.7 %all-to-all-done.2 = bf16[8,56,128]{2,1,0:T(8,128)(2,1)S(1)} async-done(((bf16[8,56,128]{2,1,0:T(8,128)(2,1)}), bf16[8,56,128]{2,1,0:T(8,128)(2,1)S(1)}, u32[]{:S(2)}, u32[]{:S(2)}) %all-to-all-start.2) | async-done | bytes 114720 | tf_op jit(solution)/shard_map/all_to_all | solution.py:28
  92.0 9.0 %all_to_all.57 = bf16[4,48,128]{2,1,0:T(8,128)(2,1)S(1)} all-to-all(bf16[4,48,128]{2,1,0:T(8,128)(2,1)S(1)} %broadcast_in_dim.37), channel_id=1, replica_groups={{0,8,16,24},{32,40,48,56},{64,72,80,88},{96,104,112,120},{128,136,144,1..., dimensions={0} | all-to-all | bytes 98304 | tf_op jit(solution)/shard_map/all_to_all | solution.py:28
  101.0 0.1 multiply_convert_fusion.3
  101.1 0.1 convert_multiply_fusion.1
  101.2 0.2 multiply_reduce_fusion.8
  101.4 0.3 fusion.3
  101.7 0.4 copy-done.15
  102.1 0.2 fusion
  102.4 0.2 fusion.39
  102.6 0.1 subtract_convert_fusion.1
  102.7 7.0 %all_to_all.58 = bf16[4,48,128]{2,1,0:T(8,128)(2,1)S(1)} all-to-all(bf16[4,48,128]{2,1,0:T(8,128)(2,1)S(1)} %maximum_maximum_fusion), channel_id=1, replica_groups={{0,8,16,24},{32,40,48,56},{64,72,80,88},{96,104,112,120},{128,136,144,1..., dimensions={0} | all-to-all | bytes 98304 | tf_op jit(solution)/shard_map/all_to_all | solution.py:28
  109.7 27.7 %all_to_all.59 = bf16[8,48,128]{2,1,0:T(8,128)(2,1)S(1)} all-to-all(bf16[8,48,128]{2,1,0:T(8,128)(2,1)S(1)} %broadcast_in_dim.38), channel_id=1, replica_groups={{0,32,64,96,128,160,192,224},{8,40,72,104,136,168,200,232},{16,48,80,11..., dimensions={0} | all-to-all | bytes 196608 | tf_op jit(solution)/shard_map/all_to_all | solution.py:28
  137.4 8.5 %all_to_all.60 = bf16[4,48,128]{2,1,0:T(8,128)(2,1)S(1)} all-to-all(bf16[4,48,128]{2,1,0:T(8,128)(2,1)S(1)} %broadcast_in_dim.39), channel_id=1, replica_groups={{0,8,16,24},{32,40,48,56},{64,72,80,88},{96,104,112,120},{128,136,144,1..., dimensions={0} | all-to-all | bytes 98304 | tf_op jit(solution)/shard_map/all_to_all | solution.py:28
  145.9 0.1 slice_reduce_fusion.2
  146.1 0.2 multiply_reduce_fusion.4
  146.3 0.1 multiply_convert_fusion.8
  146.4 0.1 convolution_convert_fusion.4
  146.6 13.7 %all_to_all.61 = bf16[8,24,128]{2,1,0:T(8,128)(2,1)S(1)} all-to-all(bf16[8,24,128]{2,1,0:T(8,128)(2,1)S(1)} %broadcast_in_dim.40), channel_id=1, replica_groups=mesh['grp'=2,'kv'=32,'tp'=8] {'tp'}, dimensions={0} | all-to-all | bytes 98304 | tf_op jit(solution)/shard_map/all_to_all | solution.py:28
  160.3 0.1 multiply_reduce_fusion.1
  160.4 0.2 convolution_convert_fusion.1
  160.6 0.1 fusion.43
  160.7 0.1 copy.35
  160.8 0.2 convolution_convert_fusion
  161.0 0.1 fusion.42
  161.1 0.1 concatenate.47
  161.2 0.1 concatenate.46
  161.3 0.1 concatenate.45
  161.4 0.1 concatenate.44
  161.5 7.9 %all_to_all.62 = bf16[4,24,768]{2,1,0:T(8,128)(2,1)S(1)} all-to-all(bf16[4,24,768]{2,1,0:T(8,128)(2,1)S(1)} %pad_maximum_fusion), channel_id=1, replica_groups={{0,8,16,24},{32,40,48,56},{64,72,80,88},{96,104,112,120},{128,136,144,1..., dimensions={0} | all-to-all | bytes 294912 | tf_op jit(solution)/shard_map/all_to_all | solution.py:28
  169.4 32.2 %all-gather = bf16[192,768]{1,0:T(8,128)(2,1)S(1)} all-gather(bf16[24,768]{1,0:T(8,128)(2,1)S(1)} %reduce_sum.249), channel_id=2, replica_groups={{0,32,64,96,128,160,192,224},{8,40,72,104,136,168,200,232},{16,48,80,11..., dimensions={0}, use_global_device_ids=true | all-gather | bytes 331776 | tf_op jit(solution)/shard_map/all_gather | solution.py:251
  201.6 0.2 fusion.22
  201.8 0.1 fusion.7
  202.0 7.0 %all_to_all.63 = bf16[4,24,384]{2,1,0:T(8,128)(2,1)S(1)} all-to-all(bf16[4,24,384]{2,1,0:T(8,128)(2,1)S(1)} %broadcast_in_dim.42), channel_id=1, replica_groups={{0,8,16,24},{32,40,48,56},{64,72,80,88},{96,104,112,120},{128,136,144,1..., dimensions={0} | all-to-all | bytes 147456 | tf_op jit(solution)/shard_map/all_to_all | solution.py:28
  209.0 0.1 concatenate.48
  209.1 0.2 convolution_convert_fusion.5
  209.3 15.5 %all_to_all.64 = bf16[8,24,128]{2,1,0:T(8,128)(2,1)S(1)} all-to-all(bf16[8,24,128]{2,1,0:T(8,128)(2,1)S(1)} %broadcast_in_dim.43), channel_id=1, replica_groups=mesh['grp'=2,'kv'=32,'tp'=8] {'tp'}, dimensions={0} | all-to-all | bytes 98304 | tf_op jit(solution)/shard_map/all_to_all | solution.py:28
  224.8 0.1 fusion.19
  224.9 0.7 copy.39
  (82 shorter events, 0.7 us)
Async XLA Ops:
  0.0 209.1 %copy-start = (bf16[1408,128]{1,0:T(8,128)(2,1)S(1)}, bf16[1408,128]{1,0:T(8,128)(2,1)}, u32[]{:S(2)}) copy-start(bf16[1408,128]{1,0:T(8,128)(2,1)} %param.32) | copy-start | bytes 1081348
  0.0 0.8 copy-start.8
  0.0 0.7 copy-start.16
  49.5 0.9 copy-start.3
  49.7 0.9 copy-start.4
  58.0 0.7 copy-start.10
  58.8 8.8 %copy-start.6 = (bf16[128,512]{1,0:T(8,128)(2,1)S(1)}, bf16[128,512]{1,0:T(8,128)(2,1)}, u32[]{:S(2)}) copy-start(bf16[128,512]{1,0:T(8,128)(2,1)} %param.22) | copy-start | bytes 393220
  59.5 8.4 %copy-start.7 = (bf16[128,512]{1,0:T(8,128)(2,1)S(1)}, bf16[128,512]{1,0:T(8,128)(2,1)}, u32[]{:S(2)}) copy-start(bf16[128,512]{1,0:T(8,128)(2,1)} %param.23) | copy-start | bytes 393220
  59.5 8.6 %copy-start.11 = (f32[2]{0:T(128)S(1)}, f32[2]{0:T(128)}, u32[]{:S(2)}) copy-start(f32[2]{0:T(128)} %param.24) | copy-start | bytes 28
  59.5 8.7 %copy-start.13 = (f32[128]{0:T(128)S(1)}, f32[128]{0:T(128)}, u32[]{:S(2)}) copy-start(f32[128]{0:T(128)} %constant.63) | copy-start | bytes 1540
  59.5 8.8 %copy-start.5 = (bf16[512,128]{1,0:T(8,128)(2,1)S(1)}, bf16[512,128]{1,0:T(8,128)(2,1)}, u32[]{:S(2)}) copy-start(bf16[512,128]{1,0:T(8,128)(2,1)} %param.28) | copy-start | bytes 393220
  59.5 8.8 %copy-start.9 = (f32[512]{0:T(512)S(1)}, f32[512]{0:T(512)}, u32[]{:S(2)}) copy-start(f32[512]{0:T(512)} %param.27) | copy-start | bytes 6148
  59.5 32.4 %all-to-all-start.2 = ((bf16[8,56,128]{2,1,0:T(8,128)(2,1)}), bf16[8,56,128]{2,1,0:T(8,128)(2,1)S(1)}, u32[]{:S(2)}, u32[]{:S(2)}) async-start(bf16[8,56,128]{2,1,0:T(8,128)(2,1)} %broadcast_in_dim.34), calls=%async_computation.2 | async-start | bytes 229376 | tf_op jit(solution)/shard_map/all_to_all | solution.py:28
  67.7 1.0 copy-start.1
  67.7 1.1 copy-start.2
  68.3 0.7 copy-start.12
  69.2 32.2 %copy-start.14 = (bf16[24,32,512]{2,1,0:T(8,128)(2,1)S(1)}, bf16[24,32,512]{2,1,0:T(8,128)(2,1)}, u32[]{:S(2)}) copy-start(bf16[24,32,512]{2,1,0:T(8,128)(2,1)} %param.25) | copy-start | bytes 2359300
  101.0 1.1 copy-start.15

commit v7 on v6

--- a/solution.py
+++ b/solution.py
@@ -100,6 +100,10 @@
     return jnp.stack(blocks)
 
 
+def with_gain(gain, w):
+    return (gain[:, None] * w.astype(jnp.float32)).astype(jnp.bfloat16)
+
+
 def rotate(halves, cosine, sine):
     outs = []
     for h in range(0, halves.shape[0], 2):
@@ -108,9 +112,12 @@
     return outs
 
 
-def decay_factors(lengths, log_decay, span, at):
+def gaps_to(lengths, span, at):
     slots = at * span + jnp.arange(span, dtype=jnp.int32)
-    gaps = (lengths[:, None] - slots[None, :]).astype(jnp.float32)
+    return (lengths[:, None] - slots[None, :]).astype(jnp.float32)
+
+
+def decay_factors(gaps, log_decay):
     live = gaps > 0.0
     decays = jnp.exp(log_decay[None, :, None] * jnp.maximum(gaps, 0.0)[:, None, :])
     return jnp.where(live[:, None, :], decays, 0.0)
@@ -150,52 +157,63 @@
     kv_at = lax.axis_index("kv")
     own_at = (lax.axis_index("tp") * own_width).astype(jnp.uint32)
     tokens, kv_at, own_at = lax.optimization_barrier((tokens, kv_at, own_at))
-    own_gain = lax.dynamic_slice(attn_gain, (own_at,), (own_width,))
-    own_scaled = (tokens.astype(jnp.float32) * own_gain[None, :]).astype(jnp.bfloat16)
-    gathered = spread(jnp.stack([tokens, own_scaled]), "tp", tp)
-    x, scaled = (
-        jnp.moveaxis(gathered[:, i], 0, 1).reshape(rows, tp * own_width) for i in (0, 1)
-    )
+    gathered = spread(tokens, "tp", tp)
+    w_joint = with_gain(attn_gain, jnp.concatenate([w_query, w_key], axis=1))
+    gaps = gaps_to(lengths, key_cache.shape[1], kv_at)
+    positions = lengths.astype(jnp.float32)
+    gathered, w_joint, gaps, positions = lax.optimization_barrier(
+        (gathered, w_joint, gaps, positions)
+    )
+    x = jnp.moveaxis(gathered, 0, 1).reshape(rows, tp * own_width)
     own_squares = jnp.sum(x.astype(jnp.float32) * x.astype(jnp.float32), axis=1)
     dot = lambda a, w: jnp.dot(a, w, preferred_element_type=jnp.float32)
 
     quarter = w_ffn_gate.shape[1] // NEAR
     padded = -(-(quarter + 1) // LANES) * LANES
 
-    def with_gain(gain, w):
-        return (gain[:, None] * w.astype(jnp.float32)).astype(jnp.bfloat16)
-
     def ahead(
-        x, scaled, lengths, log_decay, w_value, w_gate, kv_at, gn_gain, w_out, ffn_gain, w_fg, w_fu
+        x,
+        positions,
+        gaps,
+        log_decay,
+        attn_gain,
+        w_value,
+        w_gate,
+        gn_gain,
+        w_out,
+        ffn_gain,
+        w_fg,
+        w_fu,
     ):
         half = DK // 2
         inverse = (ROPE_BASE ** (-np.arange(half) / half)).astype(np.float32)
-        angles = lengths.astype(jnp.float32)[:, None] * inverse[None, :]
+        angles = positions[:, None] * inverse[None, :]
         return (
             jnp.cos(angles),
             jnp.sin(angles),
-            decay_factors(lengths, log_decay, key_cache.shape[1], kv_at),
-            dot(scaled, w_value),
-            dot(scaled, w_gate),
+            decay_factors(gaps, log_decay),
+            dot(x, with_gain(attn_gain, w_value)),
+            dot(x, with_gain(attn_gain, w_gate)),
             x.astype(jnp.float32),
             with_gain(gn_gain, w_out),
             with_gain(ffn_gain, w_fg),
             with_gain(ffn_gain, w_fu),
         )
 
+    joint = near_blocks(dot(x, w_joint))
     q_raw, k_raw, factor, made = reduce_pair(
-        near_blocks(dot(scaled, w_query)),
-        near_blocks(dot(scaled, w_key)),
+        joint[:NEAR],
+        joint[NEAR:],
         own_squares,
         ahead,
         (
             x,
-            scaled,
-            lengths,
+            positions,
+            gaps,
             log_decay,
+            attn_gain,
             w_value,
             w_gate,
-            kv_at,
             gn_gain,
             w_out,
             ffn_gain,

time: 226 us -> 225 us (level)
  blocking collectives: 184 us -> 135 us
  starting transfers between devices: 8.16 us -> 52.1 us
  waiting for transfers between devices: 22.7 us -> 25.4 us
    all_to_all x10 -> x9, blocking collectives: 152 us -> 103 us  [exchange(): lax.all_to_all(blocks, axis, split_axis=0, concat_axis=0, tiled=True, axi...]
    all_to_all x1 -> x2, starting transfers between devices: 8.16 us -> 52.1 us  [exchange(): lax.all_to_all(blocks, axis, split_axis=0, concat_axis=0, tiled=True, axi...]
    all_to_all x1 -> x2, waiting for transfers between devices: 22.7 us -> 25.4 us  [exchange(): lax.all_to_all(blocks, axis, split_axis=0, concat_axis=0, tiled=True, axi...]
  transfers between devices with their start and end apart: 1 -> 2, of which waited for: 1 -> 2; matrix products, arithmetic and copies ran while one was open for 0% -> 1% of each run, Pallas kernels for 0% -> 0%
where the time goes in v7:
time: 225 us; the launch traced here: 224 us
  blocking collectives  135 us (60%)
  starting transfers between devices  52.1 us (23%)
  waiting for transfers between devices  25.4 us (11%)
  local copies, waits for them, and re-layouts  5.54 us (2%)
  other arithmetic  3.62 us (2%)
    all_to_all x9, blocking collectives, exchange(): lax.all_to_all(blocks, axis, split_axis=0, concat_axis=0, tiled=True, axi...  103 us
    all_to_all x2, starting transfers between devices, exchange(): lax.all_to_all(blocks, axis, split_axis=0, concat_axis=0, tiled=True, axi...  52.1 us
    all_gather x1, blocking collectives, local(): lax.all_gather(got.astype(jnp.bfloat16), 'kv', axis_index_groups=groups_f...  32.1 us
    all_to_all x2, waiting for transfers between devices, exchange(): lax.all_to_all(blocks, axis, split_axis=0, concat_axis=0, tiled=True, axi...  25.4 us
  transfers between devices with their start and end apart: 2, of which 2 were waited for; matrix products, arithmetic and copies ran while one was open for 1% of the time, Pallas kernels for 0%

profile of v7, /device:TPU:33, one launch (start us, length us, event | category | flops | bytes accessed | tf_op | source)
XLA Modules:
  0.0 224.4 jit_solution(8955151617861072389)
XLA Ops:
  0.0 0.7 copy-done.7
  0.7 0.7 reshape.131
  1.5 44.7 %all-to-all-start = ((bf16[8,2,192]{2,1,0:T(2,128)(2,1)}), bf16[8,2,192]{2,1,0:T(2,128)(2,1)S(1)}, u32[]{:S(2)}, u32[]{:S(2)}) async-start(bf16[8,2,192]{2,1,0:T(2,128)(2,1)} %reshape.131), calls=%async_computation | async-start | bytes 16384 | tf_op jit(solution)/shard_map/all_to_all | solution.py:28
  46.1 0.6 copy-done.6
  46.8 1.1 multiply_convert_fusion.2
  47.9 0.1 subtract_convert_fusion.2
  48.0 2.9 %all-to-all-done = bf16[8,2,192]{2,1,0:T(2,128)(2,1)S(1)} async-done(((bf16[8,2,192]{2,1,0:T(2,128)(2,1)}), bf16[8,2,192]{2,1,0:T(2,128)(2,1)S(1)}, u32[]{:S(2)}, u32[]{:S(2)}) %all-to-all-start) | async-done | bytes 6176 | tf_op jit(solution)/shard_map/all_to_all | solution.py:28
  50.8 0.1 reshape.132
  51.0 0.1 copy.47
  51.0 0.2 convolution_convert_fusion.2
  51.3 7.0 %all_to_all.55 = bf16[4,56,128]{2,1,0:T(8,128)(2,1)S(1)} all-to-all(bf16[4,56,128]{2,1,0:T(8,128)(2,1)S(1)} %pad_maximum_fusion.1), channel_id=1, replica_groups={{0,8,16,24},{32,40,48,56},{64,72,80,88},{96,104,112,120},{128,136,144,1..., dimensions={0} | all-to-all | bytes 114688 | tf_op jit(solution)/shard_map/all_to_all | solution.py:28
  58.4 0.0 copy-start.5
  58.4 0.0 copy-start.4
  58.4 0.7 broadcast_in_dim.34
  59.1 7.5 %all-to-all-start.2 = ((bf16[8,56,128]{2,1,0:T(8,128)(2,1)}), bf16[8,56,128]{2,1,0:T(8,128)(2,1)S(1)}, u32[]{:S(2)}, u32[]{:S(2)}) async-start(bf16[8,56,128]{2,1,0:T(8,128)(2,1)} %broadcast_in_dim.34), calls=%async_computation.2 | async-start | bytes 229376 | tf_op jit(solution)/shard_map/all_to_all | solution.py:28
  66.6 0.0 copy-start.1
  66.6 0.2 fusion.6
  66.8 0.2 fusion.7
  67.0 0.1 exponential_select_fusion
  67.1 0.1 multiply_sine_fusion
  67.3 0.1 multiply_convert_fusion.3
  67.4 0.1 copy-done.1
  67.5 0.1 copy-done.2
  67.7 0.3 copy-done.10
  68.0 0.2 multiply_convert_fusion
  68.2 0.0 copy-start.13
  68.2 22.6 %all-to-all-done.2 = bf16[8,56,128]{2,1,0:T(8,128)(2,1)S(1)} async-done(((bf16[8,56,128]{2,1,0:T(8,128)(2,1)}), bf16[8,56,128]{2,1,0:T(8,128)(2,1)S(1)}, u32[]{:S(2)}, u32[]{:S(2)}) %all-to-all-start.2) | async-done | bytes 114720 | tf_op jit(solution)/shard_map/all_to_all | solution.py:28
  90.9 9.0 %all_to_all.56 = bf16[4,48,128]{2,1,0:T(8,128)(2,1)S(1)} all-to-all(bf16[4,48,128]{2,1,0:T(8,128)(2,1)S(1)} %broadcast_in_dim.37), channel_id=1, replica_groups={{0,8,16,24},{32,40,48,56},{64,72,80,88},{96,104,112,120},{128,136,144,1..., dimensions={0} | all-to-all | bytes 98304 | tf_op jit(solution)/shard_map/all_to_all | solution.py:28
  99.9 0.1 multiply_convert_fusion.8
  100.0 0.1 convert_multiply_fusion.1
  100.1 0.2 multiply_reduce_fusion.8
  100.3 0.3 fusion.3
  100.6 0.4 copy-done.14
  101.0 0.2 fusion
  101.3 0.2 fusion.42
  101.5 0.1 subtract_convert_fusion.1
  101.6 7.0 %all_to_all.57 = bf16[4,48,128]{2,1,0:T(8,128)(2,1)S(1)} all-to-all(bf16[4,48,128]{2,1,0:T(8,128)(2,1)S(1)} %maximum_maximum_fusion), channel_id=1, replica_groups={{0,8,16,24},{32,40,48,56},{64,72,80,88},{96,104,112,120},{128,136,144,1..., dimensions={0} | all-to-all | bytes 98304 | tf_op jit(solution)/shard_map/all_to_all | solution.py:28
  108.6 27.7 %all_to_all.58 = bf16[8,48,128]{2,1,0:T(8,128)(2,1)S(1)} all-to-all(bf16[8,48,128]{2,1,0:T(8,128)(2,1)S(1)} %broadcast_in_dim.38), channel_id=1, replica_groups={{0,32,64,96,128,160,192,224},{8,40,72,104,136,168,200,232},{16,48,80,11..., dimensions={0} | all-to-all | bytes 196608 | tf_op jit(solution)/shard_map/all_to_all | solution.py:28
  136.3 8.5 %all_to_all.59 = bf16[4,48,128]{2,1,0:T(8,128)(2,1)S(1)} all-to-all(bf16[4,48,128]{2,1,0:T(8,128)(2,1)S(1)} %broadcast_in_dim.39), channel_id=1, replica_groups={{0,8,16,24},{32,40,48,56},{64,72,80,88},{96,104,112,120},{128,136,144,1..., dimensions={0} | all-to-all | bytes 98304 | tf_op jit(solution)/shard_map/all_to_all | solution.py:28
  144.8 0.1 slice_reduce_fusion.2
  145.0 0.2 multiply_reduce_fusion.4
  145.2 0.1 multiply_convert_fusion.13
  145.3 0.1 convolution_convert_fusion.3
  145.4 13.7 %all_to_all.60 = bf16[8,24,128]{2,1,0:T(8,128)(2,1)S(1)} all-to-all(bf16[8,24,128]{2,1,0:T(8,128)(2,1)S(1)} %broadcast_in_dim.40), channel_id=1, replica_groups=mesh['grp'=2,'kv'=32,'tp'=8] {'tp'}, dimensions={0} | all-to-all | bytes 98304 | tf_op jit(solution)/shard_map/all_to_all | solution.py:28
  159.2 0.1 multiply_reduce_fusion.1
  159.3 0.2 convolution_convert_fusion.1
  159.5 0.1 fusion.46
  159.6 0.1 copy.36
  159.7 0.2 convolution_convert_fusion
  159.9 0.1 fusion.45
  160.0 0.1 concatenate.55
  160.1 0.1 concatenate.54
  160.2 0.1 concatenate.53
  160.3 0.1 concatenate.52
  160.4 7.9 %all_to_all.61 = bf16[4,24,768]{2,1,0:T(8,128)(2,1)S(1)} all-to-all(bf16[4,24,768]{2,1,0:T(8,128)(2,1)S(1)} %pad_maximum_fusion), channel_id=1, replica_groups={{0,8,16,24},{32,40,48,56},{64,72,80,88},{96,104,112,120},{128,136,144,1..., dimensions={0} | all-to-all | bytes 294912 | tf_op jit(solution)/shard_map/all_to_all | solution.py:28
  168.3 32.1 %all-gather = bf16[192,768]{1,0:T(8,128)(2,1)S(1)} all-gather(bf16[24,768]{1,0:T(8,128)(2,1)S(1)} %reduce_sum.249), channel_id=2, replica_groups={{0,32,64,96,128,160,192,224},{8,40,72,104,136,168,200,232},{16,48,80,11..., dimensions={0}, use_global_device_ids=true | all-gather | bytes 331776 | tf_op jit(solution)/shard_map/all_gather | solution.py:269
  200.5 0.2 fusion.26
  200.7 0.1 fusion.11
  200.8 7.0 %all_to_all.62 = bf16[4,24,384]{2,1,0:T(8,128)(2,1)S(1)} all-to-all(bf16[4,24,384]{2,1,0:T(8,128)(2,1)S(1)} %broadcast_in_dim.42), channel_id=1, replica_groups={{0,8,16,24},{32,40,48,56},{64,72,80,88},{96,104,112,120},{128,136,144,1..., dimensions={0} | all-to-all | bytes 147456 | tf_op jit(solution)/shard_map/all_to_all | solution.py:28
  207.8 0.1 concatenate.56
  208.0 0.2 convolution_convert_fusion.4
  208.2 15.5 %all_to_all.63 = bf16[8,24,128]{2,1,0:T(8,128)(2,1)S(1)} all-to-all(bf16[8,24,128]{2,1,0:T(8,128)(2,1)S(1)} %broadcast_in_dim.43), channel_id=1, replica_groups=mesh['grp'=2,'kv'=32,'tp'=8] {'tp'}, dimensions={0} | all-to-all | bytes 98304 | tf_op jit(solution)/shard_map/all_to_all | solution.py:28
  223.7 0.1 fusion.23
  223.7 0.7 copy.40
  (75 shorter events, 0.6 us)
Async XLA Ops:
  0.0 208.0 %copy-start = (bf16[1408,128]{1,0:T(8,128)(2,1)S(1)}, bf16[1408,128]{1,0:T(8,128)(2,1)}, u32[]{:S(2)}) copy-start(bf16[1408,128]{1,0:T(8,128)(2,1)} %param.32) | copy-start | bytes 1081348
  0.0 0.7 copy-start.7
  1.5 49.4 %all-to-all-start = ((bf16[8,2,192]{2,1,0:T(2,128)(2,1)}), bf16[8,2,192]{2,1,0:T(2,128)(2,1)S(1)}, u32[]{:S(2)}, u32[]{:S(2)}) async-start(bf16[8,2,192]{2,1,0:T(2,128)(2,1)} %reshape.131), calls=%async_computation | async-start | bytes 16384 | tf_op jit(solution)/shard_map/all_to_all | solution.py:28
  46.1 0.7 copy-start.6
  46.8 1.1 copy-start.12
  58.4 8.9 %copy-start.5 = (bf16[512,128]{1,0:T(8,128)(2,1)S(1)}, bf16[512,128]{1,0:T(8,128)(2,1)}, u32[]{:S(2)}) copy-start(bf16[512,128]{1,0:T(8,128)(2,1)} %param.28) | copy-start | bytes 393220
  58.4 8.4 %copy-start.4 = (bf16[128,512]{1,0:T(8,128)(2,1)S(1)}, bf16[128,512]{1,0:T(8,128)(2,1)}, u32[]{:S(2)}) copy-start(bf16[128,512]{1,0:T(8,128)(2,1)} %param.23) | copy-start | bytes 393220
  59.1 7.5 %copy-start.3 = (bf16[128,512]{1,0:T(8,128)(2,1)S(1)}, bf16[128,512]{1,0:T(8,128)(2,1)}, u32[]{:S(2)}) copy-start(bf16[128,512]{1,0:T(8,128)(2,1)} %param.22) | copy-start | bytes 393220
  59.1 7.9 %copy-start.9 = (f32[2]{0:T(128)S(1)}, f32[2]{0:T(128)}, u32[]{:S(2)}) copy-start(f32[2]{0:T(128)} %param.24) | copy-start | bytes 28
  59.1 8.0 %copy-start.11 = (f32[128]{0:T(128)S(1)}, f32[128]{0:T(128)}, u32[]{:S(2)}) copy-start(f32[128]{0:T(128)} %constant.63) | copy-start | bytes 1540
  59.1 8.2 %copy-start.8 = (f32[512]{0:T(512)S(1)}, f32[512]{0:T(512)}, u32[]{:S(2)}) copy-start(f32[512]{0:T(512)} %param.27) | copy-start | bytes 6148
  59.1 31.7 %all-to-all-start.2 = ((bf16[8,56,128]{2,1,0:T(8,128)(2,1)}), bf16[8,56,128]{2,1,0:T(8,128)(2,1)S(1)}, u32[]{:S(2)}, u32[]{:S(2)}) async-start(bf16[8,56,128]{2,1,0:T(8,128)(2,1)} %broadcast_in_dim.34), calls=%async_computation.2 | async-start | bytes 229376 | tf_op jit(solution)/shard_map/all_to_all | solution.py:28
  66.6 1.0 copy-start.1
  66.6 1.1 copy-start.2
  67.3 0.7 copy-start.10
  68.2 32.1 %copy-start.13 = (bf16[24,32,512]{2,1,0:T(8,128)(2,1)S(1)}, bf16[24,32,512]{2,1,0:T(8,128)(2,1)}, u32[]{:S(2)}) copy-start(bf16[24,32,512]{2,1,0:T(8,128)(2,1)} %param.25) | copy-start | bytes 2359300
  99.9 1.1 copy-start.14

commit v8 on v6

--- a/solution.py
+++ b/solution.py
@@ -54,26 +54,19 @@
     return jnp.concatenate([blocks[i] for i in range(blocks.shape[0])], axis=1)
 
 
-def reduce_pair(first, second, extra=None, work=None, inputs=()):
+def reduce_pair(first, second, extra=None, beside=()):
     far = lax.axis_size("kv") // NEAR
     rows = first.shape[1]
     blocks = jnp.concatenate([first, second], axis=1)
     if extra is not None:
         tail = jnp.broadcast_to(hi_lo_rows(extra), (NEAR, 8, LANES))
         blocks = jnp.concatenate([blocks, tail], axis=1)
-    blocks, inputs = lax.optimization_barrier((blocks.astype(jnp.bfloat16), inputs))
+    blocks, beside = lax.optimization_barrier((blocks.astype(jnp.bfloat16), beside))
     got = wide_sum(exchange(blocks, "kv", groups_near()))
     if extra is not None:
         vector = got[2 * rows] + got[2 * rows + 1]
         got = jnp.concatenate([got[: 2 * rows], hi_lo_rows(vector[: extra.shape[0]])], axis=0)
-    got = got.astype(jnp.bfloat16)
-    if work is not None:
-        got, inputs = lax.optimization_barrier((got, inputs))
-        done = work(*inputs)
-    got = spread(got, "kv", far, groups_far())
-    if work is not None:
-        got, done = lax.optimization_barrier((got, done))
-    got = wide_sum(got)
+    got = wide_sum(spread(got.astype(jnp.bfloat16), "kv", far, groups_far()))
     mine = got[: 2 * rows].astype(jnp.bfloat16)
     if extra is not None:
         vector = (got[2 * rows] + got[2 * rows + 1])[: extra.shape[0]]
@@ -85,7 +78,7 @@
     outs = (whole[:, :rows].astype(jnp.float32), whole[:, rows:].astype(jnp.float32))
     if extra is None:
         return outs
-    return (*outs, vector, done)
+    return (*outs, vector, beside)
 
 
 def near_columns(gate, up, stat, padded):
@@ -100,6 +93,10 @@
     return jnp.stack(blocks)
 
 
+def with_gain(gain, w):
+    return (gain[:, None] * w.astype(jnp.float32)).astype(jnp.bfloat16)
+
+
 def rotate(halves, cosine, sine):
     outs = []
     for h in range(0, halves.shape[0], 2):
@@ -108,9 +105,12 @@
     return outs
 
 
-def decay_factors(lengths, log_decay, span, at):
+def gaps_to(lengths, span, at):
     slots = at * span + jnp.arange(span, dtype=jnp.int32)
-    gaps = (lengths[:, None] - slots[None, :]).astype(jnp.float32)
+    return lengths[:, None] - slots.astype(jnp.float32)[None, :]
+
+
+def decay_factors(gaps, log_decay):
     live = gaps > 0.0
     decays = jnp.exp(log_decay[None, :, None] * jnp.maximum(gaps, 0.0)[:, None, :])
     return jnp.where(live[:, None, :], decays, 0.0)
@@ -150,60 +150,38 @@
     kv_at = lax.axis_index("kv")
     own_at = (lax.axis_index("tp") * own_width).astype(jnp.uint32)
     tokens, kv_at, own_at = lax.optimization_barrier((tokens, kv_at, own_at))
-    own_gain = lax.dynamic_slice(attn_gain, (own_at,), (own_width,))
-    own_scaled = (tokens.astype(jnp.float32) * own_gain[None, :]).astype(jnp.bfloat16)
-    gathered = spread(jnp.stack([tokens, own_scaled]), "tp", tp)
-    x, scaled = (
-        jnp.moveaxis(gathered[:, i], 0, 1).reshape(rows, tp * own_width) for i in (0, 1)
-    )
-    own_squares = jnp.sum(x.astype(jnp.float32) * x.astype(jnp.float32), axis=1)
+    gathered = spread(tokens, "tp", tp)
     dot = lambda a, w: jnp.dot(a, w, preferred_element_type=jnp.float32)
-
+    half = DK // 2
+    inverse = (ROPE_BASE ** (-np.arange(half) / half)).astype(np.float32)
+    positions = lax.optimization_barrier(lengths.astype(jnp.float32))
+    angles = positions[:, None] * inverse[None, :]
+    gaps = lax.optimization_barrier(gaps_to(positions, key_cache.shape[1], kv_at))
+    made = (
+        with_gain(attn_gain, jnp.concatenate([w_query, w_key, w_value, w_gate], axis=1)),
+        with_gain(gn_gain, w_out),
+        with_gain(ffn_gain, w_ffn_gate),
+        with_gain(ffn_gain, w_ffn_up),
+        jnp.cos(angles),
+        jnp.sin(angles),
+        decay_factors(gaps, log_decay),
+    )
+    gathered, made = lax.optimization_barrier((gathered, made))
+    w_joint, out_gained, gate_gained, up_gained, cosine, sine, decays = made
+    x = jnp.moveaxis(gathered, 0, 1).reshape(rows, tp * own_width)
+    wide_x = x.astype(jnp.float32)
+    own_squares = jnp.sum(wide_x * wide_x, axis=1)
     quarter = w_ffn_gate.shape[1] // NEAR
     padded = -(-(quarter + 1) // LANES) * LANES
-
-    def with_gain(gain, w):
-        return (gain[:, None] * w.astype(jnp.float32)).astype(jnp.bfloat16)
-
-    def ahead(
-        x, scaled, lengths, log_decay, w_value, w_gate, kv_at, gn_gain, w_out, ffn_gain, w_fg, w_fu
-    ):
-        half = DK // 2
-        inverse = (ROPE_BASE ** (-np.arange(half) / half)).astype(np.float32)
-        angles = lengths.astype(jnp.float32)[:, None] * inverse[None, :]
-        return (
-            jnp.cos(angles),
-            jnp.sin(angles),
-            decay_factors(lengths, log_decay, key_cache.shape[1], kv_at),
-            dot(scaled, w_value),
-            dot(scaled, w_gate),
-            x.astype(jnp.float32),
-            with_gain(gn_gain, w_out),
-            with_gain(ffn_gain, w_fg),
-            with_gain(ffn_gain, w_fu),
-        )
-
-    q_raw, k_raw, factor, made = reduce_pair(
-        near_blocks(dot(scaled, w_query)),
-        near_blocks(dot(scaled, w_key)),
+    joint = dot(x, w_joint)
+    width = heads_here * DK
+    pairs = near_blocks(joint[:, : 2 * width])
+    q_raw, k_raw, factor, (part_value, part_gate, x) = reduce_pair(
+        pairs[:NEAR],
+        pairs[NEAR:],
         own_squares,
-        ahead,
-        (
-            x,
-            scaled,
-            lengths,
-            log_decay,
-            w_value,
-            w_gate,
-            kv_at,
-            gn_gain,
-            w_out,
-            ffn_gain,
-            w_ffn_gate,
-            w_ffn_up,
-        ),
-    )
-    cosine, sine, decays, part_value, part_gate, x, out_gained, gate_gained, up_gained = made
+        (joint[:, 2 * width : 3 * width], joint[:, 3 * width :], wide_x),
+    )
     factor = factor[:, None]
     queries = [a * DK ** (-0.5) for a in rotate(q_raw * factor, cosine, sine)]
     keys = rotate(k_raw * factor, cosine, sine)

time: 226 us -> 225 us (level)
  starting transfers between devices: 8.16 us -> 44.7 us
  waiting for transfers between devices: 22.7 us -> 0.1 us
  blocking collectives: 184 us -> 168 us
  other arithmetic: 2.71 us -> 5.3 us
    all_to_all x1, starting transfers between devices: 8.16 us -> 44.7 us  [exchange(): lax.all_to_all(blocks, axis, split_axis=0, concat_axis=0, tiled=True, axi...]
    all_to_all x1, waiting for transfers between devices: 22.7 us -> 0.1 us  [exchange(): lax.all_to_all(blocks, axis, split_axis=0, concat_axis=0, tiled=True, axi...]
    all_to_all x10, blocking collectives: 152 us -> 137 us  [exchange(): lax.all_to_all(blocks, axis, split_axis=0, concat_axis=0, tiled=True, axi...]
  transfers between devices with their start and end apart: 1 -> 1, of which waited for: 1 -> 1; matrix products, arithmetic and copies ran while one was open for 0% -> 2% of each run, Pallas kernels for 0% -> 0%
where the time goes in v8:
time: 225 us
  blocking collectives  168 us (75%)
  starting transfers between devices  44.7 us (20%)
  other arithmetic  5.3 us (2%)
  local copies, waits for them, and re-layouts  4.32 us (2%)
    all_to_all x10, blocking collectives, exchange(): lax.all_to_all(blocks, axis, split_axis=0, concat_axis=0, tiled=True, axi...  137 us
    all_to_all x1, starting transfers between devices, exchange(): lax.all_to_all(blocks, axis, split_axis=0, concat_axis=0, tiled=True, axi...  44.7 us
    all_gather x1, blocking collectives, local(): lax.all_gather(got.astype(jnp.bfloat16), 'kv', axis_index_groups=groups_f...  31.7 us
  transfers between devices with their start and end apart: 1, of which 1 were waited for; matrix products, arithmetic and copies ran while one was open for 2% of the time, Pallas kernels for 0%

profile of v8, /device:TPU:33, one launch (start us, length us, event | category | flops | bytes accessed | tf_op | source)
XLA Modules:
  0.0 224.7 jit_solution(350860061294051130)
XLA Ops:
  0.0 0.0 copy-start
  0.0 0.8 broadcast_bitcast_fusion
  0.8 0.7 reshape.130
  1.5 44.7 %all-to-all-start = ((bf16[8,2,192]{2,1,0:T(2,128)(2,1)}), bf16[8,2,192]{2,1,0:T(2,128)(2,1)S(1)}, u32[]{:S(2)}, u32[]{:S(2)}) async-start(bf16[8,2,192]{2,1,0:T(2,128)(2,1)} %reshape.130), calls=%async_computation | async-start | bytes 16384 | tf_op jit(solution)/shard_map/all_to_all | solution.py:28
  46.2 0.7 convert_element_type.150
  46.8 0.1 broadcast_subtract_fusion
  46.9 0.0 copy-start.6
  46.9 1.0 multiply_convert_fusion.3
  48.0 0.0 copy-done.6
  48.0 0.0 copy-start.7
  48.0 0.1 exponential_select_fusion
  48.1 0.0 copy-done.1
  48.1 0.5 copy-done.7
  48.6 0.0 copy-start.8
  48.7 1.2 multiply_convert_fusion.1
  49.9 0.0 copy-done.2
  50.0 0.0 copy-start.9
  50.0 0.2 multiply_convert_fusion
  50.1 0.5 copy-done.9
  50.6 0.1 multiply_sine_fusion
  50.7 0.1 all-to-all-done
  50.8 0.1 reshape.131
  51.0 0.1 copy.47
  51.0 0.2 fusion.44
  51.3 0.0 copy-start.10
  51.4 7.1 %all_to_all.55 = bf16[4,56,128]{2,1,0:T(8,128)(2,1)S(1)} all-to-all(bf16[4,56,128]{2,1,0:T(8,128)(2,1)S(1)} %pad_maximum_fusion.1), channel_id=1, replica_groups={{0,8,16,24},{32,40,48,56},{64,72,80,88},{96,104,112,120},{128,136,144,1..., dimensions={0} | all-to-all | bytes 114688 | tf_op jit(solution)/shard_map/all_to_all | solution.py:28
  58.6 31.4 %all_to_all.56 = bf16[8,56,128]{2,1,0:T(8,128)(2,1)S(1)} all-to-all(bf16[8,56,128]{2,1,0:T(8,128)(2,1)S(1)} %broadcast_in_dim.36), channel_id=1, replica_groups={{0,32,64,96,128,160,192,224},{8,40,72,104,136,168,200,232},{16,48,80,11..., dimensions={0} | all-to-all | bytes 229376 | tf_op jit(solution)/shard_map/all_to_all | solution.py:28
  90.1 0.0 copy-start.11
  90.1 9.2 %all_to_all.57 = bf16[4,48,128]{2,1,0:T(8,128)(2,1)S(1)} all-to-all(bf16[4,48,128]{2,1,0:T(8,128)(2,1)S(1)} %broadcast_in_dim.37), channel_id=1, replica_groups={{0,8,16,24},{32,40,48,56},{64,72,80,88},{96,104,112,120},{128,136,144,1..., dimensions={0} | all-to-all | bytes 98304 | tf_op jit(solution)/shard_map/all_to_all | solution.py:28
  99.2 0.1 convert_multiply_fusion.1
  99.3 0.2 multiply_reduce_fusion.8
  99.5 0.3 fusion.3
  99.9 0.2 fusion
  100.1 0.2 fusion.38
  100.3 0.1 subtract_convert_fusion.1
  100.4 0.1 multiply_convert_fusion.4
  100.5 7.0 %all_to_all.58 = bf16[4,48,128]{2,1,0:T(8,128)(2,1)S(1)} all-to-all(bf16[4,48,128]{2,1,0:T(8,128)(2,1)S(1)} %maximum_maximum_fusion), channel_id=1, replica_groups={{0,8,16,24},{32,40,48,56},{64,72,80,88},{96,104,112,120},{128,136,144,1..., dimensions={0} | all-to-all | bytes 98304 | tf_op jit(solution)/shard_map/all_to_all | solution.py:28
  107.5 27.7 %all_to_all.59 = bf16[8,48,128]{2,1,0:T(8,128)(2,1)S(1)} all-to-all(bf16[8,48,128]{2,1,0:T(8,128)(2,1)S(1)} %broadcast_in_dim.38), channel_id=1, replica_groups={{0,32,64,96,128,160,192,224},{8,40,72,104,136,168,200,232},{16,48,80,11..., dimensions={0} | all-to-all | bytes 196608 | tf_op jit(solution)/shard_map/all_to_all | solution.py:28
  135.2 8.5 %all_to_all.60 = bf16[4,48,128]{2,1,0:T(8,128)(2,1)S(1)} all-to-all(bf16[4,48,128]{2,1,0:T(8,128)(2,1)S(1)} %broadcast_in_dim.39), channel_id=1, replica_groups={{0,8,16,24},{32,40,48,56},{64,72,80,88},{96,104,112,120},{128,136,144,1..., dimensions={0} | all-to-all | bytes 98304 | tf_op jit(solution)/shard_map/all_to_all | solution.py:28
  143.7 0.1 slice_reduce_fusion.2
  143.9 0.2 multiply_reduce_fusion.4
  144.1 0.1 multiply_convert_fusion.9
  144.2 0.1 convolution_convert_fusion.2
  144.4 15.4 %all_to_all.61 = bf16[8,24,128]{2,1,0:T(8,128)(2,1)S(1)} all-to-all(bf16[8,24,128]{2,1,0:T(8,128)(2,1)S(1)} %broadcast_in_dim.40), channel_id=1, replica_groups=mesh['grp'=2,'kv'=32,'tp'=8] {'tp'}, dimensions={0} | all-to-all | bytes 98304 | tf_op jit(solution)/shard_map/all_to_all | solution.py:28
  159.8 0.1 multiply_reduce_fusion.1
  159.9 0.2 convolution_convert_fusion
  160.0 0.1 fusion.42
  160.1 0.2 convolution_convert_fusion.1
  160.3 0.1 fusion.43
  160.4 0.1 copy.36
  160.5 0.1 concatenate.52
  160.6 0.1 concatenate.53
  160.7 0.1 concatenate.54
  160.8 0.1 concatenate.55
  160.9 7.9 %all_to_all.62 = bf16[4,24,768]{2,1,0:T(8,128)(2,1)S(1)} all-to-all(bf16[4,24,768]{2,1,0:T(8,128)(2,1)S(1)} %pad_maximum_fusion), channel_id=1, replica_groups={{0,8,16,24},{32,40,48,56},{64,72,80,88},{96,104,112,120},{128,136,144,1..., dimensions={0} | all-to-all | bytes 294912 | tf_op jit(solution)/shard_map/all_to_all | solution.py:28
  168.9 31.7 %all-gather = bf16[192,768]{1,0:T(8,128)(2,1)S(1)} all-gather(bf16[24,768]{1,0:T(8,128)(2,1)S(1)} %reduce_sum.249), channel_id=2, replica_groups={{0,32,64,96,128,160,192,224},{8,40,72,104,136,168,200,232},{16,48,80,11..., dimensions={0}, use_global_device_ids=true | all-gather | bytes 331776 | tf_op jit(solution)/shard_map/all_gather | solution.py:229
  200.6 0.2 fusion.22
  200.8 0.1 fusion.7
  200.9 7.0 %all_to_all.63 = bf16[4,24,384]{2,1,0:T(8,128)(2,1)S(1)} all-to-all(bf16[4,24,384]{2,1,0:T(8,128)(2,1)S(1)} %broadcast_in_dim.42), channel_id=1, replica_groups={{0,8,16,24},{32,40,48,56},{64,72,80,88},{96,104,112,120},{128,136,144,1..., dimensions={0} | all-to-all | bytes 147456 | tf_op jit(solution)/shard_map/all_to_all | solution.py:28
  207.9 0.1 concatenate.56
  208.0 0.2 convolution_convert_fusion.3
  208.2 15.7 %all_to_all.64 = bf16[8,24,128]{2,1,0:T(8,128)(2,1)S(1)} all-to-all(bf16[8,24,128]{2,1,0:T(8,128)(2,1)S(1)} %broadcast_in_dim.43), channel_id=1, replica_groups=mesh['grp'=2,'kv'=32,'tp'=8] {'tp'}, dimensions={0} | all-to-all | bytes 98304 | tf_op jit(solution)/shard_map/all_to_all | solution.py:28
  223.9 0.1 fusion.19
  224.0 0.7 copy.40
  (67 shorter events, 0.6 us)
Async XLA Ops:
  0.0 208.0 %copy-start = (bf16[1408,128]{1,0:T(8,128)(2,1)S(1)}, bf16[1408,128]{1,0:T(8,128)(2,1)}, u32[]{:S(2)}) copy-start(bf16[1408,128]{1,0:T(8,128)(2,1)} %param.32) | copy-start | bytes 1081348
  0.0 48.1 %copy-start.1 = (bf16[128,1408]{1,0:T(8,128)(2,1)S(1)}, bf16[128,1408]{1,0:T(8,128)(2,1)}, u32[]{:S(2)}) copy-start(bf16[128,1408]{1,0:T(8,128)(2,1)} %param.31) | copy-start | bytes 1081348
  1.5 49.4 %all-to-all-start = ((bf16[8,2,192]{2,1,0:T(2,128)(2,1)}), bf16[8,2,192]{2,1,0:T(2,128)(2,1)S(1)}, u32[]{:S(2)}, u32[]{:S(2)}) async-start(bf16[8,2,192]{2,1,0:T(2,128)(2,1)} %reshape.130), calls=%async_computation | async-start | bytes 16384 | tf_op jit(solution)/shard_map/all_to_all | solution.py:28
  46.9 1.1 copy-start.6
  48.0 0.7 copy-start.7
  48.6 1.3 copy-start.2
  48.6 1.3 copy-start.3
  48.6 1.3 copy-start.4
  48.6 1.3 copy-start.5
  48.6 1.3 copy-start.8
  50.0 0.7 copy-start.9
  51.3 48.2 %copy-start.10 = (bf16[24,32,512]{2,1,0:T(8,128)(2,1)S(1)}, bf16[24,32,512]{2,1,0:T(8,128)(2,1)}, u32[]{:S(2)}) copy-start(bf16[24,32,512]{2,1,0:T(8,128)(2,1)} %param.25) | copy-start | bytes 2359300
  90.1 9.8 %copy-start.11 = (bf16[24,32,512]{2,1,0:T(8,128)(2,1)S(1)}, bf16[24,32,512]{2,1,0:T(8,128)(2,1)}, u32[]{:S(2)}) copy-start(bf16[24,32,512]{2,1,0:T(8,128)(2,1)} %param.26) | copy-start | bytes 2359300

commit v9 on v8

--- a/solution.py
+++ b/solution.py
@@ -1,6 +1,5 @@
 import jax
 import jax.numpy as jnp
-import numpy as np
 from jax import lax
 from jax.sharding import PartitionSpec as P
 
@@ -153,7 +152,7 @@
     gathered = spread(tokens, "tp", tp)
     dot = lambda a, w: jnp.dot(a, w, preferred_element_type=jnp.float32)
     half = DK // 2
-    inverse = (ROPE_BASE ** (-np.arange(half) / half)).astype(np.float32)
+    inverse = ROPE_BASE ** (-jnp.arange(half, dtype=jnp.float32) / half)
     positions = lax.optimization_barrier(lengths.astype(jnp.float32))
     angles = positions[:, None] * inverse[None, :]
     gaps = lax.optimization_barrier(gaps_to(positions, key_cache.shape[1], kv_at))

time: 225 us -> 225 us (level)
  no operation moved by 1% of the time
where the time goes in v9:
time: 225 us; the launch traced here: 224 us
  blocking collectives  168 us (75%)
  starting transfers between devices  44.7 us (20%)
  other arithmetic  5.31 us (2%)
  local copies, waits for them, and re-layouts  3.83 us (2%)
    all_to_all x10, blocking collectives, exchange(): lax.all_to_all(blocks, axis, split_axis=0, concat_axis=0, tiled=True, axi...  136 us
    all_to_all x1, starting transfers between devices, exchange(): lax.all_to_all(blocks, axis, split_axis=0, concat_axis=0, tiled=True, axi...  44.7 us
    all_gather x1, blocking collectives, local(): lax.all_gather(got.astype(jnp.bfloat16), 'kv', axis_index_groups=groups_f...  31.7 us
  transfers between devices with their start and end apart: 1, of which 1 were waited for; matrix products, arithmetic and copies ran while one was open for 2% of the time, Pallas kernels for 0%

profile of v9, /device:TPU:33, one launch (start us, length us, event | category | flops | bytes accessed | tf_op | source)
XLA Modules:
  0.0 224.2 jit_solution(3254286087748615964)
XLA Ops:
  0.0 0.8 broadcast_bitcast_fusion
  0.8 0.7 reshape.136
  1.5 44.7 %all-to-all-start = ((bf16[8,2,192]{2,1,0:T(2,128)(2,1)}), bf16[8,2,192]{2,1,0:T(2,128)(2,1)S(1)}, u32[]{:S(2)}, u32[]{:S(2)}) async-start(bf16[8,2,192]{2,1,0:T(2,128)(2,1)} %reshape.136), calls=%async_computation | async-start | bytes 16384 | tf_op jit(solution)/shard_map/all_to_all | solution.py:27
  46.2 0.7 convert_element_type.150
  46.8 0.1 broadcast_subtract_fusion
  46.9 0.0 copy-start.6
  46.9 1.0 multiply_convert_fusion.3
  48.0 0.0 copy-done.6
  48.0 0.0 copy-start.7
  48.0 0.1 exponential_select_fusion
  48.1 0.5 copy-done.7
  48.7 0.0 copy-start.8
  48.7 1.2 multiply_convert_fusion.1
  49.9 0.0 copy-done.2
  49.9 0.0 copy-done.3
  49.9 0.0 copy-done.4
  50.0 0.0 copy-done.5
  50.0 0.0 copy-done.8
  50.0 0.2 multiply_convert_fusion
  50.1 0.1 multiply_sine_fusion
  50.3 0.6 all-to-all-done
  50.8 0.1 reshape.137
  51.0 0.1 copy.46
  51.0 0.2 fusion.44
  51.3 0.0 copy-start.9
  51.4 7.1 %all_to_all.55 = bf16[4,56,128]{2,1,0:T(8,128)(2,1)S(1)} all-to-all(bf16[4,56,128]{2,1,0:T(8,128)(2,1)S(1)} %pad_maximum_fusion.1), channel_id=1, replica_groups={{0,8,16,24},{32,40,48,56},{64,72,80,88},{96,104,112,120},{128,136,144,1..., dimensions={0} | all-to-all | bytes 114688 | tf_op jit(solution)/shard_map/all_to_all | solution.py:27
  58.6 31.4 %all_to_all.56 = bf16[8,56,128]{2,1,0:T(8,128)(2,1)S(1)} all-to-all(bf16[8,56,128]{2,1,0:T(8,128)(2,1)S(1)} %broadcast_in_dim.36), channel_id=1, replica_groups={{0,32,64,96,128,160,192,224},{8,40,72,104,136,168,200,232},{16,48,80,11..., dimensions={0} | all-to-all | bytes 229376 | tf_op jit(solution)/shard_map/all_to_all | solution.py:27
  90.1 0.0 copy-start.10
  90.1 9.2 %all_to_all.57 = bf16[4,48,128]{2,1,0:T(8,128)(2,1)S(1)} all-to-all(bf16[4,48,128]{2,1,0:T(8,128)(2,1)S(1)} %broadcast_in_dim.37), channel_id=1, replica_groups={{0,8,16,24},{32,40,48,56},{64,72,80,88},{96,104,112,120},{128,136,144,1..., dimensions={0} | all-to-all | bytes 98304 | tf_op jit(solution)/shard_map/all_to_all | solution.py:27
  99.2 0.1 convert_multiply_fusion.1
  99.3 0.2 multiply_reduce_fusion.8
  99.5 0.3 fusion.3
  99.9 0.2 fusion
  100.1 0.2 fusion.38
  100.3 0.1 subtract_convert_fusion.1
  100.4 0.1 multiply_convert_fusion.4
  100.5 7.0 %all_to_all.58 = bf16[4,48,128]{2,1,0:T(8,128)(2,1)S(1)} all-to-all(bf16[4,48,128]{2,1,0:T(8,128)(2,1)S(1)} %maximum_maximum_fusion), channel_id=1, replica_groups={{0,8,16,24},{32,40,48,56},{64,72,80,88},{96,104,112,120},{128,136,144,1..., dimensions={0} | all-to-all | bytes 98304 | tf_op jit(solution)/shard_map/all_to_all | solution.py:27
  107.5 27.7 %all_to_all.59 = bf16[8,48,128]{2,1,0:T(8,128)(2,1)S(1)} all-to-all(bf16[8,48,128]{2,1,0:T(8,128)(2,1)S(1)} %broadcast_in_dim.38), channel_id=1, replica_groups={{0,32,64,96,128,160,192,224},{8,40,72,104,136,168,200,232},{16,48,80,11..., dimensions={0} | all-to-all | bytes 196608 | tf_op jit(solution)/shard_map/all_to_all | solution.py:27
  135.2 8.5 %all_to_all.60 = bf16[4,48,128]{2,1,0:T(8,128)(2,1)S(1)} all-to-all(bf16[4,48,128]{2,1,0:T(8,128)(2,1)S(1)} %broadcast_in_dim.39), channel_id=1, replica_groups={{0,8,16,24},{32,40,48,56},{64,72,80,88},{96,104,112,120},{128,136,144,1..., dimensions={0} | all-to-all | bytes 98304 | tf_op jit(solution)/shard_map/all_to_all | solution.py:27
  143.7 0.1 slice_reduce_fusion.2
  143.9 0.2 multiply_reduce_fusion.4
  144.1 0.1 multiply_convert_fusion.9
  144.2 0.1 convolution_convert_fusion.2
  144.4 14.9 %all_to_all.61 = bf16[8,24,128]{2,1,0:T(8,128)(2,1)S(1)} all-to-all(bf16[8,24,128]{2,1,0:T(8,128)(2,1)S(1)} %broadcast_in_dim.40), channel_id=1, replica_groups=mesh['grp'=2,'kv'=32,'tp'=8] {'tp'}, dimensions={0} | all-to-all | bytes 98304 | tf_op jit(solution)/shard_map/all_to_all | solution.py:27
  159.3 0.1 multiply_reduce_fusion.1
  159.4 0.2 convolution_convert_fusion
  159.6 0.1 fusion.42
  159.7 0.2 convolution_convert_fusion.1
  159.8 0.1 fusion.43
  159.9 0.1 copy.35
  160.0 0.1 concatenate.52
  160.1 0.1 concatenate.53
  160.2 0.1 concatenate.54
  160.3 0.1 concatenate.55
  160.4 7.9 %all_to_all.62 = bf16[4,24,768]{2,1,0:T(8,128)(2,1)S(1)} all-to-all(bf16[4,24,768]{2,1,0:T(8,128)(2,1)S(1)} %pad_maximum_fusion), channel_id=1, replica_groups={{0,8,16,24},{32,40,48,56},{64,72,80,88},{96,104,112,120},{128,136,144,1..., dimensions={0} | all-to-all | bytes 294912 | tf_op jit(solution)/shard_map/all_to_all | solution.py:27
  168.4 31.7 %all-gather = bf16[192,768]{1,0:T(8,128)(2,1)S(1)} all-gather(bf16[24,768]{1,0:T(8,128)(2,1)S(1)} %reduce_sum.249), channel_id=2, replica_groups={{0,32,64,96,128,160,192,224},{8,40,72,104,136,168,200,232},{16,48,80,11..., dimensions={0}, use_global_device_ids=true | all-gather | bytes 331776 | tf_op jit(solution)/shard_map/all_gather | solution.py:228
  200.1 0.2 fusion.22
  200.3 0.1 fusion.7
  200.4 7.0 %all_to_all.63 = bf16[4,24,384]{2,1,0:T(8,128)(2,1)S(1)} all-to-all(bf16[4,24,384]{2,1,0:T(8,128)(2,1)S(1)} %broadcast_in_dim.42), channel_id=1, replica_groups={{0,8,16,24},{32,40,48,56},{64,72,80,88},{96,104,112,120},{128,136,144,1..., dimensions={0} | all-to-all | bytes 147456 | tf_op jit(solution)/shard_map/all_to_all | solution.py:27
  207.4 0.1 concatenate.56
  207.6 0.2 convolution_convert_fusion.3
  207.8 15.7 %all_to_all.64 = bf16[8,24,128]{2,1,0:T(8,128)(2,1)S(1)} all-to-all(bf16[8,24,128]{2,1,0:T(8,128)(2,1)S(1)} %broadcast_in_dim.43), channel_id=1, replica_groups=mesh['grp'=2,'kv'=32,'tp'=8] {'tp'}, dimensions={0} | all-to-all | bytes 98304 | tf_op jit(solution)/shard_map/all_to_all | solution.py:27
  223.4 0.1 fusion.19
  223.5 0.7 copy.39
  (66 shorter events, 0.6 us)
Async XLA Ops:
  0.0 207.6 %copy-start = (bf16[1408,128]{1,0:T(8,128)(2,1)S(1)}, bf16[1408,128]{1,0:T(8,128)(2,1)}, u32[]{:S(2)}) copy-start(bf16[1408,128]{1,0:T(8,128)(2,1)} %param.31) | copy-start | bytes 1081348
  0.0 48.1 %copy-start.1 = (bf16[128,1408]{1,0:T(8,128)(2,1)S(1)}, bf16[128,1408]{1,0:T(8,128)(2,1)}, u32[]{:S(2)}) copy-start(bf16[128,1408]{1,0:T(8,128)(2,1)} %param.30) | copy-start | bytes 1081348
  1.5 49.4 %all-to-all-start = ((bf16[8,2,192]{2,1,0:T(2,128)(2,1)}), bf16[8,2,192]{2,1,0:T(2,128)(2,1)S(1)}, u32[]{:S(2)}, u32[]{:S(2)}) async-start(bf16[8,2,192]{2,1,0:T(2,128)(2,1)} %reshape.136), calls=%async_computation | async-start | bytes 16384 | tf_op jit(solution)/shard_map/all_to_all | solution.py:27
  46.9 1.1 copy-start.6
  48.0 0.7 copy-start.7
  48.6 1.3 copy-start.2
  48.6 1.3 copy-start.3
  48.6 1.3 copy-start.4
  48.7 1.3 copy-start.5
  48.7 1.3 copy-start.8
  51.3 48.2 %copy-start.9 = (bf16[24,32,512]{2,1,0:T(8,128)(2,1)S(1)}, bf16[24,32,512]{2,1,0:T(8,128)(2,1)}, u32[]{:S(2)}) copy-start(bf16[24,32,512]{2,1,0:T(8,128)(2,1)} %param.24) | copy-start | bytes 2359300
  90.1 9.8 %copy-start.10 = (bf16[24,32,512]{2,1,0:T(8,128)(2,1)S(1)}, bf16[24,32,512]{2,1,0:T(8,128)(2,1)}, u32[]{:S(2)}) copy-start(bf16[24,32,512]{2,1,0:T(8,128)(2,1)} %param.25) | copy-start | bytes 2359300

commit v10 on v9

--- a/solution.py
+++ b/solution.py
@@ -153,17 +153,24 @@
     dot = lambda a, w: jnp.dot(a, w, preferred_element_type=jnp.float32)
     half = DK // 2
     inverse = ROPE_BASE ** (-jnp.arange(half, dtype=jnp.float32) / half)
+    w_joint = with_gain(attn_gain, jnp.concatenate([w_query, w_key, w_value, w_gate], axis=1))
+    w_joint, ffn_gain, w_ffn_gate, w_ffn_up = lax.optimization_barrier(
+        (w_joint, ffn_gain, w_ffn_gate, w_ffn_up)
+    )
+    ffn_gained = (with_gain(ffn_gain, w_ffn_gate), with_gain(ffn_gain, w_ffn_up))
+    ffn_gained, lengths = lax.optimization_barrier((ffn_gained, lengths))
     positions = lax.optimization_barrier(lengths.astype(jnp.float32))
     angles = positions[:, None] * inverse[None, :]
     gaps = lax.optimization_barrier(gaps_to(positions, key_cache.shape[1], kv_at))
+    decays = decay_factors(gaps, log_decay)
+    decays, gn_gain, w_out = lax.optimization_barrier((decays, gn_gain, w_out))
     made = (
-        with_gain(attn_gain, jnp.concatenate([w_query, w_key, w_value, w_gate], axis=1)),
+        w_joint,
         with_gain(gn_gain, w_out),
-        with_gain(ffn_gain, w_ffn_gate),
-        with_gain(ffn_gain, w_ffn_up),
+        *ffn_gained,
         jnp.cos(angles),
         jnp.sin(angles),
-        decay_factors(gaps, log_decay),
+        decays,
     )
     gathered, made = lax.optimization_barrier((gathered, made))
     w_joint, out_gained, gate_gained, up_gained, cosine, sine, decays = made

time: 225 us -> 225 us (level)
  transfers between devices with their start and end apart: 1 -> 1, of which waited for: 1 -> 1; matrix products, arithmetic and copies ran while one was open for 2% -> 1% of each run, Pallas kernels for 0% -> 0%
where the time goes in v10:
time: 225 us; the launch traced here: 224 us
  blocking collectives  168 us (75%)
  starting transfers between devices  44.8 us (20%)
  local copies, waits for them, and re-layouts  5.12 us (2%)
  other arithmetic  3.86 us (2%)
    all_to_all x10, blocking collectives, exchange(): lax.all_to_all(blocks, axis, split_axis=0, concat_axis=0, tiled=True, axi...  136 us
    all_to_all x1, starting transfers between devices, exchange(): lax.all_to_all(blocks, axis, split_axis=0, concat_axis=0, tiled=True, axi...  44.8 us
    all_gather x1, blocking collectives, local(): lax.all_gather(got.astype(jnp.bfloat16), 'kv', axis_index_groups=groups_f...  31.7 us
  transfers between devices with their start and end apart: 1, of which 1 were waited for; matrix products, arithmetic and copies ran while one was open for 1% of the time, Pallas kernels for 0%

profile of v10, /device:TPU:33, one launch (start us, length us, event | category | flops | bytes accessed | tf_op | source)
XLA Modules:
  0.0 224.1 jit_solution(4653213031267758579)
XLA Ops:
  0.0 0.0 copy-start
  0.0 0.7 copy-done.4
  0.7 0.7 reshape.136
  1.5 44.8 %all-to-all-start = ((bf16[8,2,192]{2,1,0:T(2,128)(2,1)}), bf16[8,2,192]{2,1,0:T(2,128)(2,1)S(1)}, u32[]{:S(2)}, u32[]{:S(2)}) async-start(bf16[8,2,192]{2,1,0:T(2,128)(2,1)} %reshape.136), calls=%async_computation | async-start | bytes 16384 | tf_op jit(solution)/shard_map/all_to_all | solution.py:27
  46.3 0.0 copy-done.6
  46.3 0.0 copy-start.7
  46.3 1.3 multiply_convert_fusion
  47.6 0.0 copy-start.3
  47.7 0.2 multiply_convert_fusion.1
  47.9 0.0 copy-start.11
  47.9 0.6 copy-done.11
  48.5 0.1 broadcast_subtract_fusion
  48.6 0.0 copy-start.8
  48.6 0.6 copy-done.8
  49.3 0.1 exponential_select_fusion
  49.4 0.6 copy-done.5
  50.0 0.1 multiply_convert_fusion.3
  50.1 0.1 multiply_sine_fusion
  50.2 0.7 all-to-all-done
  51.0 0.1 reshape.137
  51.1 0.1 copy.46
  51.2 0.2 fusion.44
  51.5 0.0 copy-start.9
  51.5 7.1 %all_to_all.55 = bf16[4,56,128]{2,1,0:T(8,128)(2,1)S(1)} all-to-all(bf16[4,56,128]{2,1,0:T(8,128)(2,1)S(1)} %pad_maximum_fusion.1), channel_id=1, replica_groups={{0,8,16,24},{32,40,48,56},{64,72,80,88},{96,104,112,120},{128,136,144,1..., dimensions={0} | all-to-all | bytes 114688 | tf_op jit(solution)/shard_map/all_to_all | solution.py:27
  58.7 31.4 %all_to_all.56 = bf16[8,56,128]{2,1,0:T(8,128)(2,1)S(1)} all-to-all(bf16[8,56,128]{2,1,0:T(8,128)(2,1)S(1)} %broadcast_in_dim.36), channel_id=1, replica_groups={{0,32,64,96,128,160,192,224},{8,40,72,104,136,168,200,232},{16,48,80,11..., dimensions={0} | all-to-all | bytes 229376 | tf_op jit(solution)/shard_map/all_to_all | solution.py:27
  90.2 0.0 copy-start.10
  90.2 9.2 %all_to_all.57 = bf16[4,48,128]{2,1,0:T(8,128)(2,1)S(1)} all-to-all(bf16[4,48,128]{2,1,0:T(8,128)(2,1)S(1)} %broadcast_in_dim.37), channel_id=1, replica_groups={{0,8,16,24},{32,40,48,56},{64,72,80,88},{96,104,112,120},{128,136,144,1..., dimensions={0} | all-to-all | bytes 98304 | tf_op jit(solution)/shard_map/all_to_all | solution.py:27
  99.4 0.1 convert_multiply_fusion.1
  99.4 0.2 multiply_reduce_fusion.8
  99.6 0.0 copy-done.9
  99.6 0.3 fusion.3
  100.0 0.0 copy-done.10
  100.0 0.2 fusion
  100.2 0.2 fusion.38
  100.4 0.1 subtract_convert_fusion.1
  100.5 0.1 multiply_convert_fusion.4
  100.7 7.0 %all_to_all.58 = bf16[4,48,128]{2,1,0:T(8,128)(2,1)S(1)} all-to-all(bf16[4,48,128]{2,1,0:T(8,128)(2,1)S(1)} %maximum_maximum_fusion), channel_id=1, replica_groups={{0,8,16,24},{32,40,48,56},{64,72,80,88},{96,104,112,120},{128,136,144,1..., dimensions={0} | all-to-all | bytes 98304 | tf_op jit(solution)/shard_map/all_to_all | solution.py:27
  107.6 27.7 %all_to_all.59 = bf16[8,48,128]{2,1,0:T(8,128)(2,1)S(1)} all-to-all(bf16[8,48,128]{2,1,0:T(8,128)(2,1)S(1)} %broadcast_in_dim.38), channel_id=1, replica_groups={{0,32,64,96,128,160,192,224},{8,40,72,104,136,168,200,232},{16,48,80,11..., dimensions={0} | all-to-all | bytes 196608 | tf_op jit(solution)/shard_map/all_to_all | solution.py:27
  135.3 8.5 %all_to_all.60 = bf16[4,48,128]{2,1,0:T(8,128)(2,1)S(1)} all-to-all(bf16[4,48,128]{2,1,0:T(8,128)(2,1)S(1)} %broadcast_in_dim.39), channel_id=1, replica_groups={{0,8,16,24},{32,40,48,56},{64,72,80,88},{96,104,112,120},{128,136,144,1..., dimensions={0} | all-to-all | bytes 98304 | tf_op jit(solution)/shard_map/all_to_all | solution.py:27
  143.8 0.1 slice_reduce_fusion.2
  144.0 0.2 multiply_reduce_fusion.4
  144.2 0.1 multiply_convert_fusion.9
  144.3 0.1 convolution_convert_fusion.2
  144.5 14.7 %all_to_all.61 = bf16[8,24,128]{2,1,0:T(8,128)(2,1)S(1)} all-to-all(bf16[8,24,128]{2,1,0:T(8,128)(2,1)S(1)} %broadcast_in_dim.40), channel_id=1, replica_groups=mesh['grp'=2,'kv'=32,'tp'=8] {'tp'}, dimensions={0} | all-to-all | bytes 98304 | tf_op jit(solution)/shard_map/all_to_all | solution.py:27
  159.2 0.1 multiply_reduce_fusion.1
  159.3 0.2 convolution_convert_fusion
  159.5 0.1 fusion.42
  159.6 0.2 convolution_convert_fusion.1
  159.8 0.1 fusion.43
  159.9 0.1 copy.35
  160.0 0.1 concatenate.52
  160.1 0.1 concatenate.53
  160.2 0.1 concatenate.54
  160.3 0.1 concatenate.55
  160.4 7.9 %all_to_all.62 = bf16[4,24,768]{2,1,0:T(8,128)(2,1)S(1)} all-to-all(bf16[4,24,768]{2,1,0:T(8,128)(2,1)S(1)} %pad_maximum_fusion), channel_id=1, replica_groups={{0,8,16,24},{32,40,48,56},{64,72,80,88},{96,104,112,120},{128,136,144,1..., dimensions={0} | all-to-all | bytes 294912 | tf_op jit(solution)/shard_map/all_to_all | solution.py:27
  168.3 31.7 %all-gather = bf16[192,768]{1,0:T(8,128)(2,1)S(1)} all-gather(bf16[24,768]{1,0:T(8,128)(2,1)S(1)} %reduce_sum.249), channel_id=2, replica_groups={{0,32,64,96,128,160,192,224},{8,40,72,104,136,168,200,232},{16,48,80,11..., dimensions={0}, use_global_device_ids=true | all-gather | bytes 331776 | tf_op jit(solution)/shard_map/all_gather | solution.py:235
  200.0 0.2 fusion.22
  200.2 0.1 fusion.7
  200.4 7.0 %all_to_all.63 = bf16[4,24,384]{2,1,0:T(8,128)(2,1)S(1)} all-to-all(bf16[4,24,384]{2,1,0:T(8,128)(2,1)S(1)} %broadcast_in_dim.42), channel_id=1, replica_groups={{0,8,16,24},{32,40,48,56},{64,72,80,88},{96,104,112,120},{128,136,144,1..., dimensions={0} | all-to-all | bytes 147456 | tf_op jit(solution)/shard_map/all_to_all | solution.py:27
  207.4 0.1 concatenate.56
  207.5 0.2 convolution_convert_fusion.3
  207.7 15.7 %all_to_all.64 = bf16[8,24,128]{2,1,0:T(8,128)(2,1)S(1)} all-to-all(bf16[8,24,128]{2,1,0:T(8,128)(2,1)S(1)} %broadcast_in_dim.43), channel_id=1, replica_groups=mesh['grp'=2,'kv'=32,'tp'=8] {'tp'}, dimensions={0} | all-to-all | bytes 98304 | tf_op jit(solution)/shard_map/all_to_all | solution.py:27
  223.4 0.1 fusion.19
  223.5 0.7 copy.39
  (68 shorter events, 0.6 us)
Async XLA Ops:
  0.0 207.5 %copy-start = (bf16[1408,128]{1,0:T(8,128)(2,1)S(1)}, bf16[1408,128]{1,0:T(8,128)(2,1)}, u32[]{:S(2)}) copy-start(bf16[1408,128]{1,0:T(8,128)(2,1)} %param.31) | copy-start | bytes 1081348
  0.0 0.7 copy-start.4
  1.5 44.8 %copy-start.6 = (f32[128]{0:T(128)S(1)}, f32[128]{0:T(128)}, u32[]{:S(2)}) copy-start(f32[128]{0:T(128)} %param.18) | copy-start | bytes 1540
  1.5 49.5 %all-to-all-start = ((bf16[8,2,192]{2,1,0:T(2,128)(2,1)}), bf16[8,2,192]{2,1,0:T(2,128)(2,1)S(1)}, u32[]{:S(2)}, u32[]{:S(2)}) async-start(bf16[8,2,192]{2,1,0:T(2,128)(2,1)} %reshape.136), calls=%async_computation | async-start | bytes 16384 | tf_op jit(solution)/shard_map/all_to_all | solution.py:27
  46.3 1.3 copy-start.1
  46.3 1.4 copy-start.2
  46.3 1.4 copy-start.7
  47.6 1.7 copy-start.3
  47.9 0.7 copy-start.11
  48.6 0.7 copy-start.8
  49.3 0.7 copy-start.5
  51.5 48.2 %copy-start.9 = (bf16[24,32,512]{2,1,0:T(8,128)(2,1)S(1)}, bf16[24,32,512]{2,1,0:T(8,128)(2,1)}, u32[]{:S(2)}) copy-start(bf16[24,32,512]{2,1,0:T(8,128)(2,1)} %param.24) | copy-start | bytes 2359300
  90.2 9.8 %copy-start.10 = (bf16[24,32,512]{2,1,0:T(8,128)(2,1)S(1)}, bf16[24,32,512]{2,1,0:T(8,128)(2,1)}, u32[]{:S(2)}) copy-start(bf16[24,32,512]{2,1,0:T(8,128)(2,1)} %param.25) | copy-start | bytes 2359300

commit v11 on v10

--- a/solution.py
+++ b/solution.py
@@ -154,16 +154,16 @@
     half = DK // 2
     inverse = ROPE_BASE ** (-jnp.arange(half, dtype=jnp.float32) / half)
     w_joint = with_gain(attn_gain, jnp.concatenate([w_query, w_key, w_value, w_gate], axis=1))
-    w_joint, ffn_gain, w_ffn_gate, w_ffn_up = lax.optimization_barrier(
-        (w_joint, ffn_gain, w_ffn_gate, w_ffn_up)
+    w_joint, ffn_gain, w_ffn_gate, w_ffn_up, lengths, log_decay, gn_gain, w_out = (
+        lax.optimization_barrier(
+            (w_joint, ffn_gain, w_ffn_gate, w_ffn_up, lengths, log_decay, gn_gain, w_out)
+        )
     )
     ffn_gained = (with_gain(ffn_gain, w_ffn_gate), with_gain(ffn_gain, w_ffn_up))
-    ffn_gained, lengths = lax.optimization_barrier((ffn_gained, lengths))
     positions = lax.optimization_barrier(lengths.astype(jnp.float32))
     angles = positions[:, None] * inverse[None, :]
     gaps = lax.optimization_barrier(gaps_to(positions, key_cache.shape[1], kv_at))
     decays = decay_factors(gaps, log_decay)
-    decays, gn_gain, w_out = lax.optimization_barrier((decays, gn_gain, w_out))
     made = (
         w_joint,
         with_gain(gn_gain, w_out),

time: 225 us -> 224 us (level)
  no operation moved by 1% of the time
where the time goes in v11:
time: 224 us
  blocking collectives  167 us (75%)
  starting transfers between devices  44.8 us (20%)
  other arithmetic  3.88 us (2%)
  local copies, waits for them, and re-layouts  3.84 us (2%)
    all_to_all x10, blocking collectives, exchange(): lax.all_to_all(blocks, axis, split_axis=0, concat_axis=0, tiled=True, axi...  135 us
    all_to_all x1, starting transfers between devices, exchange(): lax.all_to_all(blocks, axis, split_axis=0, concat_axis=0, tiled=True, axi...  44.8 us
    all_gather x1, blocking collectives, local(): lax.all_gather(got.astype(jnp.bfloat16), 'kv', axis_index_groups=groups_f...  31.8 us
  transfers between devices with their start and end apart: 1, of which 1 were waited for; matrix products, arithmetic and copies ran while one was open for 1% of the time, Pallas kernels for 0%

profile of v11, /device:TPU:33, one launch (start us, length us, event | category | flops | bytes accessed | tf_op | source)
XLA Modules:
  0.0 223.6 jit_solution(3767349227332789888)
XLA Ops:
  0.0 0.0 copy-start
  0.0 0.7 copy-done.4
  0.7 0.7 reshape.136
  1.5 44.8 %all-to-all-start = ((bf16[8,2,192]{2,1,0:T(2,128)(2,1)}), bf16[8,2,192]{2,1,0:T(2,128)(2,1)S(1)}, u32[]{:S(2)}, u32[]{:S(2)}) async-start(bf16[8,2,192]{2,1,0:T(2,128)(2,1)} %reshape.136), calls=%async_computation | async-start | bytes 16384 | tf_op jit(solution)/shard_map/all_to_all | solution.py:27
  46.3 0.0 copy-done.6
  46.3 0.0 copy-start.5
  46.3 0.0 copy-start.7
  46.3 0.0 copy-start.2
  46.3 1.3 multiply_convert_fusion
  47.6 0.0 copy-done.11
  47.7 0.0 copy-start.1
  47.7 0.1 broadcast_subtract_fusion
  47.8 0.0 copy-done.3
  47.8 0.1 multiply_convert_fusion.3
  48.0 0.0 copy-start.8
  48.0 0.1 exponential_select_fusion
  48.1 0.6 copy-done.1
  48.6 0.2 multiply_convert_fusion.1
  48.9 0.1 multiply_sine_fusion
  49.0 2.0 all-to-all-done
  51.0 0.1 reshape.137
  51.1 0.1 copy.46
  51.2 0.2 fusion.44
  51.5 0.0 copy-start.9
  51.5 7.1 %all_to_all.55 = bf16[4,56,128]{2,1,0:T(8,128)(2,1)S(1)} all-to-all(bf16[4,56,128]{2,1,0:T(8,128)(2,1)S(1)} %pad_maximum_fusion.1), channel_id=1, replica_groups={{0,8,16,24},{32,40,48,56},{64,72,80,88},{96,104,112,120},{128,136,144,1..., dimensions={0} | all-to-all | bytes 114688 | tf_op jit(solution)/shard_map/all_to_all | solution.py:27
  58.7 31.4 %all_to_all.56 = bf16[8,56,128]{2,1,0:T(8,128)(2,1)S(1)} all-to-all(bf16[8,56,128]{2,1,0:T(8,128)(2,1)S(1)} %broadcast_in_dim.36), channel_id=1, replica_groups={{0,32,64,96,128,160,192,224},{8,40,72,104,136,168,200,232},{16,48,80,11..., dimensions={0} | all-to-all | bytes 229376 | tf_op jit(solution)/shard_map/all_to_all | solution.py:27
  90.2 0.0 copy-start.10
  90.2 9.2 %all_to_all.57 = bf16[4,48,128]{2,1,0:T(8,128)(2,1)S(1)} all-to-all(bf16[4,48,128]{2,1,0:T(8,128)(2,1)S(1)} %broadcast_in_dim.37), channel_id=1, replica_groups={{0,8,16,24},{32,40,48,56},{64,72,80,88},{96,104,112,120},{128,136,144,1..., dimensions={0} | all-to-all | bytes 98304 | tf_op jit(solution)/shard_map/all_to_all | solution.py:27
  99.4 0.1 convert_multiply_fusion.1
  99.4 0.2 multiply_reduce_fusion.8
  99.6 0.0 copy-done.9
  99.6 0.3 fusion.3
  100.0 0.2 fusion
  100.2 0.2 fusion.38
  100.4 0.1 subtract_convert_fusion.1
  100.6 0.1 multiply_convert_fusion.4
  100.7 7.0 %all_to_all.58 = bf16[4,48,128]{2,1,0:T(8,128)(2,1)S(1)} all-to-all(bf16[4,48,128]{2,1,0:T(8,128)(2,1)S(1)} %maximum_maximum_fusion), channel_id=1, replica_groups={{0,8,16,24},{32,40,48,56},{64,72,80,88},{96,104,112,120},{128,136,144,1..., dimensions={0} | all-to-all | bytes 98304 | tf_op jit(solution)/shard_map/all_to_all | solution.py:27
  107.6 27.7 %all_to_all.59 = bf16[8,48,128]{2,1,0:T(8,128)(2,1)S(1)} all-to-all(bf16[8,48,128]{2,1,0:T(8,128)(2,1)S(1)} %broadcast_in_dim.38), channel_id=1, replica_groups={{0,32,64,96,128,160,192,224},{8,40,72,104,136,168,200,232},{16,48,80,11..., dimensions={0} | all-to-all | bytes 196608 | tf_op jit(solution)/shard_map/all_to_all | solution.py:27
  135.3 8.5 %all_to_all.60 = bf16[4,48,128]{2,1,0:T(8,128)(2,1)S(1)} all-to-all(bf16[4,48,128]{2,1,0:T(8,128)(2,1)S(1)} %broadcast_in_dim.39), channel_id=1, replica_groups={{0,8,16,24},{32,40,48,56},{64,72,80,88},{96,104,112,120},{128,136,144,1..., dimensions={0} | all-to-all | bytes 98304 | tf_op jit(solution)/shard_map/all_to_all | solution.py:27
  143.8 0.1 slice_reduce_fusion.2
  144.0 0.2 multiply_reduce_fusion.4
  144.2 0.1 multiply_convert_fusion.9
  144.3 0.1 convolution_convert_fusion.2
  144.5 13.7 %all_to_all.61 = bf16[8,24,128]{2,1,0:T(8,128)(2,1)S(1)} all-to-all(bf16[8,24,128]{2,1,0:T(8,128)(2,1)S(1)} %broadcast_in_dim.40), channel_id=1, replica_groups=mesh['grp'=2,'kv'=32,'tp'=8] {'tp'}, dimensions={0} | all-to-all | bytes 98304 | tf_op jit(solution)/shard_map/all_to_all | solution.py:27
  158.2 0.1 multiply_reduce_fusion.1
  158.4 0.2 convolution_convert_fusion
  158.5 0.1 fusion.42
  158.6 0.2 convolution_convert_fusion.1
  158.8 0.1 fusion.43
  158.9 0.1 copy.35
  159.0 0.1 concatenate.52
  159.1 0.1 concatenate.53
  159.2 0.1 concatenate.54
  159.3 0.1 concatenate.55
  159.4 7.9 %all_to_all.62 = bf16[4,24,768]{2,1,0:T(8,128)(2,1)S(1)} all-to-all(bf16[4,24,768]{2,1,0:T(8,128)(2,1)S(1)} %pad_maximum_fusion), channel_id=1, replica_groups={{0,8,16,24},{32,40,48,56},{64,72,80,88},{96,104,112,120},{128,136,144,1..., dimensions={0} | all-to-all | bytes 294912 | tf_op jit(solution)/shard_map/all_to_all | solution.py:27
  167.4 31.8 %all-gather = bf16[192,768]{1,0:T(8,128)(2,1)S(1)} all-gather(bf16[24,768]{1,0:T(8,128)(2,1)S(1)} %reduce_sum.249), channel_id=2, replica_groups={{0,32,64,96,128,160,192,224},{8,40,72,104,136,168,200,232},{16,48,80,11..., dimensions={0}, use_global_device_ids=true | all-gather | bytes 331776 | tf_op jit(solution)/shard_map/all_gather | solution.py:235
  199.2 0.2 fusion.22
  199.4 0.1 fusion.7
  199.5 7.2 %all_to_all.63 = bf16[4,24,384]{2,1,0:T(8,128)(2,1)S(1)} all-to-all(bf16[4,24,384]{2,1,0:T(8,128)(2,1)S(1)} %broadcast_in_dim.42), channel_id=1, replica_groups={{0,8,16,24},{32,40,48,56},{64,72,80,88},{96,104,112,120},{128,136,144,1..., dimensions={0} | all-to-all | bytes 147456 | tf_op jit(solution)/shard_map/all_to_all | solution.py:27
  206.7 0.1 concatenate.56
  206.8 0.2 convolution_convert_fusion.3
  207.0 15.8 %all_to_all.64 = bf16[8,24,128]{2,1,0:T(8,128)(2,1)S(1)} all-to-all(bf16[8,24,128]{2,1,0:T(8,128)(2,1)S(1)} %broadcast_in_dim.43), channel_id=1, replica_groups=mesh['grp'=2,'kv'=32,'tp'=8] {'tp'}, dimensions={0} | all-to-all | bytes 98304 | tf_op jit(solution)/shard_map/all_to_all | solution.py:27
  222.8 0.1 fusion.19
  222.9 0.7 copy.39
  (68 shorter events, 0.6 us)
Async XLA Ops:
  0.0 206.8 %copy-start = (bf16[1408,128]{1,0:T(8,128)(2,1)S(1)}, bf16[1408,128]{1,0:T(8,128)(2,1)}, u32[]{:S(2)}) copy-start(bf16[1408,128]{1,0:T(8,128)(2,1)} %param.31) | copy-start | bytes 1081348
  0.0 0.7 copy-start.4
  1.5 44.8 %copy-start.6 = (f32[128]{0:T(128)S(1)}, f32[128]{0:T(128)}, u32[]{:S(2)}) copy-start(f32[128]{0:T(128)} %param.18) | copy-start | bytes 1540
  1.5 49.5 %all-to-all-start = ((bf16[8,2,192]{2,1,0:T(2,128)(2,1)}), bf16[8,2,192]{2,1,0:T(2,128)(2,1)S(1)}, u32[]{:S(2)}, u32[]{:S(2)}) async-start(bf16[8,2,192]{2,1,0:T(2,128)(2,1)} %reshape.136), calls=%async_computation | async-start | bytes 16384 | tf_op jit(solution)/shard_map/all_to_all | solution.py:27
  46.3 1.4 copy-start.11
  46.3 1.5 copy-start.3
  46.3 1.5 copy-start.5
  46.3 1.7 copy-start.7
  46.3 1.8 copy-start.2
  47.7 1.0 copy-start.1
  48.0 0.7 copy-start.8
  51.5 48.2 %copy-start.9 = (bf16[24,32,512]{2,1,0:T(8,128)(2,1)S(1)}, bf16[24,32,512]{2,1,0:T(8,128)(2,1)}, u32[]{:S(2)}) copy-start(bf16[24,32,512]{2,1,0:T(8,128)(2,1)} %param.24) | copy-start | bytes 2359300
  90.2 9.8 %copy-start.10 = (bf16[24,32,512]{2,1,0:T(8,128)(2,1)S(1)}, bf16[24,32,512]{2,1,0:T(8,128)(2,1)}, u32[]{:S(2)}) copy-start(bf16[24,32,512]{2,1,0:T(8,128)(2,1)} %param.25) | copy-start | bytes 2359300
